TPU v7x, 256 devices: a whole 4x4x8 slice. The times are simulated.
256 devices in a mesh: tp: 256 (over z, y, x, core).
Axes of the slice: x: 4, y: 4, z: 8, core: 2. Of those that a mesh axis runs over, the one named last changes fastest.
Arguments:
- tokens: bfloat16 [32, 4096], replicated, may hold values from -18 to 18
- norm_gain: float32 [2, 4096], replicated, may hold values from 0.1 to 1.9
- w_gate: bfloat16 [2, 4096, 8192], P(None, None, 'tp'), may hold values from -0.09375 to 0.09375
- w_value: bfloat16 [2, 4096, 8192], P(None, None, 'tp'), may hold values from -0.09375 to 0.09375
- w_write: bfloat16 [2, 4096, 1024], P(None, None, 'tp'), may hold values from -0.09375 to 0.09375
- w_read: bfloat16 [2, 4096, 1024], P(None, None, 'tp'), may hold values from -0.09375 to 0.09375
- w_step: bfloat16 [2, 4096, 128], replicated, may hold values from -0.09375 to 0.09375
- step_bias: float32 [2, 128], replicated, may hold values from -2 to 1
- decay_rate: float32 [2, 128], replicated, may hold values from 0.05 to 3
- skip_gain: float32 [2, 128], replicated, may hold values from 1 to 4
- conv_value_weight: float32 [2, 3, 8192], P(None, None, 'tp'), may hold values from -2.5 to 2.5
- conv_key_weight: float32 [2, 3, 2, 1024], P(None, None, None, 'tp'), may hold values from -2.5 to 2.5
- group_gain: float32 [2, 8192], P(None, 'tp'), may hold values from 0.1 to 1.9
- w_out: bfloat16 [2, 8192, 4096], P(None, 'tp'), may hold values from -0.0625 to 0.0625
- ssm_state: float32 [2, 32, 8192, 128], P(None, None, 'tp'), may hold values from -3 to 3
- conv_value: float32 [2, 32, 2, 8192], P(None, None, None, 'tp'), may hold values from -5 to 5
- conv_key: float32 [2, 32, 2, 2, 1024], P(None, None, None, None, 'tp'), may hold values from -5 to 5
Outputs:
- tokens_out: bfloat16 [32, 4096], replicated
- ssm_state_out: float32 [2, 32, 8192, 128], P(None, None, 'tp')
- conv_value_out: float32 [2, 32, 2, 8192], P(None, None, None, 'tp')
- conv_key_out: float32 [2, 32, 2, 2, 1024], P(None, None, None, None, 'tp')
All inputs are finite; a program needn't handle non-finite values.
Results may differ from a plain program's by a relative error of at most 0.011.
Values may be sent and summed in bfloat16 or wider, within the bound.
No kernel may reach another device: no remote copies, remote signals or barrier semaphores. Data moves between devices by JAX's collectives and lax.ppermute only.
A program may use at most 64 MiB of HBM per device.

v0:
```python
import jax
import jax.numpy as jnp
from jax import lax
from jax.sharding import Mesh
from jax.sharding import PartitionSpec as P

D = 4096
HEAD_DIM = 64
GROUPS = 8
STATE = 128
LAYERS = 2
HEADS = 128
GW = 1024
TP = ("tp_0", "tp_1", "tp_2", "tp_3")


EPS = 1e-06


def from_everyone(value, axis):
    copies = jnp.broadcast_to(value, (lax.axis_size(axis), *value.shape))
    return lax.all_to_all(copies, axis, split_axis=0, concat_axis=0, tiled=True)


def joined_along(pieces, dim):
    lengths = list(pieces.shape[1:])
    lengths[dim] *= pieces.shape[0]
    return jnp.moveaxis(pieces, 0, dim).reshape(lengths)


def whole_of(value, axes, dim):
    far, near = axes
    initial = from_everyone(value, far)
    pieces = jnp.swapaxes(from_everyone(initial, near), 0, 1)
    return joined_along(pieces.reshape(-1, *value.shape), dim)


def taken_together(value, axis):
    return from_everyone(value, axis).sum(axis=0)


def one_axis_at_a_time(value, axes):
    far, near = axes
    return taken_together(taken_together(value, near), far)


def split_up(value, dim, count):
    lengths = value.shape
    pieces = value.reshape(*lengths[:dim], count, lengths[dim] // count, *lengths[dim + 1 :])
    return jnp.moveaxis(pieces, dim, 0)


def summed_on_arrival(value, axis, dim):
    pieces = split_up(value, dim, lax.axis_size(axis))
    arrived = lax.all_to_all(pieces, axis, split_axis=0, concat_axis=0, tiled=True)
    return arrived.astype(jnp.float32).sum(axis=0)


def summed_rows(value, axes, dim):
    far, near = axes
    own = summed_on_arrival(split_up(value, dim, lax.axis_size(far)), near, dim + 1)
    return jnp.sum(
        lax.all_to_all(own.astype(jnp.bfloat16), far, 0, 0, tiled=True).astype(jnp.float32), axis=0
    )


def filled_up(lines, count):
    spare = -lines.shape[0] % count
    if not spare:
        return lines
    return jnp.concatenate([lines, jnp.zeros((spare, *lines.shape[1:]), lines.dtype)])


def nested_sum(value, axes):
    lines = value.reshape(-1)
    own = summed_rows(filled_up(lines, lax.axis_size(axes[0]) * lax.axis_size(axes[1])), axes, 0)
    whole = whole_of(own.astype(jnp.bfloat16), axes, 0)
    return whole[: len(lines)].reshape(value.shape).astype(jnp.float32)


def per_device(
    tokens,
    norm_gain,
    w_gate,
    w_value,
    w_write,
    w_read,
    w_step,
    step_bias,
    decay_rate,
    skip_gain,
    conv_value_weight,
    conv_key_weight,
    group_gain,
    w_out,
    ssm_state,
    conv_value,
    conv_key,
):
    highest = lax.Precision.HIGHEST
    chan_count = w_gate.shape[2]
    position = lax.axis_index(TP)
    first_chan = position * chan_count
    chan_ids = first_chan + jnp.arange(chan_count, dtype=jnp.int32)
    my_group = first_chan // GW
    head_hot = (
        (chan_ids // HEAD_DIM)[:, None] == jnp.arange(HEADS, dtype=jnp.int32)[None, :]
    ).astype(jnp.float32)
    group_hot = ((chan_ids // GW)[:, None] == jnp.arange(GROUPS, dtype=jnp.int32)[None, :]).astype(
        jnp.float32
    )
    hidden = tokens
    ssm_list = []
    value_list = []
    key_list = []
    for layer in range(LAYERS):
        resid = hidden.astype(jnp.float32)
        inv_scale = lax.rsqrt(jnp.sum(resid * resid, axis=1) / D + EPS)[:, None]
        scaled = (resid * norm_gain[layer]).astype(jnp.bfloat16)

        def project(weight):
            return jnp.dot(scaled, weight[layer], preferred_element_type=jnp.float32) * inv_scale

        gate_in = project(w_gate)
        value_in = project(w_value)
        write_in = project(w_write)
        read_in = project(w_read)
        step_in = project(w_step)
        value_window = jnp.concatenate([conv_value[layer], value_in[:, None, :]], axis=1)
        value_list.append(value_window[:, 1:])
        values = jax.nn.silu(jnp.sum(value_window * conv_value_weight[layer][None], axis=1))
        fresh = jnp.stack([write_in, read_in], axis=1)[:, None]
        key_window = jnp.concatenate([conv_key[layer], fresh], axis=1)
        key_list.append(key_window[:, 1:])
        mixed_keys = jax.nn.silu(jnp.sum(key_window * conv_key_weight[layer][None], axis=1))
        every_group = whole_of(mixed_keys, (("tp_0", "tp_1"), ("tp_2", "tp_3")), 2)
        by_entry = every_group.reshape(every_group.shape[0], 2, STATE, GROUPS)
        own_keys = lax.dynamic_slice_in_dim(by_entry, my_group, 1, 3)[..., 0]
        writes = own_keys[:, 0]
        reads = own_keys[:, 1]
        delta = jax.nn.softplus(step_in + step_bias[layer][None])
        decay = jnp.exp(-delta * decay_rate[layer][None])
        delta_chan = jnp.dot(delta, head_hot.T, precision=highest)
        decay_chan = jnp.dot(decay, head_hot.T, precision=highest)
        skip_chan = jnp.dot(skip_gain[layer], head_hot.T, precision=highest)
        state = (
            decay_chan[..., None] * ssm_state[layer]
            + (delta_chan * values)[..., None] * writes[:, None, :]
        )
        ssm_list.append(state)
        read_out = jnp.sum(state * reads[:, None, :], axis=2) + skip_chan[None] * values
        gated = read_out * jax.nn.silu(gate_in)
        squares = jnp.dot(gated * gated, group_hot, precision=highest)
        square_total = one_axis_at_a_time(squares, (("tp_0", "tp_1"), ("tp_2", "tp_3")))
        group_scale = lax.rsqrt(square_total / GW + EPS)
        scale_chan = jnp.dot(group_scale, group_hot.T, precision=highest)
        normed = (gated * scale_chan * group_gain[layer][None]).astype(jnp.bfloat16)
        partial_out = jnp.dot(normed, w_out[layer], preferred_element_type=jnp.float32)
        update = nested_sum(partial_out.astype(jnp.bfloat16), (("tp_0", "tp_1"), ("tp_2", "tp_3")))
        hidden = (resid + update).astype(jnp.bfloat16)
    return (hidden, jnp.stack(ssm_list), jnp.stack(value_list), jnp.stack(key_list))


def solution(mesh):
    torus = Mesh(mesh.devices.reshape(8, 4, 4, 2), ("tp_0", "tp_1", "tp_2", "tp_3"))
    in_specs = (
        P(),
        P(),
        P(None, None, TP),
        P(None, None, TP),
        P(None, None, TP),
        P(None, None, TP),
        P(),
        P(),
        P(),
        P(),
        P(None, None, TP),
        P(None, None, None, TP),
        P(None, TP),
        P(None, TP, None),
        P(None, None, TP, None),
        P(None, None, None, TP),
        P(None, None, None, None, TP),
    )
    out_specs = (
        P(),
        P(None, None, TP, None),
        P(None, None, None, TP),
        P(None, None, None, None, TP),
    )
    return jax.shard_map(
        per_device, mesh=torus, in_specs=in_specs, out_specs=out_specs, check_vma=False
    )
```

profile of v0, /device:TPU:1, one launch (start us, length us, event | category | flops | bytes accessed | tf_op | source)
XLA Modules:
  0.0 231.6 jit_solution(5091522746502764204)
XLA Ops:
  7.3 12.0 %all-to-all-start = ((f32[32,1,256]{2,1,0:T(1,128)}), f32[32,1,256]{2,1,0:T(1,128)S(1)}, u32[]{:S(2)}, u32[]{:S(2)}) async-start(f32[32,1,256]{2,1,0:T(1,128)} %reshape.91), calls=%async_computation | async-start | bytes 65536 | tf_op jit(solution)/shard_map/all_to_all | solution.py:22
  20.1 1.2 convolution_multiply_fusion.9
  21.4 1.5 compare_select_fusion.1
  23.4 4.6 %all-to-all-done = f32[32,1,256]{2,1,0:T(1,128)S(1)} async-done(((f32[32,1,256]{2,1,0:T(1,128)}), f32[32,1,256]{2,1,0:T(1,128)S(1)}, u32[]{:S(2)}, u32[]{:S(2)}) %all-to-all-start) | async-done | bytes 32800 | tf_op jit(solution)/shard_map/all_to_all | solution.py:22
  30.7 6.4 %all-to-all-start.1 = ((f32[8,1,8192]{2,1,0:T(1,128)}), f32[8,1,8192]{2,1,0:T(1,128)S(1)}, u32[]{:S(2)}, u32[]{:S(2)}) async-start(f32[8,1,8192]{2,1,0:T(1,128)} %reshape.93), calls=%async_computation.1 | async-start | bytes 524288 | tf_op jit(solution)/shard_map/all_to_all | solution.py:22
  37.3 6.3 %all-to-all-done.1 = f32[8,1,8192]{2,1,0:T(1,128)S(1)} async-done(((f32[8,1,8192]{2,1,0:T(1,128)}), f32[8,1,8192]{2,1,0:T(1,128)S(1)}, u32[]{:S(2)}, u32[]{:S(2)}) %all-to-all-start.1) | async-done | bytes 262176 | tf_op jit(solution)/shard_map/all_to_all | solution.py:22
  43.6 1.3 reduce.7
  47.9 8.0 %all_to_all.96 = f32[8,1,256]{2,1,0:T(1,128)S(1)} all-to-all(f32[8,1,256]{2,1,0:T(1,128)S(1)} %reshape.95), channel_id=1, replica_groups=mesh['tp_0'=8,'tp_1'=4,'tp_2'=4,'tp_3'=2] {'tp_2','tp_3'}, dimensions={0} | all-to-all | bytes 16384 | tf_op jit(solution)/shard_map/all_to_all | solution.py:22
  57.5 3.9 %all-to-all-start.3 = ((f32[32,1,256]{2,1,0:T(1,128)}), f32[32,1,256]{2,1,0:T(1,128)S(1)}, u32[]{:S(2)}, u32[]{:S(2)}) async-start(f32[32,1,256]{2,1,0:T(1,128)} %reshape.97), calls=%async_computation.3 | async-start | bytes 65536 | tf_op jit(solution)/shard_map/all_to_all | solution.py:22
  61.3 8.6 %all-to-all-done.3 = f32[32,1,256]{2,1,0:T(1,128)S(1)} async-done(((f32[32,1,256]{2,1,0:T(1,128)}), f32[32,1,256]{2,1,0:T(1,128)S(1)}, u32[]{:S(2)}, u32[]{:S(2)}) %all-to-all-start.3) | async-done | bytes 32800 | tf_op jit(solution)/shard_map/all_to_all | solution.py:22
  71.3 11.0 %all_to_all.97 = bf16[8,32,512]{2,1,0:T(8,128)(2,1)S(1)} all-to-all(bf16[8,32,512]{2,1,0:T(8,128)(2,1)S(1)} %bitcast.227), channel_id=1, replica_groups=mesh['tp_0'=8,'tp_1'=4,'tp_2'=4,'tp_3'=2] {'tp_2','tp_3'}, dimensions={0} | all-to-all | bytes 524288 | tf_op jit(solution)/shard_map/all_to_all | solution.py:55
  83.5 11.6 %all_to_all.98 = bf16[32,2,256]{2,1,0:T(2,128)(2,1)S(1)} all-to-all(bf16[32,2,256]{2,1,0:T(2,128)(2,1)S(1)} %reshape.99), channel_id=1, replica_groups=mesh['tp_0'=8,'tp_1'=4,'tp_2'=4,'tp_3'=2] {'tp_0','tp_1'}, dimensions={0} | all-to-all | bytes 65536 | tf_op jit(solution)/shard_map/all_to_all | solution.py:63
  96.1 11.7 %all_to_all.99 = bf16[32,2,256]{2,1,0:T(2,128)(2,1)S(1)} all-to-all(bf16[32,2,256]{2,1,0:T(2,128)(2,1)S(1)} %reshape.101), channel_id=1, replica_groups=mesh['tp_0'=8,'tp_1'=4,'tp_2'=4,'tp_3'=2] {'tp_0','tp_1'}, dimensions={0} | all-to-all | bytes 65536 | tf_op jit(solution)/shard_map/all_to_all | solution.py:22
  108.6 6.8 %all-to-all-start.7 = ((bf16[8,32,512]{2,1,0:T(8,128)(2,1)}), bf16[8,32,512]{2,1,0:T(8,128)(2,1)S(1)}, u32[]{:S(2)}, u32[]{:S(2)}) async-start(bf16[8,32,512]{2,1,0:T(8,128)(2,1)} %broadcast_in_dim.67), calls=%async_computation.7 | async-start | bytes 524288 | tf_op jit(solution)/shard_map/all_to_all | solution.py:22
  115.5 6.4 %all-to-all-done.7 = bf16[8,32,512]{2,1,0:T(8,128)(2,1)S(1)} async-done(((bf16[8,32,512]{2,1,0:T(8,128)(2,1)}), bf16[8,32,512]{2,1,0:T(8,128)(2,1)S(1)}, u32[]{:S(2)}, u32[]{:S(2)}) %all-to-all-start.7) | async-done | bytes 262176 | tf_op jit(solution)/shard_map/all_to_all | solution.py:22
  123.7 3.9 %all-to-all-start.8 = ((f32[32,1,256]{2,1,0:T(1,128)}), f32[32,1,256]{2,1,0:T(1,128)S(1)}, u32[]{:S(2)}, u32[]{:S(2)}) async-start(f32[32,1,256]{2,1,0:T(1,128)} %reshape.103), calls=%async_computation.8 | async-start | bytes 65536 | tf_op jit(solution)/shard_map/all_to_all | solution.py:22
  127.5 1.5 compare_select_fusion
  129.3 6.9 %all-to-all-done.8 = f32[32,1,256]{2,1,0:T(1,128)S(1)} async-done(((f32[32,1,256]{2,1,0:T(1,128)}), f32[32,1,256]{2,1,0:T(1,128)S(1)}, u32[]{:S(2)}, u32[]{:S(2)}) %all-to-all-start.8) | async-done | bytes 32800 | tf_op jit(solution)/shard_map/all_to_all | solution.py:22
  137.2 1.2 reshape.105
  138.4 5.5 %all-to-all-start.9 = ((f32[8,1,8192]{2,1,0:T(1,128)}), f32[8,1,8192]{2,1,0:T(1,128)S(1)}, u32[]{:S(2)}, u32[]{:S(2)}) async-start(f32[8,1,8192]{2,1,0:T(1,128)} %reshape.105), calls=%async_computation.9 | async-start | bytes 524288 | tf_op jit(solution)/shard_map/all_to_all | solution.py:22
  144.1 6.2 %all-to-all-done.9 = f32[8,1,8192]{2,1,0:T(1,128)S(1)} async-done(((f32[8,1,8192]{2,1,0:T(1,128)}), f32[8,1,8192]{2,1,0:T(1,128)S(1)}, u32[]{:S(2)}, u32[]{:S(2)}) %all-to-all-start.9) | async-done | bytes 262176 | tf_op jit(solution)/shard_map/all_to_all | solution.py:22
  150.4 1.3 reduce.13
  154.7 8.0 %all_to_all.100 = f32[8,1,256]{2,1,0:T(1,128)S(1)} all-to-all(f32[8,1,256]{2,1,0:T(1,128)S(1)} %reshape.107), channel_id=1, replica_groups=mesh['tp_0'=8,'tp_1'=4,'tp_2'=4,'tp_3'=2] {'tp_2','tp_3'}, dimensions={0} | all-to-all | bytes 16384 | tf_op jit(solution)/shard_map/all_to_all | solution.py:22
  163.6 11.6 %all_to_all.101 = f32[32,1,256]{2,1,0:T(1,128)S(1)} all-to-all(f32[32,1,256]{2,1,0:T(1,128)S(1)} %reshape.109), channel_id=1, replica_groups=mesh['tp_0'=8,'tp_1'=4,'tp_2'=4,'tp_3'=2] {'tp_0','tp_1'}, dimensions={0} | all-to-all | bytes 65536 | tf_op jit(solution)/shard_map/all_to_all | solution.py:22
  177.2 5.2 %all-to-all-start.12 = ((bf16[8,32,512]{2,1,0:T(8,128)(2,1)}), bf16[8,32,512]{2,1,0:T(8,128)(2,1)S(1)}, u32[]{:S(2)}, u32[]{:S(2)}) async-start(bf16[8,32,512]{2,1,0:T(8,128)(2,1)} %bitcast.213), calls=%async_computation.12 | async-start | bytes 524288 | tf_op jit(solution)/shard_map/all_to_all | solution.py:55
  183.1 5.7 %all-to-all-done.12 = bf16[8,32,512]{2,1,0:T(8,128)(2,1)S(1)} async-done(((bf16[8,32,512]{2,1,0:T(8,128)(2,1)}), bf16[8,32,512]{2,1,0:T(8,128)(2,1)S(1)}, u32[]{:S(2)}, u32[]{:S(2)}) %all-to-all-start.12) | async-done | bytes 262176 | tf_op jit(solution)/shard_map/all_to_all | solution.py:55
  190.2 3.9 %all-to-all-start.13 = ((bf16[32,2,256]{2,1,0:T(2,128)(2,1)}), bf16[32,2,256]{2,1,0:T(2,128)(2,1)S(1)}, u32[]{:S(2)}, u32[]{:S(2)}) async-start(bf16[32,2,256]{2,1,0:T(2,128)(2,1)} %reshape.111), calls=%async_computation.13 | async-start | bytes 65536 | tf_op jit(solution)/shard_map/all_to_all | solution.py:63
  194.1 8.6 %all-to-all-done.13 = bf16[32,2,256]{2,1,0:T(2,128)(2,1)S(1)} async-done(((bf16[32,2,256]{2,1,0:T(2,128)(2,1)}), bf16[32,2,256]{2,1,0:T(2,128)(2,1)S(1)}, u32[]{:S(2)}, u32[]{:S(2)}) %all-to-all-start.13) | async-done | bytes 32800 | tf_op jit(solution)/shard_map/all_to_all | solution.py:63
  204.3 3.9 %all-to-all-start.14 = ((bf16[32,2,256]{2,1,0:T(2,128)(2,1)}), bf16[32,2,256]{2,1,0:T(2,128)(2,1)S(1)}, u32[]{:S(2)}, u32[]{:S(2)}) async-start(bf16[32,2,256]{2,1,0:T(2,128)(2,1)} %reshape.113), calls=%async_computation.14 | async-start | bytes 65536 | tf_op jit(solution)/shard_map/all_to_all | solution.py:22
  208.8 8.0 %all-to-all-done.14 = bf16[32,2,256]{2,1,0:T(2,128)(2,1)S(1)} async-done(((bf16[32,2,256]{2,1,0:T(2,128)(2,1)}), bf16[32,2,256]{2,1,0:T(2,128)(2,1)S(1)}, u32[]{:S(2)}, u32[]{:S(2)}) %all-to-all-start.14) | async-done | bytes 32800 | tf_op jit(solution)/shard_map/all_to_all | solution.py:22
  217.6 6.7 %all-to-all-start.15 = ((bf16[8,32,512]{2,1,0:T(8,128)(2,1)}), bf16[8,32,512]{2,1,0:T(8,128)(2,1)S(1)}, u32[]{:S(2)}, u32[]{:S(2)}) async-start(bf16[8,32,512]{2,1,0:T(8,128)(2,1)} %broadcast_in_dim.75), calls=%async_computation.15 | async-start | bytes 524288 | tf_op jit(solution)/shard_map/all_to_all | solution.py:22
  226.0 4.8 %all-to-all-done.15 = bf16[8,32,512]{2,1,0:T(8,128)(2,1)S(1)} async-done(((bf16[8,32,512]{2,1,0:T(8,128)(2,1)}), bf16[8,32,512]{2,1,0:T(8,128)(2,1)S(1)}, u32[]{:S(2)}, u32[]{:S(2)}) %all-to-all-start.15) | async-done | bytes 262176 | tf_op jit(solution)/shard_map/all_to_all | solution.py:22
  (155 shorter events, 36.3 us)
Async XLA Ops:
  0.6 20.8 %copy-start.1 = (bf16[32,4096]{1,0:T(8,128)(2,1)S(1)}, bf16[32,4096]{1,0:T(8,128)(2,1)}, u32[]{:S(2)}) copy-start(bf16[32,4096]{1,0:T(8,128)(2,1)} %param.17) | copy-start | bytes 786436
  0.6 20.7 %copy-start.3 = (f32[2,32,2,32]{3,2,1,0:T(2,128)S(1)}, f32[2,32,2,32]{3,2,1,0:T(2,128)}, u32[]{:S(2)}) copy-start(f32[2,32,2,32]{3,2,1,0:T(2,128)} %param.32) | copy-start | bytes 49156
  0.7 20.7 %copy-start.4 = (f32[2,3,32]{2,0,1:T(2,128)S(1)}, f32[2,3,32]{2,0,1:T(2,128)}, u32[]{:S(2)}) copy-start(f32[2,3,32]{2,0,1:T(2,128)} %param.27) | copy-start | bytes 2308
  0.7 20.7 %copy-start.5 = (f32[2,128]{1,0:T(2,128)S(1)}, f32[2,128]{1,0:T(2,128)}, u32[]{:S(2)}) copy-start(f32[2,128]{1,0:T(2,128)} %param.25) | copy-start | bytes 3076
  0.7 22.6 %copy-start.12 = (f32[2,128]{1,0:T(2,128)S(1)}, f32[2,128]{1,0:T(2,128)}, u32[]{:S(2)}) copy-start(f32[2,128]{1,0:T(2,128)} %param.26) | copy-start | bytes 3076
  7.3 20.7 %all-to-all-start = ((f32[32,1,256]{2,1,0:T(1,128)}), f32[32,1,256]{2,1,0:T(1,128)S(1)}, u32[]{:S(2)}, u32[]{:S(2)}) async-start(f32[32,1,256]{2,1,0:T(1,128)} %reshape.91), calls=%async_computation | async-start | bytes 65536 | tf_op jit(solution)/shard_map/all_to_all | solution.py:22
  30.7 12.9 %all-to-all-start.1 = ((f32[8,1,8192]{2,1,0:T(1,128)}), f32[8,1,8192]{2,1,0:T(1,128)S(1)}, u32[]{:S(2)}, u32[]{:S(2)}) async-start(f32[8,1,8192]{2,1,0:T(1,128)} %reshape.93), calls=%async_computation.1 | async-start | bytes 524288 | tf_op jit(solution)/shard_map/all_to_all | solution.py:22
  45.3 1.5 copy-start
  45.9 1.4 copy-start.8
  45.9 15.4 %copy-start.6 = (f32[2,32]{1,0:T(2,128)S(1)}, f32[2,32]{1,0:T(2,128)}, u32[]{:S(2)}) copy-start(f32[2,32]{1,0:T(2,128)} %param.29) | copy-start | bytes 772
  45.9 25.1 %copy-start.2 = (bf16[2,32,4096]{2,1,0:T(8,128)(2,1)S(1)}, bf16[2,32,4096]{2,1,0:T(8,128)(2,1)}, u32[]{:S(2)}) copy-start(bf16[2,32,4096]{2,1,0:T(8,128)(2,1)} %param.30) | copy-start | bytes 1572868
  57.5 12.5 %all-to-all-start.3 = ((f32[32,1,256]{2,1,0:T(1,128)}), f32[32,1,256]{2,1,0:T(1,128)S(1)}, u32[]{:S(2)}, u32[]{:S(2)}) async-start(f32[32,1,256]{2,1,0:T(1,128)} %reshape.97), calls=%async_computation.3 | async-start | bytes 65536 | tf_op jit(solution)/shard_map/all_to_all | solution.py:22
  95.3 26.9 %copy-start.10 = (bf16[2,4096,4]{1,2,0:T(4,128)(2,1)S(1)}, bf16[2,4096,4]{1,2,0:T(4,128)(2,1)}, u32[]{:S(2)}) copy-start(bf16[2,4096,4]{1,2,0:T(4,128)(2,1)} %param.22) | copy-start | bytes 196612
  107.8 14.5 %copy-start.11 = (bf16[2,4096,4]{1,2,0:T(4,128)(2,1)S(1)}, bf16[2,4096,4]{1,2,0:T(4,128)(2,1)}, u32[]{:S(2)}) copy-start(bf16[2,4096,4]{1,2,0:T(4,128)(2,1)} %param.21) | copy-start | bytes 196612
  108.6 14.0 %copy-start.7 = (bf16[2,4096,32]{1,2,0:T(8,128)(2,1)S(1)}, bf16[2,4096,32]{1,2,0:T(8,128)(2,1)}, u32[]{:S(2)}) copy-start(bf16[2,4096,32]{1,2,0:T(8,128)(2,1)} %param.20) | copy-start | bytes 1572868
  108.6 13.3 %all-to-all-start.7 = ((bf16[8,32,512]{2,1,0:T(8,128)(2,1)}), bf16[8,32,512]{2,1,0:T(8,128)(2,1)S(1)}, u32[]{:S(2)}, u32[]{:S(2)}) async-start(bf16[8,32,512]{2,1,0:T(8,128)(2,1)} %broadcast_in_dim.67), calls=%async_computation.7 | async-start | bytes 524288 | tf_op jit(solution)/shard_map/all_to_all | solution.py:22
  123.7 12.5 %all-to-all-start.8 = ((f32[32,1,256]{2,1,0:T(1,128)}), f32[32,1,256]{2,1,0:T(1,128)S(1)}, u32[]{:S(2)}, u32[]{:S(2)}) async-start(f32[32,1,256]{2,1,0:T(1,128)} %reshape.103), calls=%async_computation.8 | async-start | bytes 65536 | tf_op jit(solution)/shard_map/all_to_all | solution.py:22
  138.4 12.0 %all-to-all-start.9 = ((f32[8,1,8192]{2,1,0:T(1,128)}), f32[8,1,8192]{2,1,0:T(1,128)S(1)}, u32[]{:S(2)}, u32[]{:S(2)}) async-start(f32[8,1,8192]{2,1,0:T(1,128)} %reshape.105), calls=%async_computation.9 | async-start | bytes 524288 | tf_op jit(solution)/shard_map/all_to_all | solution.py:22
  152.7 1.4 copy-start.9
  177.2 11.7 %all-to-all-start.12 = ((bf16[8,32,512]{2,1,0:T(8,128)(2,1)}), bf16[8,32,512]{2,1,0:T(8,128)(2,1)S(1)}, u32[]{:S(2)}, u32[]{:S(2)}) async-start(bf16[8,32,512]{2,1,0:T(8,128)(2,1)} %bitcast.213), calls=%async_computation.12 | async-start | bytes 524288 | tf_op jit(solution)/shard_map/all_to_all | solution.py:55
  190.2 12.5 %all-to-all-start.13 = ((bf16[32,2,256]{2,1,0:T(2,128)(2,1)}), bf16[32,2,256]{2,1,0:T(2,128)(2,1)S(1)}, u32[]{:S(2)}, u32[]{:S(2)}) async-start(bf16[32,2,256]{2,1,0:T(2,128)(2,1)} %reshape.111), calls=%async_computation.13 | async-start | bytes 65536 | tf_op jit(solution)/shard_map/all_to_all | solution.py:63
  204.3 12.5 %all-to-all-start.14 = ((bf16[32,2,256]{2,1,0:T(2,128)(2,1)}), bf16[32,2,256]{2,1,0:T(2,128)(2,1)S(1)}, u32[]{:S(2)}, u32[]{:S(2)}) async-start(bf16[32,2,256]{2,1,0:T(2,128)(2,1)} %reshape.113), calls=%async_computation.14 | async-start | bytes 65536 | tf_op jit(solution)/shard_map/all_to_all | solution.py:22
  217.6 13.2 %all-to-all-start.15 = ((bf16[8,32,512]{2,1,0:T(8,128)(2,1)}), bf16[8,32,512]{2,1,0:T(8,128)(2,1)S(1)}, u32[]{:S(2)}, u32[]{:S(2)}) async-start(bf16[8,32,512]{2,1,0:T(8,128)(2,1)} %broadcast_in_dim.75), calls=%async_computation.15 | async-start | bytes 524288 | tf_op jit(solution)/shard_map/all_to_all | solution.py:22
where the time goes:
time: 233 us; the launch traced here: 232 us
  waiting for transfers between devices  66.1 us (28%)
  blocking collectives  61.8 us (27%)
  starting transfers between devices  57.9 us (25%)
  local copies, waits for them, and re-layouts  17.5 us (8%)
  other arithmetic  16.8 us (7%)
  matrix products  9.95 us (4%)
    all_to_all x8, waiting for transfers between devices, from_everyone(): return lax.all_to_all(copies, axis, split_axis=0, concat_axis=0, tiled=True)  51.8 us
    all_to_all x8, starting transfers between devices, from_everyone(): return lax.all_to_all(copies, axis, split_axis=0, concat_axis=0, tiled=True)  48.9 us
    all_to_all x4, blocking collectives, from_everyone(): return lax.all_to_all(copies, axis, split_axis=0, concat_axis=0, tiled=True)  39.3 us
    all_to_all x1, blocking collectives, summed_rows(): lax.all_to_all(own.astype(jnp.bfloat16), far, 0, 0, tiled=True)  11.6 us
    all_to_all x1, blocking collectives, summed_on_arrival(): lax.all_to_all(pieces, axis, split_axis=0, concat_axis=0, tiled=True)  11 us
    all_to_all x1, waiting for transfers between devices, summed_rows(): lax.all_to_all(own.astype(jnp.bfloat16), far, 0, 0, tiled=True)  8.62 us
    unnamed x62, local copies, waits for them, and re-layouts  7.93 us
    dot_general x10, matrix products, project(): jnp.dot(scaled, weight[layer], preferred_element_type=jnp.float32)  7.6 us
  transfers between devices with their start and end apart: 10, of which 10 were waited for; matrix products, arithmetic and copies ran while one was open for 4% of the time, Pallas kernels for 0%

commit v1 on v0

v1 whole, which is shorter than its diff:
```python
import functools

import jax
import jax.numpy as jnp
from jax import lax
from jax.experimental import pallas as pl
from jax.experimental.pallas import tpu as pltpu
from jax.sharding import Mesh
from jax.sharding import PartitionSpec as P

D = 4096
B = 32
CH = 32
N = 128
GW = 1024
EPS = 1e-06
TP = ("z", "y", "x", "c")
PLANE = ("y", "x", "c")
F32 = jnp.float32
BF16 = jnp.bfloat16


def vmem():
    return pl.BlockSpec(memory_space=pltpu.VMEM)


def anywhere():
    return pl.BlockSpec(memory_space=pl.ANY)


def shaped(shape, dtype):
    return jax.ShapeDtypeStruct(shape, dtype)


def silu(v):
    return v / (1.0 + jnp.exp(-v))


def as_col(row):
    n = row.shape[1]
    at = lax.broadcasted_iota(jnp.int32, (n, n), 0)
    of = lax.broadcasted_iota(jnp.int32, (n, n), 1)
    return jnp.sum(jnp.where(at == of, row, 0.0), axis=1, keepdims=True)


def as_row(col):
    n = col.shape[0]
    at = lax.broadcasted_iota(jnp.int32, (n, n), 0)
    of = lax.broadcasted_iota(jnp.int32, (n, n), 1)
    return jnp.sum(jnp.where(at == of, col, 0.0), axis=0, keepdims=True)


def dot_nt(a, b):
    return lax.dot_general(a, b, (((1,), (1,)), ((), ())), preferred_element_type=F32)


def keys_kernel(layer, spot, hid, gain, w_write, w_read, conv, taps, *rest):
    if layer:
        before, msg, conv_out, scaled, inv_out = rest
    else:
        msg, conv_out, scaled, inv_out = rest
    squares = jnp.zeros((B, 128), F32)
    for j in range(D // 128):
        cols = slice(128 * j, 128 * j + 128)
        part = (hid[j] if layer else hid[:, cols]).astype(F32)
        squares += part * part
        scaled[:, cols] = (part * gain[layer : layer + 1, cols]).astype(BF16)
    inv = lax.rsqrt(jnp.sum(squares, axis=1, keepdims=True) / D + EPS)
    inv_out[...] = jnp.broadcast_to(inv, (B, 128))
    inv_row = as_row(inv)
    mixed = []
    for kind, weight in ((0, w_write), (1, w_read)):
        fresh = dot_nt(weight[layer], scaled[...]) * inv_row
        old, newer = conv[layer, 0, kind], conv[layer, 1, kind]
        tap = [as_col(taps[layer, k, kind : kind + 1, :]) for k in range(3)]
        mixed.append(silu(old * tap[0] + newer * tap[1] + fresh * tap[2]))
        if layer:
            conv_out[0, 0, kind] = before[0, kind]
            conv_out[0, 1, kind] = before[1, kind]
            conv_out[1, 0, kind] = newer
            conv_out[1, 1, kind] = fresh
        else:
            conv_out[0, kind] = newer
            conv_out[1, kind] = fresh
    lines = jnp.concatenate([mixed[0], mixed[1], jnp.zeros((4, 128 - 2 * B), F32)], axis=1)
    core = spot[2]
    for plane in range(8):
        line = lines[plane % 4 : plane % 4 + 1]
        line = jnp.where(core == plane // 4, line, 0.0)
        block = jnp.broadcast_to(line, (16, 128))
        msg[0, plane] = block
        msg[1, plane] = block


def make_keys(layer, spot, hid, gain, w_write, w_read, conv, taps, before):
    args = [spot, hid, gain, w_write, w_read, conv, taps]
    conv_shape = (2, 2, 4, B)
    if layer:
        args.append(before)
        conv_shape = (2, *conv_shape)
    return pl.pallas_call(
        functools.partial(keys_kernel, layer),
        in_specs=[pl.BlockSpec(memory_space=pltpu.SMEM)] + [vmem()] * (len(args) - 1),
        out_specs=[vmem()] * 4,
        out_shape=[
            shaped((2, 8, 16, 128), F32),
            shaped(conv_shape, F32),
            shaped((B, D), BF16),
            shaped((B, 128), F32),
        ],
        name=f"keys{layer}",
    )(*args)


def values_kernel(layer, spot, scaled, inv, w_gate, w_value, w_step, bias, rate, skip, conv, taps, *rest):
    if layer:
        before, packed, conv_out = rest
    else:
        packed, conv_out = rest
    hidden = scaled[...]
    inv_col = inv[:, :CH]
    gate = dot_nt(hidden, w_gate[layer]) * inv_col
    fresh = dot_nt(hidden, w_value[layer]) * inv_col
    step = jnp.dot(hidden, w_step[layer], preferred_element_type=F32) * inv[...]
    old, newer = conv[layer, :, 0, :], conv[layer, :, 1, :]
    tap = [taps[k, layer : layer + 1, :] for k in range(3)]
    values = silu(old * tap[0] + newer * tap[1] + fresh * tap[2])
    if layer:
        conv_out[0] = before[...]
        conv_out[1, :, 0, :] = newer
        conv_out[1, :, 1, :] = fresh
    else:
        conv_out[:, 0, :] = newer
        conv_out[:, 1, :] = fresh
    head = spot[1]
    mine = lax.broadcasted_iota(jnp.int32, (1, 128), 1) == head

    def of_head(table):
        return jnp.sum(jnp.where(mine, table, 0.0), axis=1, keepdims=True)

    raw = of_head(step + bias[layer : layer + 1, :])
    delta = jnp.maximum(raw, 0.0) + jnp.log1p(jnp.exp(-jnp.abs(raw)))
    decay = jnp.exp(-delta * of_head(rate[layer : layer + 1, :]))
    packed[0] = (delta * values).T
    packed[1] = of_head(skip[layer : layer + 1, :]) * values
    packed[2] = silu(gate)
    packed[3] = jnp.broadcast_to(decay, (B, CH))


def make_values(layer, spot, scaled, inv, w_gate, w_value, w_step, bias, rate, skip, conv, taps, before):
    args = [spot, scaled, inv, w_gate, w_value, w_step, bias, rate, skip, conv, taps]
    specs = [pl.BlockSpec(memory_space=pltpu.SMEM), vmem(), vmem()]
    specs += [vmem()] * 8
    conv_shape = (B, 2, CH)
    if layer:
        args.append(before)
        specs.append(vmem())
        conv_shape = (2, *conv_shape)
    return pl.pallas_call(
        functools.partial(values_kernel, layer),
        in_specs=specs,
        out_specs=[vmem()] * 2,
        out_shape=[shaped((4, B, CH), F32), shaped(conv_shape, F32)],
        name=f"values{layer}",
    )(*args)


def mix_kernel(layer, keys, packed, state, gain, w_out, *rest):
    states_out, sent, fresh, sem = rest[-4:]
    both = (keys[0] + keys[1]).T
    writes, reads = both[:B], both[B : 2 * B]
    push = packed[0]
    decay = packed[3]
    lane = lax.broadcasted_iota(jnp.int32, (CH, B), 1)
    found = jnp.zeros((CH, B), F32)
    for b in range(B):
        new = decay[b : b + 1, :1] * state[layer, b] + push[:, b : b + 1] * writes[b : b + 1]
        fresh[b] = new
        total = jnp.sum(new * reads[b : b + 1], axis=1, keepdims=True)
        found = jnp.where(lane == b, total, found)
    write_back = pltpu.make_async_copy(fresh, states_out.at[layer], sem)
    write_back.start()
    gated = (found.T + packed[1]) * packed[2]
    total = as_row(jnp.sum(gated * gated, axis=1, keepdims=True))
    high = total.astype(BF16).astype(F32)
    low = total - high
    row = lax.broadcasted_iota(jnp.int32, (8, B), 0)
    tail = jnp.where(row == 0, high, jnp.where(row == 1, low, 0.0))
    tail = jnp.concatenate([tail, jnp.zeros((8, 128 - B), F32)], axis=1).astype(BF16)
    out = jnp.dot((gated * gain[layer : layer + 1, :]).astype(BF16), w_out[layer], preferred_element_type=F32)
    for j in range(D // 128):
        sent[j, :B] = out[:, 128 * j : 128 * j + 128].astype(BF16)
        sent[j, B:] = tail
    write_back.wait()


def make_mix(layer, keys, packed, state, gain, w_out, states_out):
    args = [keys, packed, state, gain, w_out]
    specs = [vmem()] * 5
    aliases = {}
    if layer:
        args.append(states_out)
        specs.append(anywhere())
        aliases = {5: 0}
    return pl.pallas_call(
        functools.partial(mix_kernel, layer),
        in_specs=specs,
        out_specs=[anywhere(), vmem()],
        out_shape=[shaped(state.shape, F32), shaped((32, 40, 128), BF16)],
        scratch_shapes=[pltpu.VMEM((B, CH, N), F32), pltpu.SemaphoreType.DMA],
        input_output_aliases=aliases,
        name=f"mix{layer}",
    )(*args)


def scale_kernel(got, sent):
    total = got[0].astype(F32)
    for j in range(1, 32):
        total += got[j].astype(F32)
    squares = total[B : B + 1, :B] + total[B + 1 : B + 2, :B]
    factor = as_col(lax.rsqrt(squares / GW + EPS))
    chunk = (total[:B] * factor).astype(BF16)
    for plane in range(8):
        sent[plane] = chunk


def make_scale(got):
    return pl.pallas_call(
        scale_kernel,
        in_specs=[vmem()],
        out_specs=vmem(),
        out_shape=shaped((8, B, 128), BF16),
        name="scale",
    )(got)


def add_kernel(layer, spot, got, hid, sent):
    total = got[0].astype(F32)
    for plane in range(1, 8):
        total += got[plane].astype(F32)
    at = spot[0]
    if layer:
        own = hid[at]
    else:
        own = hid[:, pl.ds(pl.multiple_of(128 * at, 128), 128)]
    chunk = (own.astype(F32) + total).astype(BF16)
    for j in range(32):
        sent[j] = chunk


def make_add(layer, spot, got, hid):
    return pl.pallas_call(
        functools.partial(add_kernel, layer),
        in_specs=[pl.BlockSpec(memory_space=pltpu.SMEM), vmem(), vmem()],
        out_specs=vmem(),
        out_shape=shaped((32, B, 128), BF16),
        name=f"add{layer}",
    )(spot, got, hid)


def exchange(value, axes):
    return lax.all_to_all(value, axes, split_axis=0, concat_axis=0, tiled=True)


def per_device(
    tokens,
    norm_gain,
    w_gate,
    w_value,
    w_write,
    w_read,
    w_step,
    step_bias,
    decay_rate,
    skip_gain,
    conv_value_weight,
    conv_key_weight,
    group_gain,
    w_out,
    ssm_state,
    conv_value,
    conv_key,
):
    core = lax.axis_index("c")
    place = lax.axis_index(PLANE)
    head = lax.axis_index(("z", "y", "x"))
    spot = jnp.stack([place, head, core]).astype(jnp.int32)
    w_gate, w_value, w_write, w_read = (jnp.swapaxes(w, 1, 2) for w in (w_gate, w_value, w_write, w_read))
    conv_key = jnp.transpose(conv_key, (0, 2, 3, 4, 1))
    value_taps = jnp.swapaxes(conv_value_weight, 0, 1)
    hid = tokens
    states = key_out = value_out = None
    for layer in range(2):
        msg, key_out, scaled, inv = make_keys(
            layer, spot, hid, norm_gain, w_write, w_read, conv_key, conv_key_weight, key_out
        )
        keys = exchange(msg.reshape(256, 128), ("c", "z", "y", "x")).reshape(2, 128, 128)
        packed, value_out = make_values(
            layer, spot, scaled, inv, w_gate, w_value, w_step, step_bias, decay_rate, skip_gain,
            conv_value, value_taps, value_out,
        )
        states, sent = make_mix(layer, keys, packed, ssm_state, group_gain, w_out, states)
        sent = make_scale(exchange(sent, PLANE))
        sent = make_add(layer, spot, exchange(sent, ("z",)), hid)
        hid = exchange(sent, PLANE)
    tokens_out = jnp.transpose(hid, (1, 0, 2)).reshape(B, D)
    return (tokens_out, states, value_out, jnp.transpose(key_out, (0, 4, 1, 2, 3)))


def solution(mesh):
    torus = Mesh(mesh.devices.reshape(8, 4, 4, 2), TP)
    in_specs = (
        P(),
        P(),
        P(None, None, TP),
        P(None, None, TP),
        P(None, None, TP),
        P(None, None, TP),
        P(),
        P(),
        P(),
        P(),
        P(None, None, TP),
        P(None, None, None, TP),
        P(None, TP),
        P(None, TP, None),
        P(None, None, TP, None),
        P(None, None, None, TP),
        P(None, None, None, None, TP),
    )
    out_specs = (
        P(),
        P(None, None, TP, None),
        P(None, None, None, TP),
        P(None, None, None, None, TP),
    )
    return jax.shard_map(
        per_device, mesh=torus, in_specs=in_specs, out_specs=out_specs, check_vma=False
    )
```

time: 233 us -> 152 us (0.65)
  waiting for transfers between devices: 66.1 us -> 19.7 us
  starting transfers between devices: 57.9 us -> 20.8 us
  Pallas kernels: 0 us -> 27.7 us
  blocking collectives: 61.8 us -> 79.2 us
  other arithmetic: 16.8 us -> 0.61 us
  local copies, waits for them, and re-layouts: 17.5 us -> 2.03 us
  matrix products: 9.95 us -> 0 us
    all_to_all x10 -> x2, waiting for transfers between devices: 66.1 us -> 19.7 us  [exchange(): return lax.all_to_all(value, axes, split_axis=0, concat_axis=0, tiled=True)]
    all_to_all x10 -> x2, starting transfers between devices: 57.9 us -> 20.8 us  [exchange(): return lax.all_to_all(value, axes, split_axis=0, concat_axis=0, tiled=True)]
    pallas_call x0 -> x10, Pallas kernels: none -> 27.7 us  [the longest x2 10.1 us: make_mix(): pl.pallas_call(functools.partial(mix_kernel, layer), in_specs=specs, out_...]
    all_to_all x6, blocking collectives: 61.8 us -> 79.2 us  [exchange(): return lax.all_to_all(value, axes, split_axis=0, concat_axis=0, tiled=True)]
    dot_general x22 -> x0, matrix products: 9.95 us -> none  [the longest x10 7.6 us: project(): jnp.dot(scaled, weight[layer], preferred_element_type=jnp.float32)]
    all_to_all x10 -> x0, other arithmetic: 8.04 us -> none  [the longest x8 6.73 us: from_everyone(): return lax.all_to_all(copies, axis, split_axis=0, concat_axis=0, tiled=True)]
    unnamed x62 -> x4, local copies, waits for them, and re-layouts: 7.93 us -> 1.31 us
    reduce_sum x16 -> x0, other arithmetic: 2.98 us -> none  [the longest x2 1.31 us: per_device(): inv_scale = lax.rsqrt(jnp.sum(resid * resid, axis=1) / D + EPS)[:, None]]
  transfers between devices with their start and end apart: 10 -> 2, of which waited for: 10 -> 2; matrix products, arithmetic and copies ran while one was open for 4% -> 0% of each run, Pallas kernels for 0% -> 4%
where the time goes in v1:
time: 152 us; the launch traced here: 151 us
  blocking collectives  79.2 us (52%)
  Pallas kernels  27.7 us (18%)
  starting transfers between devices  20.8 us (14%)
  waiting for transfers between devices  19.7 us (13%)
  local copies, waits for them, and re-layouts  2.03 us (1%)
    all_to_all x6, blocking collectives, exchange(): return lax.all_to_all(value, axes, split_axis=0, concat_axis=0, tiled=True)  79.2 us
    all_to_all x2, starting transfers between devices, exchange(): return lax.all_to_all(value, axes, split_axis=0, concat_axis=0, tiled=True)  20.8 us
    all_to_all x2, waiting for transfers between devices, exchange(): return lax.all_to_all(value, axes, split_axis=0, concat_axis=0, tiled=True)  19.7 us
    pallas_call x2, Pallas kernels, make_mix(): pl.pallas_call(functools.partial(mix_kernel, layer), in_specs=specs, out_...  10.1 us
    pallas_call x2, Pallas kernels, make_values(): pl.pallas_call(functools.partial(values_kernel, layer), in_specs=specs, o...  6.58 us
    pallas_call x2, Pallas kernels, make_keys(): pl.pallas_call(functools.partial(keys_kernel, layer), in_specs=[pl.BlockS...  4.11 us
    pallas_call x2, Pallas kernels, make_scale(): pl.pallas_call(scale_kernel, in_specs=[vmem()], out_specs=vmem(), out_sha...  3.46 us
    pallas_call x2, Pallas kernels, make_add(): pl.pallas_call(functools.partial(add_kernel, layer), in_specs=[pl.BlockSp...  3.46 us
  transfers between devices with their start and end apart: 2, of which 2 were waited for; matrix products, arithmetic and copies ran while one was open for 0% of the time, Pallas kernels for 4%

profile of v1, /device:TPU:1, one launch (start us, length us, event | category | flops | bytes accessed | tf_op | source)
XLA Modules:
  0.0 150.8 jit_solution(17282667041314457090)
XLA Ops:
  0.6 0.6 pad_add_fusion.spot
  1.3 2.1 %keys0.1 = (f32[2,8,16,128]{3,2,1,0:T(8,128)}, f32[2,2,4,32]{3,2,1,0:T(4,128)}, bf16[32,4096]{1,0:T(8,128)(2,1)}, f32[32,128]{1,0:T(8,128)}) custom-call(s32[3]{0:T(128)} %pad_add_fusion.spot, bf16[32,4096]{1,0:T(8,128)(2,1)} %hid.3, f32[2,4096]{1,0:T(2,128)} %gain.6, bf16[2,4,4096]{2,1,0:T(4,128)(2,1)} %bitcast.30, bf16[2,4,4096]{2,1,0:T(4,128)(2,1)} %bitcast.32, ...), custom_call_target="tpu_custom_call" | custom-call | tf_op jit(solution)/shard_map/keys0/pallas_call | solution.py:101
  3.3 15.6 %all-to-all-start = ((f32[256,1,128]{2,1,0:T(1,128)}), f32[256,1,128]{2,1,0:T(1,128)S(1)}, u32[]{:S(2)}, u32[]{:S(2)}) async-start(f32[256,1,128]{2,1,0:T(1,128)} %bitcast.35), calls=%async_computation | async-start | bytes 262144 | tf_op jit(solution)/shard_map/all_to_all | solution.py:262
  19.0 3.3 %values0.1 = (f32[4,32,32]{2,1,0:T(8,128)}, f32[32,2,32]{2,1,0:T(2,128)}) custom-call(s32[3]{0:T(128)} %pad_add_fusion.spot, bf16[32,4096]{1,0:T(8,128)(2,1)} %get-tuple-element.21.scaled, f32[32,128]{1,0:T(8,128)} %get-tuple-element.22.inv, bf16[2,32,4096]{2,1,0:T(8,128)(2,1)} %bitcast.24, bf16[2,32,4096]{2,1,0:T(8,128)(2,1)} %bitcast.26, ...), custom_call_target="tpu_custom_call" | custom-call | tf_op jit(solution)/shard_map/values0/pallas_call | solution.py:159
  22.2 9.8 %all-to-all-done = f32[256,1,128]{2,1,0:T(1,128)S(1)} async-done(((f32[256,1,128]{2,1,0:T(1,128)}), f32[256,1,128]{2,1,0:T(1,128)S(1)}, u32[]{:S(2)}, u32[]{:S(2)}) %all-to-all-start) | async-done | bytes 131104 | tf_op jit(solution)/shard_map/all_to_all | solution.py:262
  32.0 0.0 copy-start.1
  32.0 0.7 copy-done.1
  32.7 5.1 %mix0.1 = (f32[2,32,32,128]{3,2,1,0:T(8,128)}, bf16[32,40,128]{2,1,0:T(8,128)(2,1)}) custom-call(f32[2,128,128]{2,1,0:T(8,128)} %bitcast.29, f32[4,32,32]{2,1,0:T(8,128)} %get-tuple-element.23.packed, f32[2,32,32,128]{3,2,1,0:T(8,128)} %state.3, f32[2,32]{1,0:T(2,128)} %gain.7, bf16[2,32,4096]{2,1,0:T(8,128)(2,1)} %w_out.3), custom_call_target="tpu_custom_call" | custom-call | tf_op jit(solution)/shard_map/mix0/pallas_call | solution.py:205
  37.7 14.1 %all_to_all.48.got = bf16[32,40,128]{2,1,0:T(8,128)(2,1)} all-to-all(bf16[32,40,128]{2,1,0:T(8,128)(2,1)} %get-tuple-element.24), channel_id=1, replica_groups=mesh['z'=8,'y'=4,'x'=4,'c'=2] {'y','x','c'}, dimensions={0} | all-to-all | bytes 655360 | tf_op jit(solution)/shard_map/all_to_all | solution.py:262
  51.8 1.7 %scale.2 = bf16[8,32,128]{2,1,0:T(8,128)(2,1)} custom-call(bf16[32,40,128]{2,1,0:T(8,128)(2,1)} %all_to_all.48.got), custom_call_target="tpu_custom_call" | custom-call | tf_op jit(solution)/shard_map/scale/pallas_call | solution.py:228
  53.6 11.1 %all_to_all.49.got = bf16[8,32,128]{2,1,0:T(8,128)(2,1)} all-to-all(bf16[8,32,128]{2,1,0:T(8,128)(2,1)} %scale.2), channel_id=1, replica_groups=mesh['z'=8,'y'=4,'x'=4,'c'=2] {'z'}, dimensions={0} | all-to-all | bytes 131072 | tf_op jit(solution)/shard_map/all_to_all | solution.py:262
  64.7 1.7 %add0.1 = bf16[32,32,128]{2,1,0:T(8,128)(2,1)} custom-call(s32[3]{0:T(128)} %pad_add_fusion.spot, bf16[8,32,128]{2,1,0:T(8,128)(2,1)} %all_to_all.49.got, bf16[32,4096]{1,0:T(8,128)(2,1)} %hid.3), custom_call_target="tpu_custom_call" | custom-call | tf_op jit(solution)/shard_map/add0/pallas_call | solution.py:252
  66.4 14.7 %all_to_all.50.hid = bf16[32,32,128]{2,1,0:T(8,128)(2,1)} all-to-all(bf16[32,32,128]{2,1,0:T(8,128)(2,1)} %add0.1), channel_id=1, replica_groups=mesh['z'=8,'y'=4,'x'=4,'c'=2] {'y','x','c'}, dimensions={0} | all-to-all | bytes 524288 | tf_op jit(solution)/shard_map/all_to_all | solution.py:262
  81.1 2.1 %keys1.1 = (f32[2,8,16,128]{3,2,1,0:T(8,128)}, f32[2,2,2,4,32]{4,3,2,1,0:T(4,128)}, bf16[32,4096]{1,0:T(8,128)(2,1)}, f32[32,128]{1,0:T(8,128)}) custom-call(s32[3]{0:T(128)} %pad_add_fusion.spot, bf16[32,32,128]{2,1,0:T(8,128)(2,1)} %all_to_all.50.hid, f32[2,4096]{1,0:T(2,128)} %gain.6, bf16[2,4,4096]{2,1,0:T(4,128)(2,1)} %bitcast.31, ...), custom_call_target="tpu_custom_call" | custom-call | tf_op jit(solution)/shard_map/keys1/pallas_call | solution.py:101
  83.2 5.2 %all-to-all-start.4 = ((f32[256,1,128]{2,1,0:T(1,128)}), f32[256,1,128]{2,1,0:T(1,128)S(1)}, u32[]{:S(2)}, u32[]{:S(2)}) async-start(f32[256,1,128]{2,1,0:T(1,128)} %bitcast.34), calls=%async_computation.4 | async-start | bytes 262144 | tf_op jit(solution)/shard_map/all_to_all | solution.py:262
  88.4 3.3 %values1.1 = (f32[4,32,32]{2,1,0:T(8,128)}, f32[2,32,2,32]{3,2,1,0:T(2,128)}) custom-call(s32[3]{0:T(128)} %pad_add_fusion.spot, bf16[32,4096]{1,0:T(8,128)(2,1)} %get-tuple-element.27.scaled, f32[32,128]{1,0:T(8,128)} %get-tuple-element.28.inv, bf16[2,32,4096]{2,1,0:T(8,128)(2,1)} %bitcast.25, bf16[2,32,4096]{2,1,0:T(8,128)(2,1)} %bitcast.27, ...), custom_call_target="tpu_custom_call" | custom-call | tf_op jit(solution)/shard_map/values1/pallas_call | solution.py:159
  91.6 10.0 %all-to-all-done.4 = f32[256,1,128]{2,1,0:T(1,128)S(1)} async-done(((f32[256,1,128]{2,1,0:T(1,128)}), f32[256,1,128]{2,1,0:T(1,128)S(1)}, u32[]{:S(2)}, u32[]{:S(2)}) %all-to-all-start.4) | async-done | bytes 131104 | tf_op jit(solution)/shard_map/all_to_all | solution.py:262
  101.6 0.0 copy-start
  101.6 0.7 copy-done
  102.3 5.1 %mix1.1 = (f32[2,32,32,128]{3,2,1,0:T(8,128)}, bf16[32,40,128]{2,1,0:T(8,128)(2,1)}) custom-call(f32[2,128,128]{2,1,0:T(8,128)} %bitcast.28, f32[4,32,32]{2,1,0:T(8,128)} %get-tuple-element.30.packed, f32[2,32,32,128]{3,2,1,0:T(8,128)} %state.3, f32[2,32]{1,0:T(2,128)} %gain.7, bf16[2,32,4096]{2,1,0:T(8,128)(2,1)} %w_out.3, ...), custom_call_target="tpu_custom_call", output_to_operand_aliasing={{0}: (5, {})} | custom-call | tf_op jit(solution)/shard_map/mix1/pallas_call | solution.py:205
  107.3 14.1 %all_to_all.51.got = bf16[32,40,128]{2,1,0:T(8,128)(2,1)} all-to-all(bf16[32,40,128]{2,1,0:T(8,128)(2,1)} %get-tuple-element.32), channel_id=1, replica_groups=mesh['z'=8,'y'=4,'x'=4,'c'=2] {'y','x','c'}, dimensions={0} | all-to-all | bytes 655360 | tf_op jit(solution)/shard_map/all_to_all | solution.py:262
  121.5 1.7 %scale.3 = bf16[8,32,128]{2,1,0:T(8,128)(2,1)} custom-call(bf16[32,40,128]{2,1,0:T(8,128)(2,1)} %all_to_all.51.got), custom_call_target="tpu_custom_call" | custom-call | tf_op jit(solution)/shard_map/scale/pallas_call | solution.py:228
  123.2 11.1 %all_to_all.52.got = bf16[8,32,128]{2,1,0:T(8,128)(2,1)} all-to-all(bf16[8,32,128]{2,1,0:T(8,128)(2,1)} %scale.3), channel_id=1, replica_groups=mesh['z'=8,'y'=4,'x'=4,'c'=2] {'z'}, dimensions={0} | all-to-all | bytes 131072 | tf_op jit(solution)/shard_map/all_to_all | solution.py:262
  134.3 1.7 %add1.1 = bf16[32,32,128]{2,1,0:T(8,128)(2,1)} custom-call(s32[3]{0:T(128)} %pad_add_fusion.spot, bf16[8,32,128]{2,1,0:T(8,128)(2,1)} %all_to_all.52.got, bf16[32,32,128]{2,1,0:T(8,128)(2,1)} %all_to_all.50.hid), custom_call_target="tpu_custom_call" | custom-call | tf_op jit(solution)/shard_map/add1/pallas_call | solution.py:252
  136.0 14.0 %all_to_all.53 = bf16[32,32,128]{2,1,0:T(8,128)(2,1)S(1)} all-to-all(bf16[32,32,128]{2,1,0:T(8,128)(2,1)} %add1.1), channel_id=1, replica_groups=mesh['z'=8,'y'=4,'x'=4,'c'=2] {'y','x','c'}, dimensions={0} | all-to-all | bytes 524288 | tf_op jit(solution)/shard_map/all_to_all | solution.py:262
  150.0 0.7 copy_bitcast_fusion
Async XLA Ops:
  3.3 28.7 %all-to-all-start = ((f32[256,1,128]{2,1,0:T(1,128)}), f32[256,1,128]{2,1,0:T(1,128)S(1)}, u32[]{:S(2)}, u32[]{:S(2)}) async-start(f32[256,1,128]{2,1,0:T(1,128)} %bitcast.35), calls=%async_computation | async-start | bytes 262144 | tf_op jit(solution)/shard_map/all_to_all | solution.py:262
  32.0 0.7 copy-start.1
  83.2 18.4 %all-to-all-start.4 = ((f32[256,1,128]{2,1,0:T(1,128)}), f32[256,1,128]{2,1,0:T(1,128)S(1)}, u32[]{:S(2)}, u32[]{:S(2)}) async-start(f32[256,1,128]{2,1,0:T(1,128)} %bitcast.34), calls=%async_computation.4 | async-start | bytes 262144 | tf_op jit(solution)/shard_map/all_to_all | solution.py:262
  101.6 0.7 copy-start

commit v2 on v1

v2 whole, which is shorter than its diff:
```python
import functools

import jax
import jax.numpy as jnp
from jax import lax
from jax.experimental import pallas as pl
from jax.experimental.pallas import tpu as pltpu
from jax.sharding import Mesh
from jax.sharding import PartitionSpec as P

D = 4096
B = 32
CH = 32
N = 128
GW = 1024
EPS = 1e-06
TP = ("z", "y", "x", "c")
PLANE = ("y", "x", "c")
F32 = jnp.float32
BF16 = jnp.bfloat16


LIMIT = pltpu.CompilerParams(vmem_limit_bytes=8 * 1024 * 1024)
LINES = (2, 8, 16, 128)


def vmem():
    return pl.BlockSpec(memory_space=pltpu.VMEM)


def anywhere():
    return pl.BlockSpec(memory_space=pl.ANY)


def shaped(shape, dtype):
    return jax.ShapeDtypeStruct(shape, dtype)


def start_all(pairs, sems):
    copies = [pltpu.make_async_copy(src, dst, sems.at[at]) for at, (src, dst) in enumerate(pairs)]
    for copy in copies:
        copy.start()
    return copies


def call(body, name, near, far, outs, scratch=(), aliases=None):
    near = [pltpu.with_memory_space_constraint(v, pltpu.VMEM) for v in near]
    far = [pltpu.with_memory_space_constraint(v, pltpu.HBM) for v in far]
    far_out = (pltpu.HBM((1,), F32).memory_space,)
    specs = [anywhere() if getattr(o, "memory_space", None) in far_out else vmem() for o in outs]
    return pl.pallas_call(
        body,
        in_specs=[vmem()] * len(near) + [anywhere()] * len(far),
        out_specs=specs,
        out_shape=list(outs),
        scratch_shapes=list(scratch),
        input_output_aliases=aliases or {},
        compiler_params=LIMIT,
        name=name,
    )(*near, *far)


def silu(v):
    return v / (1.0 + jnp.exp(-v))


def as_col(row):
    n = row.shape[1]
    at = lax.broadcasted_iota(jnp.int32, (n, n), 0)
    of = lax.broadcasted_iota(jnp.int32, (n, n), 1)
    return jnp.sum(jnp.where(at == of, row, 0.0), axis=1, keepdims=True)


def as_row(col):
    n = col.shape[0]
    at = lax.broadcasted_iota(jnp.int32, (n, n), 0)
    of = lax.broadcasted_iota(jnp.int32, (n, n), 1)
    return jnp.sum(jnp.where(at == of, col, 0.0), axis=0, keepdims=True)


def dot_nt(a, b):
    return lax.dot_general(a, b, (((1,), (1,)), ((), ())), preferred_element_type=F32)


def write_keys(part_of, near, msg, conv_out, scaled, inv_out):
    gain, w_write, w_read, conv, taps = near
    squares = jnp.zeros((B, 128), F32)
    for j in range(D // 128):
        cols = slice(128 * j, 128 * j + 128)
        part = part_of(j).astype(F32)
        squares += part * part
        scaled[:, cols] = (part * gain[:, cols]).astype(BF16)
    inv = lax.rsqrt(jnp.sum(squares, axis=1, keepdims=True) / D + EPS)
    inv_out[...] = jnp.broadcast_to(inv, (B, 128))
    inv_row = as_row(inv)
    mixed = []
    for kind, weight in ((0, w_write), (1, w_read)):
        fresh = dot_nt(weight[...], scaled[...]) * inv_row
        old, newer = conv[0, kind], conv[1, kind]
        tap = [as_col(taps[k, kind : kind + 1, :]) for k in range(3)]
        mixed.append(silu(old * tap[0] + newer * tap[1] + fresh * tap[2]))
        conv_out[0, kind] = newer
        conv_out[1, kind] = fresh
    lines = jnp.concatenate([mixed[0], mixed[1], jnp.zeros((4, 128 - 2 * B), F32)], axis=1)
    core = lax.axis_index("c")
    for plane in range(8):
        line = lines[plane % 4 : plane % 4 + 1]
        line = jnp.where(core == plane // 4, line, 0.0)
        block = jnp.broadcast_to(line, (16, 128))
        msg[0, plane] = block
        msg[1, plane] = block


KEY_PARAMS = (((1, D), F32), ((4, D), BF16), ((4, D), BF16), ((2, 2, 4, B), F32), ((3, 2, 4), F32))


def key_pairs(layer, far, near):
    gain, w_write, w_read, conv, taps = far
    source = (gain.at[layer : layer + 1], w_write.at[layer], w_read.at[layer], conv.at[layer], taps.at[layer])
    return list(zip(source, near))


def first_keys_kernel(tokens, *refs):
    far, (msg, conv_out, scaled, inv_out, hid), near, sems = refs[:5], refs[5:10], refs[10:15], refs[15]
    for copy in start_all([(tokens, hid)] + key_pairs(0, far, near), sems):
        copy.wait()
    write_keys(lambda j: hid[:, 128 * j : 128 * j + 128], near, msg, conv_out, scaled, inv_out)


def first_keys(tokens, params):
    return call(
        first_keys_kernel,
        "keys0",
        [],
        [tokens, *params],
        [
            shaped(LINES, F32),
            pltpu.VMEM((2, 2, 4, B), F32),
            pltpu.VMEM((B, D), BF16),
            pltpu.VMEM((B, 128), F32),
            pltpu.VMEM((B, D), BF16),
        ],
        [pltpu.VMEM(*p) for p in KEY_PARAMS] + [pltpu.SemaphoreType.DMA((6,))],
    )


def next_keys_kernel(hid, *refs):
    near, before, (msg, conv_out, scaled, inv_out) = refs[:5], refs[5], refs[6:]
    conv_out[0] = before[...]
    write_keys(lambda j: hid[j], near, msg, conv_out.at[1], scaled, inv_out)


def next_keys(hid, near, before):
    return call(
        next_keys_kernel,
        "keys1",
        [hid, *near, before],
        [],
        [
            shaped(LINES, F32),
            shaped((2, 2, 2, 4, B), F32),
            pltpu.VMEM((B, D), BF16),
            pltpu.VMEM((B, 128), F32),
        ],
    )


VALUE_PARAMS = (
    ((CH, D), BF16),
    ((CH, D), BF16),
    ((D, 128), BF16),
    ((2, 128), F32),
    ((2, 128), F32),
    ((2, 128), F32),
    ((B, 2, CH), F32),
    ((3, 2, CH), F32),
)
MIX_PARAMS = (((B, CH, N), F32), ((CH, D), BF16), ((2, CH), F32))


def values_kernel(layer, scaled, inv, *refs):
    refs = list(refs)

    def take(n):
        got = refs[:n]
        del refs[:n]
        return got

    before = take(layer)
    far, mix_far, key_far = take(8), take(3), take(0 if layer else 5)
    (packed, conv_out), mix_near, key_near = take(2), take(3), take(0 if layer else 5)
    near, (sems, late_sems) = take(8), take(2)
    gate_far, value_far, step_far, bias, rate, skip, conv_far, taps_far = far
    state, w_out, gain = mix_far
    source = (gate_far.at[layer], value_far.at[layer], step_far.at[layer], bias, rate, skip, conv_far.at[layer], taps_far)
    copies = start_all(list(zip(source, near)), sems)
    late = list(zip((state.at[layer], w_out.at[layer], gain), mix_near))
    if not layer:
        late += key_pairs(1, key_far, key_near)
    late = start_all(late, late_sems)
    for copy in copies:
        copy.wait()
    w_gate, w_value, w_step, bias, rate, skip, conv, taps = near
    hidden = scaled[...]
    inv_col = inv[:, :CH]
    gate = dot_nt(hidden, w_gate[...]) * inv_col
    fresh = dot_nt(hidden, w_value[...]) * inv_col
    step = jnp.dot(hidden, w_step[...], preferred_element_type=F32) * inv[...]
    old, newer = conv[:, 0, :], conv[:, 1, :]
    tap = [taps[k, layer : layer + 1, :] for k in range(3)]
    values = silu(old * tap[0] + newer * tap[1] + fresh * tap[2])
    if layer:
        conv_out[0] = before[0][...]
        conv_out[1, :, 0, :] = newer
        conv_out[1, :, 1, :] = fresh
    else:
        conv_out[:, 0, :] = newer
        conv_out[:, 1, :] = fresh
    head = lax.axis_index(("z", "y", "x"))
    mine = lax.broadcasted_iota(jnp.int32, (1, 128), 1) == head

    def of_head(table):
        return jnp.sum(jnp.where(mine, table, 0.0), axis=1, keepdims=True)

    raw = of_head(step + bias[layer : layer + 1, :])
    delta = jnp.maximum(raw, 0.0) + jnp.log1p(jnp.exp(-jnp.abs(raw)))
    decay = jnp.exp(-delta * of_head(rate[layer : layer + 1, :]))
    packed[0] = (delta * values).T
    packed[1] = of_head(skip[layer : layer + 1, :]) * values
    packed[2] = silu(gate)
    packed[3] = jnp.broadcast_to(decay, (B, CH))
    for copy in late:
        copy.wait()


def make_values(layer, scaled, inv, value_far, mix_far, key_far, before):
    near = [scaled, inv] + ([before] if layer else [])
    outs = [
        pltpu.VMEM((4, B, CH), F32),
        shaped((2, B, 2, CH), F32) if layer else pltpu.VMEM((B, 2, CH), F32),
    ]
    outs += [pltpu.VMEM(*p) for p in MIX_PARAMS]
    if not layer:
        outs += [pltpu.VMEM(*p) for p in KEY_PARAMS]
    else:
        key_far = []
    sems = [pltpu.SemaphoreType.DMA((8,)), pltpu.SemaphoreType.DMA((8,))]
    return call(
        functools.partial(values_kernel, layer),
        f"values{layer}",
        near,
        [*value_far, *mix_far, *key_far],
        outs,
        [pltpu.VMEM(*p) for p in VALUE_PARAMS] + sems,
    )


def mix_kernel(layer, keys, packed, state, w_out, gain, fresh, sent):
    both = (keys[0] + keys[1]).T
    writes, reads = both[:B], both[B : 2 * B]
    push = packed[0]
    decay = packed[3]
    lane = lax.broadcasted_iota(jnp.int32, (CH, B), 1)
    found = jnp.zeros((CH, B), F32)
    for b in range(B):
        new = decay[b : b + 1, :1] * state[b] + push[:, b : b + 1] * writes[b : b + 1]
        fresh[b] = new
        total = jnp.sum(new * reads[b : b + 1], axis=1, keepdims=True)
        found = jnp.where(lane == b, total, found)
    gated = (found.T + packed[1]) * packed[2]
    total = as_row(jnp.sum(gated * gated, axis=1, keepdims=True))
    high = total.astype(BF16).astype(F32)
    low = total - high
    row = lax.broadcasted_iota(jnp.int32, (8, B), 0)
    tail = jnp.where(row == 0, high, jnp.where(row == 1, low, 0.0))
    tail = jnp.concatenate([tail, jnp.zeros((8, 128 - B), F32)], axis=1).astype(BF16)
    out = jnp.dot((gated * gain[layer : layer + 1, :]).astype(BF16), w_out[...], preferred_element_type=F32)
    for j in range(D // 128):
        sent[j, :B] = out[:, 128 * j : 128 * j + 128].astype(BF16)
        sent[j, B:] = tail


def make_mix(layer, keys, packed, mix_near):
    return call(
        functools.partial(mix_kernel, layer),
        f"mix{layer}",
        [keys, packed, *mix_near],
        [],
        [pltpu.VMEM((B, CH, N), F32), pltpu.VMEM((32, 40, 128), BF16)],
    )


def scale_kernel(layer, got, fresh, *refs):
    sent, states, sem = refs[-3:]
    write_back = pltpu.make_async_copy(fresh, states.at[layer], sem)
    write_back.start()
    total = got[0].astype(F32)
    for j in range(1, 32):
        total += got[j].astype(F32)
    squares = total[B : B + 1, :B] + total[B + 1 : B + 2, :B]
    factor = as_col(lax.rsqrt(squares / GW + EPS))
    chunk = (total[:B] * factor).astype(BF16)
    for plane in range(8):
        sent[plane] = chunk
    write_back.wait()


def make_scale(layer, got, fresh, states):
    return call(
        functools.partial(scale_kernel, layer),
        f"scale{layer}",
        [got, fresh],
        [states] if layer else [],
        [pltpu.VMEM((8, B, 128), BF16), pltpu.HBM((2, B, CH, N), F32)],
        [pltpu.SemaphoreType.DMA],
        {2: 1} if layer else {},
    )


def add_kernel(layer, got, hid, sent):
    total = got[0].astype(F32)
    for plane in range(1, 8):
        total += got[plane].astype(F32)
    at = lax.axis_index(PLANE)
    if layer:
        own = hid[at]
    else:
        own = hid[:, pl.ds(pl.multiple_of(128 * at, 128), 128)]
    chunk = (own.astype(F32) + total).astype(BF16)
    for j in range(32):
        sent[j] = chunk


def make_add(layer, got, hid):
    return call(
        functools.partial(add_kernel, layer), f"add{layer}", [got, hid], [], [pltpu.VMEM((32, B, 128), BF16)]
    )[0]


def exchange(value, axes):
    return lax.all_to_all(value, axes, split_axis=0, concat_axis=0, tiled=True)


def per_device(
    tokens,
    norm_gain,
    w_gate,
    w_value,
    w_write,
    w_read,
    w_step,
    step_bias,
    decay_rate,
    skip_gain,
    conv_value_weight,
    conv_key_weight,
    group_gain,
    w_out,
    ssm_state,
    conv_value,
    conv_key,
):
    w_gate, w_value, w_write, w_read = (jnp.swapaxes(w, 1, 2) for w in (w_gate, w_value, w_write, w_read))
    conv_key = jnp.transpose(conv_key, (0, 2, 3, 4, 1))
    value_taps = jnp.swapaxes(conv_value_weight, 0, 1)
    key_far = [norm_gain, w_write, w_read, conv_key, conv_key_weight]
    value_far = [w_gate, w_value, w_step, step_bias, decay_rate, skip_gain, conv_value, value_taps]
    mix_far = [ssm_state, w_out, group_gain]
    states = value_out = None
    msg, key_out, scaled, inv, hid = first_keys(tokens, key_far)
    for layer in range(2):
        if layer:
            msg, key_out, scaled, inv = next_keys(hid, key_near, key_out)
        keys = exchange(msg.reshape(256, 128), ("c", "z", "y", "x")).reshape(2, 128, 128)
        packed, value_out, *near = make_values(layer, scaled, inv, value_far, mix_far, key_far, value_out)
        mix_near, key_near = near[:3], near[3:]
        fresh, sent = make_mix(layer, keys, packed, mix_near)
        sent, states = make_scale(layer, exchange(sent, PLANE), fresh, states)
        hid = exchange(make_add(layer, exchange(sent, ("z",)), hid), PLANE)
    tokens_out = jnp.transpose(hid, (1, 0, 2)).reshape(B, D)
    return (tokens_out, states, value_out, jnp.transpose(key_out, (0, 4, 1, 2, 3)))


def solution(mesh):
    torus = Mesh(mesh.devices.reshape(8, 4, 4, 2), TP)
    in_specs = (
        P(),
        P(),
        P(None, None, TP),
        P(None, None, TP),
        P(None, None, TP),
        P(None, None, TP),
        P(),
        P(),
        P(),
        P(),
        P(None, None, TP),
        P(None, None, None, TP),
        P(None, TP),
        P(None, TP, None),
        P(None, None, TP, None),
        P(None, None, None, TP),
        P(None, None, None, None, TP),
    )
    out_specs = (
        P(),
        P(None, None, TP, None),
        P(None, None, None, TP),
        P(None, None, None, None, TP),
    )
    return jax.shard_map(
        per_device, mesh=torus, in_specs=in_specs, out_specs=out_specs, check_vma=False
    )
```

time: 152 us -> 131 us (0.86)
  Pallas kernels: 27.7 us -> 14.8 us
  blocking collectives: 79.2 us -> 72.7 us
    pallas_call x10, Pallas kernels: 27.7 us -> 14.8 us  [call(): pl.pallas_call(body, in_specs=[vmem()] * len(near) + [anywhere()] * len(f...]
    all_to_all x6, blocking collectives: 79.2 us -> 72.7 us  [exchange(): return lax.all_to_all(value, axes, split_axis=0, concat_axis=0, tiled=True)]
where the time goes in v2:
time: 131 us
  blocking collectives  72.7 us (55%)
  waiting for transfers between devices  21 us (16%)
  starting transfers between devices  20.8 us (16%)
  Pallas kernels  14.8 us (11%)
    all_to_all x6, blocking collectives, exchange(): return lax.all_to_all(value, axes, split_axis=0, concat_axis=0, tiled=True)  72.7 us
    all_to_all x2, waiting for transfers between devices, exchange(): return lax.all_to_all(value, axes, split_axis=0, concat_axis=0, tiled=True)  21 us
    all_to_all x2, starting transfers between devices, exchange(): return lax.all_to_all(value, axes, split_axis=0, concat_axis=0, tiled=True)  20.8 us
    pallas_call x10, Pallas kernels, call(): pl.pallas_call(body, in_specs=[vmem()] * len(near) + [anywhere()] * len(f...  14.8 us
  transfers between devices with their start and end apart: 2, of which 2 were waited for; matrix products, arithmetic and copies ran while one was open for 0% of the time, Pallas kernels for 4%

profile of v2, /device:TPU:1, one launch (start us, length us, event | category | flops | bytes accessed | tf_op | source)
XLA Modules:
  0.0 130.8 jit_solution(12814707135329974559)
XLA Ops:
  0.6 2.0 %keys0.1 = (f32[2,8,16,128]{3,2,1,0:T(8,128)}, f32[2,2,4,32]{3,2,1,0:T(4,128)S(1)}, bf16[32,4096]{1,0:T(8,128)(2,1)S(1)}, f32[32,128]{1,0:T(8,128)S(1)}, bf16[32,4096]{1,0:T(8,128)(2,1)S(1)}) custom-call(bf16[32,4096]{1,0:T(8,128)(2,1)} %tokens.1, f32[2,4096]{1,0:T(2,128)} %refs_11_.2, bf16[2,4,4096]{2,1,0:T(4,128)(2,1)} %bitcast.27, ...), custom_call_target="tpu_custom_call" | custom-call | tf_op jit(solution)/shard_map/keys0/pallas_call | solution.py:51
  2.7 15.7 %all-to-all-start = ((f32[256,1,128]{2,1,0:T(1,128)}), f32[256,1,128]{2,1,0:T(1,128)S(1)}, u32[]{:S(2)}, u32[]{:S(2)}) async-start(f32[256,1,128]{2,1,0:T(1,128)} %bitcast.4), calls=%async_computation | async-start | bytes 262144 | tf_op jit(solution)/shard_map/all_to_all | solution.py:341
  18.3 2.4 %values0.1 = (f32[4,32,32]{2,1,0:T(8,128)S(1)}, f32[32,2,32]{2,1,0:T(2,128)S(1)}, f32[32,32,128]{2,1,0:T(8,128)S(1)}, bf16[32,4096]{1,0:T(8,128)(2,1)S(1)}, f32[...) custom-call(bf16[32,4096]{1,0:T(8,128)(2,1)S(1)} %get-tuple-element., ...), custom_call_target="tpu_custom_call" | custom-call | tf_op jit(solution)/shard_map/values0/pallas_call | solution.py:51
  20.8 10.6 %all-to-all-done = f32[256,1,128]{2,1,0:T(1,128)S(1)} async-done(((f32[256,1,128]{2,1,0:T(1,128)}), f32[256,1,128]{2,1,0:T(1,128)S(1)}, u32[]{:S(2)}, u32[]{:S(2)}) %all-to-all-start) | async-done | bytes 131104 | tf_op jit(solution)/shard_map/all_to_all | solution.py:341
  31.4 2.4 %mix0.1 = (f32[32,32,128]{2,1,0:T(8,128)S(1)}, bf16[32,40,128]{2,1,0:T(8,128)(2,1)S(1)}) custom-call(f32[2,128,128]{2,1,0:T(8,128)S(1)} %bitcast.21, f32[4,32,32]{2,1,0:T(8,128)S(1)} %get-tuple-element.39.packed, f32[32,32,128]{2,1,0:T(8,128)S(1)} %get-tuple-element.40.state, bf16[32,4096]{1,0:T(8,128)(2,1)S(1)} %get-tuple-element.41.w_out, ...), custom_call_target="tpu_custom_call" | custom-call | tf_op jit(solution)/shard_map/mix0/pallas_call | solution.py:51
  33.8 13.2 %all_to_all.48.got = bf16[32,40,128]{2,1,0:T(8,128)(2,1)S(1)} all-to-all(bf16[32,40,128]{2,1,0:T(8,128)(2,1)S(1)} %get-tuple-element.43), channel_id=1, replica_groups=mesh['z'=8,'y'=4,'x'=4,'c'=2] {'y','x','c'}, dimensions={0} | all-to-all | bytes 655360 | tf_op jit(solution)/shard_map/all_to_all | solution.py:341
  47.0 0.8 scale0.1
  47.8 9.5 %all_to_all.49.got = bf16[8,32,128]{2,1,0:T(8,128)(2,1)S(1)} all-to-all(bf16[8,32,128]{2,1,0:T(8,128)(2,1)S(1)} %get-tuple-element.45), channel_id=1, replica_groups=mesh['z'=8,'y'=4,'x'=4,'c'=2] {'z'}, dimensions={0} | all-to-all | bytes 131072 | tf_op jit(solution)/shard_map/all_to_all | solution.py:341
  57.4 13.7 %all_to_all.50.hid = bf16[32,32,128]{2,1,0:T(8,128)(2,1)S(1)} all-to-all(bf16[32,32,128]{2,1,0:T(8,128)(2,1)S(1)} %add0.1), channel_id=1, replica_groups=mesh['z'=8,'y'=4,'x'=4,'c'=2] {'y','x','c'}, dimensions={0} | all-to-all | bytes 524288 | tf_op jit(solution)/shard_map/all_to_all | solution.py:341
  71.0 1.0 keys1.1
  72.1 5.2 %all-to-all-start.4 = ((f32[256,1,128]{2,1,0:T(1,128)}), f32[256,1,128]{2,1,0:T(1,128)S(1)}, u32[]{:S(2)}, u32[]{:S(2)}) async-start(f32[256,1,128]{2,1,0:T(1,128)} %bitcast.10), calls=%async_computation.4 | async-start | bytes 262144 | tf_op jit(solution)/shard_map/all_to_all | solution.py:341
  77.2 2.8 %values1.1 = (f32[4,32,32]{2,1,0:T(8,128)S(1)}, f32[2,32,2,32]{3,2,1,0:T(2,128)}, f32[32,32,128]{2,1,0:T(8,128)S(1)}, bf16[32,4096]{1,0:T(8,128)(2,1)S(1)}, f32[2,32]{1,0:T(2,128)S(1)}) custom-call(bf16[32,4096]{1,0:T(8,128)(2,1)S(1)} %get-tuple-element.54.scaled, f32[32,128]{1,0:T(8,128)S(1)} %get-tuple-element.55.inv, ...), custom_call_target="tpu_custom_call" | custom-call | tf_op jit(solution)/shard_map/values1/pallas_call | solution.py:51
  80.1 10.3 %all-to-all-done.4 = f32[256,1,128]{2,1,0:T(1,128)S(1)} async-done(((f32[256,1,128]{2,1,0:T(1,128)}), f32[256,1,128]{2,1,0:T(1,128)S(1)}, u32[]{:S(2)}, u32[]{:S(2)}) %all-to-all-start.4) | async-done | bytes 131104 | tf_op jit(solution)/shard_map/all_to_all | solution.py:341
  90.4 2.4 %mix1.1 = (f32[32,32,128]{2,1,0:T(8,128)S(1)}, bf16[32,40,128]{2,1,0:T(8,128)(2,1)S(1)}) custom-call(f32[2,128,128]{2,1,0:T(8,128)S(1)} %bitcast.22, f32[4,32,32]{2,1,0:T(8,128)S(1)} %get-tuple-element.57.packed, f32[32,32,128]{2,1,0:T(8,128)S(1)} %get-tuple-element.58.state, bf16[32,4096]{1,0:T(8,128)(2,1)S(1)} %get-tuple-element.59.w_out, ...), custom_call_target="tpu_custom_call" | custom-call | tf_op jit(solution)/shard_map/mix1/pallas_call | solution.py:51
  92.8 13.2 %all_to_all.51.got = bf16[32,40,128]{2,1,0:T(8,128)(2,1)S(1)} all-to-all(bf16[32,40,128]{2,1,0:T(8,128)(2,1)S(1)} %get-tuple-element.61), channel_id=1, replica_groups=mesh['z'=8,'y'=4,'x'=4,'c'=2] {'y','x','c'}, dimensions={0} | all-to-all | bytes 655360 | tf_op jit(solution)/shard_map/all_to_all | solution.py:341
  106.0 0.8 scale1.1
  106.9 9.5 %all_to_all.52.got = bf16[8,32,128]{2,1,0:T(8,128)(2,1)S(1)} all-to-all(bf16[8,32,128]{2,1,0:T(8,128)(2,1)S(1)} %get-tuple-element.64), channel_id=1, replica_groups=mesh['z'=8,'y'=4,'x'=4,'c'=2] {'z'}, dimensions={0} | all-to-all | bytes 131072 | tf_op jit(solution)/shard_map/all_to_all | solution.py:341
  116.4 13.7 %all_to_all.53 = bf16[32,32,128]{2,1,0:T(8,128)(2,1)S(1)} all-to-all(bf16[32,32,128]{2,1,0:T(8,128)(2,1)S(1)} %add1.1), channel_id=1, replica_groups=mesh['z'=8,'y'=4,'x'=4,'c'=2] {'y','x','c'}, dimensions={0} | all-to-all | bytes 524288 | tf_op jit(solution)/shard_map/all_to_all | solution.py:341
  130.1 0.7 copy_bitcast_fusion
  (2 shorter events, 0.1 us)
Async XLA Ops:
  2.7 28.7 %all-to-all-start = ((f32[256,1,128]{2,1,0:T(1,128)}), f32[256,1,128]{2,1,0:T(1,128)S(1)}, u32[]{:S(2)}, u32[]{:S(2)}) async-start(f32[256,1,128]{2,1,0:T(1,128)} %bitcast.4), calls=%async_computation | async-start | bytes 262144 | tf_op jit(solution)/shard_map/all_to_all | solution.py:341
  72.1 18.3 %all-to-all-start.4 = ((f32[256,1,128]{2,1,0:T(1,128)}), f32[256,1,128]{2,1,0:T(1,128)S(1)}, u32[]{:S(2)}, u32[]{:S(2)}) async-start(f32[256,1,128]{2,1,0:T(1,128)} %bitcast.10), calls=%async_computation.4 | async-start | bytes 262144 | tf_op jit(solution)/shard_map/all_to_all | solution.py:341

commit v3 on v2

v3 whole, which is shorter than its diff:
```python
import functools

import jax
import jax.numpy as jnp
from jax import lax
from jax.experimental import pallas as pl
from jax.experimental.pallas import tpu as pltpu
from jax.sharding import Mesh
from jax.sharding import PartitionSpec as P

D = 4096
B = 32
CH = 32
N = 128
GW = 1024
EPS = 1e-06
TP = ("z", "y", "x", "c")
PLANE = ("y", "x", "c")
F32 = jnp.float32
BF16 = jnp.bfloat16


LIMIT = pltpu.CompilerParams(vmem_limit_bytes=8 * 1024 * 1024)


def vmem():
    return pl.BlockSpec(memory_space=pltpu.VMEM)


def anywhere():
    return pl.BlockSpec(memory_space=pl.ANY)


def shaped(shape, dtype):
    return jax.ShapeDtypeStruct(shape, dtype)


def start_all(pairs, sems):
    copies = [pltpu.make_async_copy(src, dst, sems.at[at]) for at, (src, dst) in enumerate(pairs)]
    for copy in copies:
        copy.start()
    return copies


def call(body, name, near, far, outs, scratch=(), aliases=None):
    near = [pltpu.with_memory_space_constraint(v, pltpu.VMEM) for v in near]
    far = [pltpu.with_memory_space_constraint(v, pltpu.HBM) for v in far]
    far_out = (pltpu.HBM((1,), F32).memory_space,)
    specs = [anywhere() if getattr(o, "memory_space", None) in far_out else vmem() for o in outs]
    return pl.pallas_call(
        body,
        in_specs=[vmem()] * len(near) + [anywhere()] * len(far),
        out_specs=specs,
        out_shape=list(outs),
        scratch_shapes=list(scratch),
        input_output_aliases=aliases or {},
        compiler_params=LIMIT,
        name=name,
    )(*near, *far)


def silu(v):
    return v / (1.0 + jnp.exp(-v))


def as_col(row):
    n = row.shape[1]
    at = lax.broadcasted_iota(jnp.int32, (n, n), 0)
    of = lax.broadcasted_iota(jnp.int32, (n, n), 1)
    return jnp.sum(jnp.where(at == of, row, 0.0), axis=1, keepdims=True)


def as_row(col):
    n = col.shape[0]
    at = lax.broadcasted_iota(jnp.int32, (n, n), 0)
    of = lax.broadcasted_iota(jnp.int32, (n, n), 1)
    return jnp.sum(jnp.where(at == of, col, 0.0), axis=0, keepdims=True)


def dot_nt(a, b):
    return lax.dot_general(a, b, (((1,), (1,)), ((), ())), preferred_element_type=F32)


def hi_lo(value):
    high = value.astype(BF16).astype(F32)
    return high, value - high


def scale_tokens(part_of, gain, scaled):
    squares = jnp.zeros((B, 128), F32)
    for j in range(D // 128):
        cols = slice(128 * j, 128 * j + 128)
        part = part_of(j).astype(F32)
        squares += part * part
        scaled[:, cols] = (part * gain[:, cols]).astype(BF16)
    return lax.rsqrt(jnp.sum(squares, axis=1, keepdims=True) / D + EPS)


KEY_WEIGHTS = ((4, D), BF16)


def keys_kernel(tokens, gain_far, write_far, read_far, conv_far, taps_far, msg, conv_out, scaled, inv_out, hid, *rest):
    gain, w_write, w_read, next_write, next_read, conv, taps, sems = rest
    pairs = [
        (tokens, hid),
        (gain_far, gain),
        (write_far.at[0], w_write),
        (read_far.at[0], w_read),
        (write_far.at[1], next_write),
        (read_far.at[1], next_read),
        (conv_far, conv),
        (taps_far, taps),
    ]
    for copy in start_all(pairs, sems):
        copy.wait()
    inv = scale_tokens(lambda j: hid[:, 128 * j : 128 * j + 128], gain.at[:1], scaled)
    inv_out[...] = jnp.broadcast_to(inv, (B, 128))
    inv_row = as_row(inv)
    mixed, later, last_taps = [], [], []
    for kind, weight in ((0, w_write), (1, w_read)):
        fresh = dot_nt(weight[...], scaled[...]) * inv_row
        old, newer = conv[0, 0, kind], conv[0, 1, kind]
        tap = [[as_col(taps[layer, k, kind : kind + 1, :]) for k in range(3)] for layer in range(2)]
        mixed.append(silu(old * tap[0][0] + newer * tap[0][1] + fresh * tap[0][2]))
        later.append(conv[1, 0, kind] * tap[1][0] + conv[1, 1, kind] * tap[1][1])
        last_taps.append(tap[1][2])
        conv_out[0, kind] = newer
        conv_out[1, kind] = fresh
    mixed_hi, mixed_lo = zip(*(hi_lo(v) for v in mixed))
    taps_hi, taps_lo = zip(*(hi_lo(v) for v in last_taps))
    first = jnp.concatenate([*mixed_hi, *later], axis=1)
    lane = lax.broadcasted_iota(jnp.int32, (4, B), 1)
    tail = jnp.zeros((4, B), F32)
    for at, col in enumerate((taps_hi[0], taps_lo[0], taps_hi[1], taps_lo[1])):
        tail = jnp.where(lane == at, col, tail)
    second = jnp.concatenate([*mixed_lo, tail, jnp.zeros((4, B), F32)], axis=1)
    row = lax.broadcasted_iota(jnp.int32, (4, 128), 0)
    for col in range(4):
        one = slice(col, col + 1)
        base = jnp.where(row == 2, first[one], second[one])
        for place in range(32):
            cols = slice(128 * place, 128 * place + 128)
            write = next_write[:, cols].astype(F32)[one]
            read = next_read[:, cols].astype(F32)[one]
            tile = jnp.where(row == 0, write, jnp.where(row == 1, read, base)).astype(BF16)
            at = 128 * (place % 2) + 16 * col + place // 2
            msg[at] = tile
            msg[at + 64] = tile


def make_keys(tokens, far):
    scratch = [((2, D), F32)] + [KEY_WEIGHTS] * 4 + [((2, 2, 2, 4, B), F32), ((2, 3, 2, 4), F32)]
    return call(
        keys_kernel,
        "keys",
        [],
        [tokens, *far],
        [
            shaped((256, 4, 128), BF16),
            pltpu.VMEM((2, 2, 4, B), F32),
            pltpu.VMEM((B, D), BF16),
            pltpu.VMEM((B, 128), F32),
            pltpu.VMEM((B, D), BF16),
        ],
        [pltpu.VMEM(*p) for p in scratch] + [pltpu.SemaphoreType.DMA((8,))],
    )


def of_head(table):
    head = lax.axis_index(("z", "y", "x"))
    mine = lax.broadcasted_iota(jnp.int32, (1, 128), 1) == head
    return jnp.sum(jnp.where(mine, table, 0.0), axis=1, keepdims=True)


def gated_values(layer, gate, fresh, raw, tables, conv, taps):
    bias, rate, skip = (t[layer : layer + 1, :] for t in tables)
    old, newer = conv[:, 0, :], conv[:, 1, :]
    tap = [taps[k, layer : layer + 1, :] for k in range(3)]
    values = silu(old * tap[0] + newer * tap[1] + fresh * tap[2])
    raw = raw + of_head(bias)
    delta = jnp.maximum(raw, 0.0) + jnp.log1p(jnp.exp(-jnp.abs(raw)))
    decay = jnp.exp(-delta * of_head(rate))
    return (delta * values).T, of_head(skip) * values, silu(gate), decay


STATE = ((B, CH, N), F32)
OUT = ((CH, D), BF16)
ROWS = 80
NOW_FAR = (((CH, D), BF16), ((CH, D), BF16), ((D, 128), BF16))
NEXT_FAR = (((D, 128), BF16), KEY_WEIGHTS, KEY_WEIGHTS)
KEPT = (
    STATE,
    OUT,
    ((2, CH), F32),
    STATE,
    OUT,
    ((2, D), F32),
    ((2, 128), F32),
    ((2, 128), F32),
    ((2, 128), F32),
    ((2, B, 2, CH), F32),
    ((3, 2, CH), F32),
    ((2, 2, 2, 4, B), F32),
)


def values_kernel(scaled, inv, *refs):
    far, refs = refs[:15], refs[15:]
    packed, conv_out, stack, *kept = refs[: 3 + len(KEPT)]
    w_gate, w_value, w_step, next_step, next_write, next_read, sems, late_sems = refs[3 + len(KEPT) :]
    gate_far, value_far, step_far, write_far, read_far, state_far, out_far, *tables_far = far
    tables_group, tables_rest = tables_far[0], tables_far[1:]
    late_sources = [
        state_far.at[0], out_far.at[0], tables_group, state_far.at[1], out_far.at[1], *tables_rest
    ]
    late = list(zip(late_sources, kept))
    small = [(src, dst) for src, dst in late[6:11]]
    now = [(gate_far.at[0], w_gate), (value_far.at[0], w_value), (step_far.at[0], w_step)] + small
    copies = start_all(now, sems)
    late = late[:6] + late[11:]
    late += [
        (gate_far.at[1], stack.at[:CH]),
        (value_far.at[1], stack.at[CH : 2 * CH]),
        (step_far.at[1], next_step),
        (write_far.at[1], next_write),
        (read_far.at[1], next_read),
    ]
    late = start_all(late, late_sems)
    for copy in copies:
        copy.wait()
    hidden = scaled[...]
    inv_col = inv[:, :CH]
    gate = dot_nt(hidden, w_gate[...]) * inv_col
    fresh = dot_nt(hidden, w_value[...]) * inv_col
    raw = of_head(jnp.dot(hidden, w_step[...], preferred_element_type=F32) * inv[...])
    tables, conv, taps = kept[6:9], kept[9], kept[10]
    push, direct, gate, decay = gated_values(0, gate, fresh, raw, tables, conv.at[0], taps)
    packed[0] = push
    packed[1] = direct
    packed[2] = gate
    packed[3] = jnp.broadcast_to(decay, (B, CH))
    conv_out[:, 0, :] = conv[0, :, 1, :]
    conv_out[:, 1, :] = fresh
    for copy in late:
        copy.wait()
    head = lax.axis_index(("z", "y", "x"))
    hot = (lax.broadcasted_iota(jnp.int32, (8, 128), 1) == head).astype(F32).astype(BF16)
    stack[2 * CH : 2 * CH + 8] = dot_nt(hot, next_step[...]).astype(BF16)
    both = jnp.concatenate([next_write[...].astype(F32), next_read[...].astype(F32)], axis=0)
    stack[2 * CH + 8 :] = both.astype(BF16)


def make_values(scaled, inv, far):
    outs = [pltpu.VMEM((4, B, CH), F32), pltpu.VMEM((B, 2, CH), F32), pltpu.VMEM((ROWS, D), BF16)]
    outs += [pltpu.VMEM(*p) for p in KEPT]
    scratch = [pltpu.VMEM(*p) for p in NOW_FAR + NEXT_FAR]
    scratch += [pltpu.SemaphoreType.DMA((8,)), pltpu.SemaphoreType.DMA((12,))]
    return call(values_kernel, "values", [scaled, inv], far, outs, scratch)


def advance(push, direct, gate, decay, writes, reads, state, w_out, gain, fresh, sent):
    lane = lax.broadcasted_iota(jnp.int32, (CH, B), 1)
    found = jnp.zeros((CH, B), F32)
    for b in range(B):
        new = decay[b : b + 1] * state[b] + push[:, b : b + 1] * writes[b : b + 1]
        fresh[b] = new
        total = jnp.sum(new * reads[b : b + 1], axis=1, keepdims=True)
        found = jnp.where(lane == b, total, found)
    gated = (found.T + direct) * gate
    total = as_row(jnp.sum(gated * gated, axis=1, keepdims=True))
    high, low = hi_lo(total)
    row = lax.broadcasted_iota(jnp.int32, (8, B), 0)
    tail = jnp.where(row == 0, high, jnp.where(row == 1, low, 0.0))
    tail = jnp.concatenate([tail, jnp.zeros((8, 128 - B), F32)], axis=1).astype(BF16)
    out = jnp.dot((gated * gain).astype(BF16), w_out[...], preferred_element_type=F32)
    for j in range(D // 128):
        sent[j, :B] = out[:, 128 * j : 128 * j + 128].astype(BF16)
        sent[j, B:] = tail


PLANE_SUMS = ((32, B + 8, 128), BF16)


def first_mix_kernel(keys, packed, state, w_out, gain, fresh, sent, weights, later, last_taps, lines):
    lines[...] = keys[lax.axis_index("z") // 4].astype(F32)
    weights[0] = lines[pl.ds(0, N, stride=4), :].astype(BF16)
    weights[1] = lines[pl.ds(1, N, stride=4), :].astype(BF16)
    first = lines[pl.ds(2, N, stride=4), :].T
    second = lines[pl.ds(3, N, stride=4), :].T
    later[0] = first[2 * B : 3 * B]
    later[1] = first[3 * B :]
    last_taps[...] = second[2 * B : 2 * B + 8]
    writes = first[:B] + second[:B]
    reads = first[B : 2 * B] + second[B : 2 * B]
    advance(
        packed[0], packed[1], packed[2], packed[3][:, :1], writes, reads, state, w_out, gain[:1, :], fresh, sent
    )


def first_mix(keys, packed, kept):
    return call(
        first_mix_kernel,
        "mix0",
        [keys, packed, *kept],
        [],
        [
            pltpu.VMEM(*STATE),
            pltpu.VMEM(*PLANE_SUMS),
            pltpu.VMEM((2, N, 128), BF16),
            pltpu.VMEM((2, B, N), F32),
            pltpu.VMEM((8, N), F32),
        ],
        [pltpu.VMEM((4 * N, 128), F32)],
    )


def next_mix_kernel(own, other, stack, later, last_taps, state, w_out, gain, norm_gain, *refs):
    tables, conv, taps, key_conv, key_before, value_before = refs[:3], refs[3], refs[4], refs[5], refs[6], refs[7]
    fresh, sent, key_out, value_out, hid, scaled = refs[8:]
    core = lax.axis_index("c")
    sums = [jnp.zeros((B, N), F32), jnp.zeros((B, N), F32)]
    for at in range(16):
        for whose, side in ((own, core), (other, 1 - core)):
            hid[2 * at + side] = whose[at, :B]
            for kind in range(2):
                sums[kind] += whose[at, B * (kind + 1) : B * (kind + 2)].astype(F32)
    inv = scale_tokens(lambda j: hid[j], norm_gain.at[1:], scaled)
    found = dot_nt(scaled[...], stack[...]) * inv
    keys = [silu(later[k] + sums[k] * inv * (last_taps[2 * k : 2 * k + 1] + last_taps[2 * k + 1 : 2 * k + 2])) for k in range(2)]
    fresh_values = found[:, CH : 2 * CH]
    push, direct, gate, decay = gated_values(
        1, found[:, :CH], fresh_values, found[:, 2 * CH : 2 * CH + 1], tables, conv.at[1], taps
    )
    advance(push, direct, gate, decay, keys[0], keys[1], state, w_out, gain[1:, :], fresh, sent)
    value_out[0] = value_before[...]
    value_out[1, :, 0, :] = conv[1, :, 1, :]
    value_out[1, :, 1, :] = fresh_values
    turned = found.T
    key_out[0] = key_before[...]
    for kind in range(2):
        key_out[1, 0, kind] = key_conv[1, 1, kind]
        key_out[1, 1, kind] = turned[2 * CH + 8 + 4 * kind : 2 * CH + 12 + 4 * kind]


def next_mix(own, other, stack, later, last_taps, kept, key_before, value_before):
    return call(
        next_mix_kernel,
        "mix1",
        [own, other, stack, later, last_taps, *kept, key_before, value_before],
        [],
        [
            pltpu.VMEM(*STATE),
            pltpu.VMEM(*PLANE_SUMS),
            shaped((2, 2, 2, 4, B), F32),
            shaped((2, B, 2, CH), F32),
        ],
        [pltpu.VMEM((32, B, 128), BF16), pltpu.VMEM((B, D), BF16)],
    )


def scale_kernel(layer, got, fresh, *refs):
    sent, states, sem = refs[-3:]
    write_back = pltpu.make_async_copy(fresh, states.at[layer], sem)
    write_back.start()
    total = got[0].astype(F32)
    for j in range(1, 32):
        total += got[j].astype(F32)
    squares = total[B : B + 1, :B] + total[B + 1 : B + 2, :B]
    factor = as_col(lax.rsqrt(squares / GW + EPS))
    chunk = (total[:B] * factor).astype(BF16)
    for plane in range(8):
        sent[plane] = chunk
    write_back.wait()


def make_scale(layer, got, fresh, states):
    return call(
        functools.partial(scale_kernel, layer),
        f"scale{layer}",
        [got, fresh],
        [states] if layer else [],
        [pltpu.VMEM((8, B, 128), BF16), pltpu.HBM((2, B, CH, N), F32)],
        [pltpu.SemaphoreType.DMA],
        {2: 1} if layer else {},
    )


def first_add_kernel(got, hid, norm_gain, weights, sent):
    total = got[0].astype(F32)
    for plane in range(1, 8):
        total += got[plane].astype(F32)
    cols = pl.ds(pl.multiple_of(128 * lax.axis_index(PLANE), 128), 128)
    chunk = (hid[:, cols].astype(F32) + total).astype(BF16)
    scaled = (chunk.astype(F32) * norm_gain[1:, cols]).astype(BF16)
    shares = [dot_nt(scaled, weights[kind]).astype(BF16) for kind in range(2)]
    for j in range(16):
        sent[j, :B] = chunk
        sent[j, B : 2 * B] = shares[0]
        sent[j, 2 * B :] = shares[1]


def next_add_kernel(got, hid, sent):
    total = got[0].astype(F32)
    for plane in range(1, 8):
        total += got[plane].astype(F32)
    chunk = (hid[lax.axis_index(("y", "x")), :B].astype(F32) + total).astype(BF16)
    for j in range(32):
        sent[j] = chunk


def exchange(value, axes):
    return lax.all_to_all(value, axes, split_axis=0, concat_axis=0, tiled=True)


def per_device(
    tokens,
    norm_gain,
    w_gate,
    w_value,
    w_write,
    w_read,
    w_step,
    step_bias,
    decay_rate,
    skip_gain,
    conv_value_weight,
    conv_key_weight,
    group_gain,
    w_out,
    ssm_state,
    conv_value,
    conv_key,
):
    w_gate, w_value, w_write, w_read = (jnp.swapaxes(w, 1, 2) for w in (w_gate, w_value, w_write, w_read))
    conv_key = jnp.transpose(conv_key, (0, 2, 3, 4, 1))
    value_taps = jnp.swapaxes(conv_value_weight, 0, 1)
    far = [w_gate, w_value, w_step, w_write, w_read, ssm_state, w_out, group_gain, norm_gain]
    far += [step_bias, decay_rate, skip_gain, conv_value, value_taps, conv_key]
    msg, key_out, scaled, inv, hid = make_keys(tokens, [norm_gain, w_write, w_read, conv_key, conv_key_weight])
    keys = exchange(msg, ("c", "z", "y", "x")).reshape(2, 4 * N, 128)
    packed, value_out, stack, *kept = make_values(scaled, inv, far)
    state, out, gain, next_state, next_out, *rest = kept
    fresh, sent, weights, later, last_taps = first_mix(keys, packed, [state, out, gain])
    sent, states = make_scale(0, exchange(sent, PLANE), fresh, None)
    (sent,) = call(
        first_add_kernel,
        "add0",
        [exchange(sent, ("z",)), hid, rest[0], weights],
        [],
        [pltpu.VMEM((16, 3 * B, 128), BF16)],
    )
    own = exchange(sent, ("y", "x"))
    other = lax.ppermute(own, "c", [(0, 1), (1, 0)])
    fresh, sent, key_out, value_out = next_mix(
        own, other, stack, later, last_taps, [next_state, next_out, gain, *rest], key_out, value_out
    )
    sent, states = make_scale(1, exchange(sent, PLANE), fresh, states)
    (sent,) = call(next_add_kernel, "add1", [exchange(sent, ("z",)), own], [], [pltpu.VMEM((32, B, 128), BF16)])
    hid = exchange(sent, PLANE)
    tokens_out = jnp.transpose(hid, (1, 0, 2)).reshape(B, D)
    return (tokens_out, states, value_out, jnp.transpose(key_out, (0, 4, 1, 2, 3)))


def solution(mesh):
    torus = Mesh(mesh.devices.reshape(8, 4, 4, 2), TP)
    in_specs = (
        P(),
        P(),
        P(None, None, TP),
        P(None, None, TP),
        P(None, None, TP),
        P(None, None, TP),
        P(),
        P(),
        P(),
        P(),
        P(None, None, TP),
        P(None, None, None, TP),
        P(None, TP),
        P(None, TP, None),
        P(None, None, TP, None),
        P(None, None, None, TP),
        P(None, None, None, None, TP),
    )
    out_specs = (
        P(),
        P(None, None, TP, None),
        P(None, None, None, TP),
        P(None, None, None, None, TP),
    )
    return jax.shard_map(
        per_device, mesh=torus, in_specs=in_specs, out_specs=out_specs, check_vma=False
    )
```

time: 131 us -> 117 us (0.89)
  waiting for transfers between devices: 21 us -> 13.5 us
  starting transfers between devices: 20.8 us -> 17.6 us
  Pallas kernels: 14.8 us -> 12.8 us
    all_to_all x2 -> x1, waiting for transfers between devices: 21 us -> 12.1 us  [exchange(): return lax.all_to_all(value, axes, split_axis=0, concat_axis=0, tiled=True)]
    all_to_all x2 -> x1, starting transfers between devices: 20.8 us -> 15.7 us  [exchange(): return lax.all_to_all(value, axes, split_axis=0, concat_axis=0, tiled=True)]
    pallas_call x10 -> x8, Pallas kernels: 14.8 us -> 12.8 us  [call(): pl.pallas_call(body, in_specs=[vmem()] * len(near) + [anywhere()] * len(f...]
    ppermute x0 -> x1, starting transfers between devices: none -> 1.95 us  [per_device(): other = lax.ppermute(own, 'c', [(0, 1), (1, 0)])]
    ppermute x0 -> x1, waiting for transfers between devices: none -> 1.35 us  [per_device(): other = lax.ppermute(own, 'c', [(0, 1), (1, 0)])]
  transfers between devices with their start and end apart: 2 -> 2, of which waited for: 2 -> 2; matrix products, arithmetic and copies ran while one was open for 0% -> 0% of each run, Pallas kernels for 4% -> 3%
where the time goes in v3:
time: 117 us
  blocking collectives  71.6 us (61%)
  starting transfers between devices  17.6 us (15%)
  waiting for transfers between devices  13.5 us (12%)
  Pallas kernels  12.8 us (11%)
    all_to_all x6, blocking collectives, exchange(): return lax.all_to_all(value, axes, split_axis=0, concat_axis=0, tiled=True)  71.6 us
    all_to_all x1, starting transfers between devices, exchange(): return lax.all_to_all(value, axes, split_axis=0, concat_axis=0, tiled=True)  15.7 us
    pallas_call x8, Pallas kernels, call(): pl.pallas_call(body, in_specs=[vmem()] * len(near) + [anywhere()] * len(f...  12.8 us
    all_to_all x1, waiting for transfers between devices, exchange(): return lax.all_to_all(value, axes, split_axis=0, concat_axis=0, tiled=True)  12.1 us
  transfers between devices with their start and end apart: 2, of which 2 were waited for; matrix products, arithmetic and copies ran while one was open for 0% of the time, Pallas kernels for 3%

profile of v3, /device:TPU:1, one launch (start us, length us, event | category | flops | bytes accessed | tf_op | source)
XLA Modules:
  0.0 117.0 jit_solution(1605710133251458789)
XLA Ops:
  0.6 2.2 %keys.1 = (bf16[256,4,128]{2,1,0:T(4,128)(2,1)}, f32[2,2,4,32]{3,2,1,0:T(4,128)S(1)}, bf16[32,4096]{1,0:T(8,128)(2,1)S(1)}, f32[32,128]{1,0:T(8,128)S(1)}, bf16[32,4096]{1,0:T(8,128)(2,1)S(1)}) custom-call(bf16[32,4096]{1,0:T(8,128)(2,1)} %tokens.1, f32[2,4096]{1,0:T(2,128)} %refs_8_.1, bf16[2,4,4096]{2,1,0:T(4,128)(2,1)} %bitcast.17, ...), custom_call_target="tpu_custom_call" | custom-call | tf_op jit(solution)/shard_map/keys/pallas_call | solution.py:50
  2.9 15.7 %all-to-all-start = ((bf16[256,4,128]{2,1,0:T(4,128)(2,1)}), bf16[256,4,128]{2,1,0:T(4,128)(2,1)S(1)}, u32[]{:S(2)}, u32[]{:S(2)}) async-start(bf16[256,4,128]{2,1,0:T(4,128)(2,1)} %get-tuple-element.37), calls=%async_computation | async-start | bytes 524288 | tf_op jit(solution)/shard_map/all_to_all | solution.py:412
  18.5 3.6 %values.1 = (f32[4,32,32]{2,1,0:T(8,128)S(1)}, f32[32,2,32]{2,1,0:T(2,128)S(1)}, bf16[80,4096]{1,0:T(8,128)(2,1)S(1)}, f32[32,32,128]{2,1,0:T(8,128)S(1)}, bf16[...) custom-call(bf16[32,4096]{1,0:T(8,128)(2,1)S(1)} %get-tuple-element., ...), custom_call_target="tpu_custom_call" | custom-call | tf_op jit(solution)/shard_map/values/pallas_call | solution.py:50
  22.1 12.1 %all-to-all-done = bf16[256,4,128]{2,1,0:T(4,128)(2,1)S(1)} async-done(((bf16[256,4,128]{2,1,0:T(4,128)(2,1)}), bf16[256,4,128]{2,1,0:T(4,128)(2,1)S(1)}, u32[]{:S(2)}, u32[]{:S(2)}) %all-to-all-start) | async-done | bytes 262176 | tf_op jit(solution)/shard_map/all_to_all | solution.py:412
  34.2 2.4 %mix0.1 = (f32[32,32,128]{2,1,0:T(8,128)S(1)}, bf16[32,40,128]{2,1,0:T(8,128)(2,1)S(1)}, bf16[2,128,128]{2,1,0:T(8,128)(2,1)S(1)}, f32[2,32,128]{2,1,0:T(8,128)S(1)}, f32[8,128]{1,0:T(8,128)S(1)}) custom-call(bf16[2,512,128]{2,1,0:T(8,128)(2,1)S(1)} %bitcast.14, f32[4,32,32]{2,1,0:T(8,128)S(1)} %get-tuple-element.40.packed, ...), custom_call_target="tpu_custom_call" | custom-call | tf_op jit(solution)/shard_map/mix0/pallas_call | solution.py:50
  36.7 13.3 %all_to_all.35.got = bf16[32,40,128]{2,1,0:T(8,128)(2,1)S(1)} all-to-all(bf16[32,40,128]{2,1,0:T(8,128)(2,1)S(1)} %get-tuple-element.44), channel_id=1, replica_groups=mesh['z'=8,'y'=4,'x'=4,'c'=2] {'y','x','c'}, dimensions={0} | all-to-all | bytes 655360 | tf_op jit(solution)/shard_map/all_to_all | solution.py:412
  50.0 0.8 scale0.1
  50.8 9.5 %all_to_all.36.got = bf16[8,32,128]{2,1,0:T(8,128)(2,1)S(1)} all-to-all(bf16[8,32,128]{2,1,0:T(8,128)(2,1)S(1)} %get-tuple-element.46), channel_id=1, replica_groups=mesh['z'=8,'y'=4,'x'=4,'c'=2] {'z'}, dimensions={0} | all-to-all | bytes 131072 | tf_op jit(solution)/shard_map/all_to_all | solution.py:412
  60.3 0.2 add0.1
  60.5 12.7 %all_to_all.37.own.hid = bf16[16,96,128]{2,1,0:T(8,128)(2,1)S(1)} all-to-all(bf16[16,96,128]{2,1,0:T(8,128)(2,1)S(1)} %add0.1), channel_id=1, replica_groups=mesh['z'=8,'y'=4,'x'=4,'c'=2] {'y','x'}, dimensions={0} | all-to-all | bytes 786432 | tf_op jit(solution)/shard_map/all_to_all | solution.py:412
  73.2 2.0 %collective-permute-start = (bf16[16,96,128]{2,1,0:T(8,128)(2,1)S(1)}, bf16[16,96,128]{2,1,0:T(8,128)(2,1)S(1)}, u32[]{:S(2)}, u32[]{:S(2)}) collective-permute-start(bf16[16,96,128]{2,1,0:T(8,128)(2,1)S(1)} %all_to_all.37.own.hid), channel_id=1, source_target_pairs={{0,1},{1,0},{2,3},{3,2},{4,5},{5,4},{6,7},{7,6},{8,9},{9,8},{10,11... | collective-permute-start | bytes 1179656 | tf_op jit(solution)/shard_map/ppermute | solution.py:453
  75.2 1.3 %collective-permute-done.other = bf16[16,96,128]{2,1,0:T(8,128)(2,1)S(1)} collective-permute-done((bf16[16,96,128]{2,1,0:T(8,128)(2,1)S(1)}, bf16[16,96,128]{2,1,0:T(8,128)(2,1)S(1)}, u32[]{:S(2)}, u32[]{:S(2)}) %collective-permute-start) | collective-permute-done | bytes 393248 | tf_op jit(solution)/shard_map/ppermute | solution.py:453
  76.5 2.8 %mix1.1 = (f32[32,32,128]{2,1,0:T(8,128)S(1)}, bf16[32,40,128]{2,1,0:T(8,128)(2,1)S(1)}, f32[2,2,2,4,32]{4,3,2,1,0:T(4,128)}, f32[2,32,2,32]{3,2,1,0:T(2,128)}) custom-call(bf16[16,96,128]{2,1,0:T(8,128)(2,1)S(1)} %all_to_all.37.own.hid, bf16[16,96,128]{2,1,0:T(8,128)(2,1)S(1)} %collective-permute-done.other, bf16[80,4096]{1,0:T(8,128)(2,1)S(1)} %get-tuple-element.50.stack, ...), custom_call_target="tpu_custom_call" | custom-call | tf_op jit(solution)/shard_map/mix1/pallas_call | solution.py:50
  79.4 12.8 %all_to_all.38.got = bf16[32,40,128]{2,1,0:T(8,128)(2,1)S(1)} all-to-all(bf16[32,40,128]{2,1,0:T(8,128)(2,1)S(1)} %get-tuple-element.63), channel_id=1, replica_groups=mesh['z'=8,'y'=4,'x'=4,'c'=2] {'y','x','c'}, dimensions={0} | all-to-all | bytes 655360 | tf_op jit(solution)/shard_map/all_to_all | solution.py:412
  92.2 0.8 scale1.1
  93.0 9.5 %all_to_all.39.got = bf16[8,32,128]{2,1,0:T(8,128)(2,1)S(1)} all-to-all(bf16[8,32,128]{2,1,0:T(8,128)(2,1)S(1)} %get-tuple-element.66), channel_id=1, replica_groups=mesh['z'=8,'y'=4,'x'=4,'c'=2] {'z'}, dimensions={0} | all-to-all | bytes 131072 | tf_op jit(solution)/shard_map/all_to_all | solution.py:412
  102.6 13.7 %all_to_all.40 = bf16[32,32,128]{2,1,0:T(8,128)(2,1)S(1)} all-to-all(bf16[32,32,128]{2,1,0:T(8,128)(2,1)S(1)} %add1.1), channel_id=1, replica_groups=mesh['z'=8,'y'=4,'x'=4,'c'=2] {'y','x','c'}, dimensions={0} | all-to-all | bytes 524288 | tf_op jit(solution)/shard_map/all_to_all | solution.py:412
  116.2 0.7 copy_bitcast_fusion
  (1 shorter events, 0.0 us)
Async XLA Ops:
  2.9 31.4 %all-to-all-start = ((bf16[256,4,128]{2,1,0:T(4,128)(2,1)}), bf16[256,4,128]{2,1,0:T(4,128)(2,1)S(1)}, u32[]{:S(2)}, u32[]{:S(2)}) async-start(bf16[256,4,128]{2,1,0:T(4,128)(2,1)} %get-tuple-element.37), calls=%async_computation | async-start | bytes 524288 | tf_op jit(solution)/shard_map/all_to_all | solution.py:412
  73.2 3.3 %collective-permute-start = (bf16[16,96,128]{2,1,0:T(8,128)(2,1)S(1)}, bf16[16,96,128]{2,1,0:T(8,128)(2,1)S(1)}, u32[]{:S(2)}, u32[]{:S(2)}) collective-permute-start(bf16[16,96,128]{2,1,0:T(8,128)(2,1)S(1)} %all_to_all.37.own.hid), channel_id=1, source_target_pairs={{0,1},{1,0},{2,3},{3,2},{4,5},{5,4},{6,7},{7,6},{8,9},{9,8},{10,11... | collective-permute-start | bytes 1179656 | tf_op jit(solution)/shard_map/ppermute | solution.py:453

commit v4 on v3

--- a/solution.py
+++ b/solution.py
@@ -206,8 +206,8 @@
 
 def values_kernel(scaled, inv, *refs):
     far, refs = refs[:15], refs[15:]
-    packed, conv_out, stack, *kept = refs[: 3 + len(KEPT)]
-    w_gate, w_value, w_step, next_step, next_write, next_read, sems, late_sems = refs[3 + len(KEPT) :]
+    packed, decay_out, conv_out, stack, *kept = refs[: 4 + len(KEPT)]
+    w_gate, w_value, w_step, next_step, next_write, next_read, sems, late_sems = refs[4 + len(KEPT) :]
     gate_far, value_far, step_far, write_far, read_far, state_far, out_far, *tables_far = far
     tables_group, tables_rest = tables_far[0], tables_far[1:]
     late_sources = [
@@ -238,7 +238,7 @@
     packed[0] = push
     packed[1] = direct
     packed[2] = gate
-    packed[3] = jnp.broadcast_to(decay, (B, CH))
+    decay_out[...] = jnp.broadcast_to(decay, (B, N))
     conv_out[:, 0, :] = conv[0, :, 1, :]
     conv_out[:, 1, :] = fresh
     for copy in late:
@@ -251,21 +251,36 @@
 
 
 def make_values(scaled, inv, far):
-    outs = [pltpu.VMEM((4, B, CH), F32), pltpu.VMEM((B, 2, CH), F32), pltpu.VMEM((ROWS, D), BF16)]
+    outs = [pltpu.VMEM((3, B, CH), F32), pltpu.VMEM((B, N), F32)]
+    outs += [pltpu.VMEM((B, 2, CH), F32), pltpu.VMEM((ROWS, D), BF16)]
     outs += [pltpu.VMEM(*p) for p in KEPT]
     scratch = [pltpu.VMEM(*p) for p in NOW_FAR + NEXT_FAR]
     scratch += [pltpu.SemaphoreType.DMA((8,)), pltpu.SemaphoreType.DMA((12,))]
     return call(values_kernel, "values", [scaled, inv], far, outs, scratch)
 
 
-def advance(push, direct, gate, decay, writes, reads, state, w_out, gain, fresh, sent):
+def advance(layer, push, direct, gate, writes, reads, state, w_out, gain, sent, states, scratch):
+    fresh, decay_rows, read_rows, sems = scratch
+    read_rows[...] = reads
+    high, low = hi_lo(push)
+    left = jnp.concatenate([high, high, low], axis=1)
+    high, low = hi_lo(writes)
+    right = jnp.concatenate([high, low, high], axis=0).astype(BF16)
+    of = lax.broadcasted_iota(jnp.int32, left.shape, 1) % B
+    left = jnp.concatenate([jnp.where(of == b, left, 0.0).astype(BF16) for b in range(B)], axis=0)
+    pushed = jnp.dot(left, right, preferred_element_type=F32)
     lane = lax.broadcasted_iota(jnp.int32, (CH, B), 1)
     found = jnp.zeros((CH, B), F32)
+    copies = []
     for b in range(B):
-        new = decay[b : b + 1] * state[b] + push[:, b : b + 1] * writes[b : b + 1]
+        new = decay_rows[b : b + 1, :] * state[b] + pushed[CH * b : CH * (b + 1)]
         fresh[b] = new
-        total = jnp.sum(new * reads[b : b + 1], axis=1, keepdims=True)
+        total = jnp.sum(new * read_rows[b : b + 1, :], axis=1, keepdims=True)
         found = jnp.where(lane == b, total, found)
+        if b % 8 == 7:
+            part = pl.ds(b - 7, 8)
+            copies.append(pltpu.make_async_copy(fresh.at[part], states.at[layer, part], sems.at[b // 8]))
+            copies[-1].start()
     gated = (found.T + direct) * gate
     total = as_row(jnp.sum(gated * gated, axis=1, keepdims=True))
     high, low = hi_lo(total)
@@ -276,12 +291,22 @@
     for j in range(D // 128):
         sent[j, :B] = out[:, 128 * j : 128 * j + 128].astype(BF16)
         sent[j, B:] = tail
+    for copy in copies:
+        copy.wait()
+
+
+STATES = ((2, B, CH, N), F32)
+ADVANCE = (STATE, ((B, N), F32), ((B, N), F32))
+
+
+def advance_scratch():
+    return [pltpu.VMEM(*p) for p in ADVANCE] + [pltpu.SemaphoreType.DMA((4,))]
 
 
 PLANE_SUMS = ((32, B + 8, 128), BF16)
 
 
-def first_mix_kernel(keys, packed, state, w_out, gain, fresh, sent, weights, later, last_taps, lines):
+def first_mix_kernel(keys, packed, decay, state, w_out, gain, states, sent, weights, later, last_taps, lines, *scratch):
     lines[...] = keys[lax.axis_index("z") // 4].astype(F32)
     weights[0] = lines[pl.ds(0, N, stride=4), :].astype(BF16)
     weights[1] = lines[pl.ds(1, N, stride=4), :].astype(BF16)
@@ -292,31 +317,32 @@
     last_taps[...] = second[2 * B : 2 * B + 8]
     writes = first[:B] + second[:B]
     reads = first[B : 2 * B] + second[B : 2 * B]
+    scratch[1][...] = decay[...]
     advance(
-        packed[0], packed[1], packed[2], packed[3][:, :1], writes, reads, state, w_out, gain[:1, :], fresh, sent
-    )
-
-
-def first_mix(keys, packed, kept):
+        0, packed[0], packed[1], packed[2], writes, reads, state, w_out, gain[:1, :], sent, states, scratch
+    )
+
+
+def first_mix(keys, packed, decay, kept):
     return call(
         first_mix_kernel,
         "mix0",
-        [keys, packed, *kept],
+        [keys, packed, decay, *kept],
         [],
         [
-            pltpu.VMEM(*STATE),
+            pltpu.HBM(*STATES),
             pltpu.VMEM(*PLANE_SUMS),
             pltpu.VMEM((2, N, 128), BF16),
             pltpu.VMEM((2, B, N), F32),
             pltpu.VMEM((8, N), F32),
         ],
-        [pltpu.VMEM((4 * N, 128), F32)],
+        [pltpu.VMEM((4 * N, 128), F32)] + advance_scratch(),
     )
 
 
 def next_mix_kernel(own, other, stack, later, last_taps, state, w_out, gain, norm_gain, *refs):
     tables, conv, taps, key_conv, key_before, value_before = refs[:3], refs[3], refs[4], refs[5], refs[6], refs[7]
-    fresh, sent, key_out, value_out, hid, scaled = refs[8:]
+    states, sent, key_out, value_out, hid, scaled, *scratch = refs[9:]
     core = lax.axis_index("c")
     sums = [jnp.zeros((B, N), F32), jnp.zeros((B, N), F32)]
     for at in range(16):
@@ -331,7 +357,8 @@
     push, direct, gate, decay = gated_values(
         1, found[:, :CH], fresh_values, found[:, 2 * CH : 2 * CH + 1], tables, conv.at[1], taps
     )
-    advance(push, direct, gate, decay, keys[0], keys[1], state, w_out, gain[1:, :], fresh, sent)
+    scratch[1][...] = jnp.broadcast_to(decay, (B, N))
+    advance(1, push, direct, gate, keys[0], keys[1], state, w_out, gain[1:, :], sent, states, scratch)
     value_out[0] = value_before[...]
     value_out[1, :, 0, :] = conv[1, :, 1, :]
     value_out[1, :, 1, :] = fresh_values
@@ -342,26 +369,24 @@
         key_out[1, 1, kind] = turned[2 * CH + 8 + 4 * kind : 2 * CH + 12 + 4 * kind]
 
 
-def next_mix(own, other, stack, later, last_taps, kept, key_before, value_before):
+def next_mix(own, other, stack, later, last_taps, kept, key_before, value_before, states):
     return call(
         next_mix_kernel,
         "mix1",
         [own, other, stack, later, last_taps, *kept, key_before, value_before],
-        [],
+        [states],
         [
-            pltpu.VMEM(*STATE),
+            pltpu.HBM(*STATES),
             pltpu.VMEM(*PLANE_SUMS),
             shaped((2, 2, 2, 4, B), F32),
             shaped((2, B, 2, CH), F32),
         ],
-        [pltpu.VMEM((32, B, 128), BF16), pltpu.VMEM((B, D), BF16)],
-    )
-
-
-def scale_kernel(layer, got, fresh, *refs):
-    sent, states, sem = refs[-3:]
-    write_back = pltpu.make_async_copy(fresh, states.at[layer], sem)
-    write_back.start()
+        [pltpu.VMEM((32, B, 128), BF16), pltpu.VMEM((B, D), BF16)] + advance_scratch(),
+        {17: 0},
+    )
+
+
+def scale_kernel(got, sent):
     total = got[0].astype(F32)
     for j in range(1, 32):
         total += got[j].astype(F32)
@@ -370,19 +395,10 @@
     chunk = (total[:B] * factor).astype(BF16)
     for plane in range(8):
         sent[plane] = chunk
-    write_back.wait()
-
-
-def make_scale(layer, got, fresh, states):
-    return call(
-        functools.partial(scale_kernel, layer),
-        f"scale{layer}",
-        [got, fresh],
-        [states] if layer else [],
-        [pltpu.VMEM((8, B, 128), BF16), pltpu.HBM((2, B, CH, N), F32)],
-        [pltpu.SemaphoreType.DMA],
-        {2: 1} if layer else {},
-    )
+
+
+def make_scale(got):
+    return call(scale_kernel, "scale", [got], [], [pltpu.VMEM((8, B, 128), BF16)])[0]
 
 
 def first_add_kernel(got, hid, norm_gain, weights, sent):
@@ -438,10 +454,10 @@
     far += [step_bias, decay_rate, skip_gain, conv_value, value_taps, conv_key]
     msg, key_out, scaled, inv, hid = make_keys(tokens, [norm_gain, w_write, w_read, conv_key, conv_key_weight])
     keys = exchange(msg, ("c", "z", "y", "x")).reshape(2, 4 * N, 128)
-    packed, value_out, stack, *kept = make_values(scaled, inv, far)
+    packed, decay, value_out, stack, *kept = make_values(scaled, inv, far)
     state, out, gain, next_state, next_out, *rest = kept
-    fresh, sent, weights, later, last_taps = first_mix(keys, packed, [state, out, gain])
-    sent, states = make_scale(0, exchange(sent, PLANE), fresh, None)
+    states, sent, weights, later, last_taps = first_mix(keys, packed, decay, [state, out, gain])
+    sent = make_scale(exchange(sent, PLANE))
     (sent,) = call(
         first_add_kernel,
         "add0",
@@ -451,10 +467,10 @@
     )
     own = exchange(sent, ("y", "x"))
     other = lax.ppermute(own, "c", [(0, 1), (1, 0)])
-    fresh, sent, key_out, value_out = next_mix(
-        own, other, stack, later, last_taps, [next_state, next_out, gain, *rest], key_out, value_out
-    )
-    sent, states = make_scale(1, exchange(sent, PLANE), fresh, states)
+    states, sent, key_out, value_out = next_mix(
+        own, other, stack, later, last_taps, [next_state, next_out, gain, *rest], key_out, value_out, states
+    )
+    sent = make_scale(exchange(sent, PLANE))
     (sent,) = call(next_add_kernel, "add1", [exchange(sent, ("z",)), own], [], [pltpu.VMEM((32, B, 128), BF16)])
     hid = exchange(sent, PLANE)
     tokens_out = jnp.transpose(hid, (1, 0, 2)).reshape(B, D)

time: 117 us -> 114 us (0.974)
  Pallas kernels: 12.8 us -> 9.72 us
    pallas_call x8, Pallas kernels: 12.8 us -> 9.72 us  [call(): pl.pallas_call(body, in_specs=[vmem()] * len(near) + [anywhere()] * len(f...]
where the time goes in v4:
time: 114 us
  blocking collectives  71.6 us (63%)
  starting transfers between devices  17.6 us (15%)
  waiting for transfers between devices  13.5 us (12%)
  Pallas kernels  9.72 us (9%)
    all_to_all x6, blocking collectives, exchange(): return lax.all_to_all(value, axes, split_axis=0, concat_axis=0, tiled=True)  71.6 us
    all_to_all x1, starting transfers between devices, exchange(): return lax.all_to_all(value, axes, split_axis=0, concat_axis=0, tiled=True)  15.7 us
    all_to_all x1, waiting for transfers between devices, exchange(): return lax.all_to_all(value, axes, split_axis=0, concat_axis=0, tiled=True)  12.1 us
    pallas_call x8, Pallas kernels, call(): pl.pallas_call(body, in_specs=[vmem()] * len(near) + [anywhere()] * len(f...  9.72 us
  transfers between devices with their start and end apart: 2, of which 2 were waited for; matrix products, arithmetic and copies ran while one was open for 0% of the time, Pallas kernels for 3%

profile of v4, /device:TPU:1, one launch (start us, length us, event | category | flops | bytes accessed | tf_op | source)
XLA Modules:
  0.0 113.8 jit_solution(15955076505605482123)
XLA Ops:
  0.6 2.2 %keys.1 = (bf16[256,4,128]{2,1,0:T(4,128)(2,1)}, f32[2,2,4,32]{3,2,1,0:T(4,128)S(1)}, bf16[32,4096]{1,0:T(8,128)(2,1)S(1)}, f32[32,128]{1,0:T(8,128)S(1)}, bf16[32,4096]{1,0:T(8,128)(2,1)S(1)}) custom-call(bf16[32,4096]{1,0:T(8,128)(2,1)} %tokens.1, f32[2,4096]{1,0:T(2,128)} %refs_8_.1, bf16[2,4,4096]{2,1,0:T(4,128)(2,1)} %bitcast.17, ...), custom_call_target="tpu_custom_call" | custom-call | tf_op jit(solution)/shard_map/keys/pallas_call | solution.py:50
  2.9 15.7 %all-to-all-start = ((bf16[256,4,128]{2,1,0:T(4,128)(2,1)}), bf16[256,4,128]{2,1,0:T(4,128)(2,1)S(1)}, u32[]{:S(2)}, u32[]{:S(2)}) async-start(bf16[256,4,128]{2,1,0:T(4,128)(2,1)} %get-tuple-element.34), calls=%async_computation | async-start | bytes 524288 | tf_op jit(solution)/shard_map/all_to_all | solution.py:428
  18.5 3.6 %values.1 = (f32[3,32,32]{2,1,0:T(8,128)S(1)}, f32[32,128]{1,0:T(8,128)S(1)}, f32[32,2,32]{2,1,0:T(2,128)S(1)}, bf16[80,4096]{1,0:T(8,128)(2,1)S(1)}, f32[32,32,...) custom-call(bf16[32,4096]{1,0:T(8,128)(2,1)S(1)} %get-tuple-element., ...), custom_call_target="tpu_custom_call" | custom-call | tf_op jit(solution)/shard_map/values/pallas_call | solution.py:50
  22.1 12.1 %all-to-all-done = bf16[256,4,128]{2,1,0:T(4,128)(2,1)S(1)} async-done(((bf16[256,4,128]{2,1,0:T(4,128)(2,1)}), bf16[256,4,128]{2,1,0:T(4,128)(2,1)S(1)}, u32[]{:S(2)}, u32[]{:S(2)}) %all-to-all-start) | async-done | bytes 262176 | tf_op jit(solution)/shard_map/all_to_all | solution.py:428
  34.2 1.1 mix0.1
  35.3 13.3 %all_to_all.35.got = bf16[32,40,128]{2,1,0:T(8,128)(2,1)S(1)} all-to-all(bf16[32,40,128]{2,1,0:T(8,128)(2,1)S(1)} %get-tuple-element.42), channel_id=1, replica_groups=mesh['z'=8,'y'=4,'x'=4,'c'=2] {'y','x','c'}, dimensions={0} | all-to-all | bytes 655360 | tf_op jit(solution)/shard_map/all_to_all | solution.py:428
  48.7 0.1 scale.2
  48.8 9.5 %all_to_all.36.got = bf16[8,32,128]{2,1,0:T(8,128)(2,1)S(1)} all-to-all(bf16[8,32,128]{2,1,0:T(8,128)(2,1)S(1)} %scale.2), channel_id=1, replica_groups=mesh['z'=8,'y'=4,'x'=4,'c'=2] {'z'}, dimensions={0} | all-to-all | bytes 131072 | tf_op jit(solution)/shard_map/all_to_all | solution.py:428
  58.3 0.2 add0.1
  58.5 12.7 %all_to_all.37.own.hid = bf16[16,96,128]{2,1,0:T(8,128)(2,1)S(1)} all-to-all(bf16[16,96,128]{2,1,0:T(8,128)(2,1)S(1)} %add0.1), channel_id=1, replica_groups=mesh['z'=8,'y'=4,'x'=4,'c'=2] {'y','x'}, dimensions={0} | all-to-all | bytes 786432 | tf_op jit(solution)/shard_map/all_to_all | solution.py:428
  71.2 2.0 %collective-permute-start = (bf16[16,96,128]{2,1,0:T(8,128)(2,1)S(1)}, bf16[16,96,128]{2,1,0:T(8,128)(2,1)S(1)}, u32[]{:S(2)}, u32[]{:S(2)}) collective-permute-start(bf16[16,96,128]{2,1,0:T(8,128)(2,1)S(1)} %all_to_all.37.own.hid), channel_id=1, source_target_pairs={{0,1},{1,0},{2,3},{3,2},{4,5},{5,4},{6,7},{7,6},{8,9},{9,8},{10,11... | collective-permute-start | bytes 1179656 | tf_op jit(solution)/shard_map/ppermute | solution.py:469
  73.1 1.3 %collective-permute-done.other = bf16[16,96,128]{2,1,0:T(8,128)(2,1)S(1)} collective-permute-done((bf16[16,96,128]{2,1,0:T(8,128)(2,1)S(1)}, bf16[16,96,128]{2,1,0:T(8,128)(2,1)S(1)}, u32[]{:S(2)}, u32[]{:S(2)}) %collective-permute-start) | collective-permute-done | bytes 393248 | tf_op jit(solution)/shard_map/ppermute | solution.py:469
  74.5 2.4 %mix1.1 = (f32[2,32,32,128]{3,2,1,0:T(8,128)}, bf16[32,40,128]{2,1,0:T(8,128)(2,1)S(1)}, f32[2,2,2,4,32]{4,3,2,1,0:T(4,128)}, f32[2,32,2,32]{3,2,1,0:T(2,128)}) custom-call(bf16[16,96,128]{2,1,0:T(8,128)(2,1)S(1)} %all_to_all.37.own.hid, bf16[16,96,128]{2,1,0:T(8,128)(2,1)S(1)} %collective-permute-done.other, ...), custom_call_target="tpu_custom_call", output_to_operand_aliasing={{0}: (17, {})} | custom-call | tf_op jit(solution)/shard_map/mix1/pallas_call | solution.py:50
  76.9 12.8 %all_to_all.38.got = bf16[32,40,128]{2,1,0:T(8,128)(2,1)S(1)} all-to-all(bf16[32,40,128]{2,1,0:T(8,128)(2,1)S(1)} %get-tuple-element.60), channel_id=1, replica_groups=mesh['z'=8,'y'=4,'x'=4,'c'=2] {'y','x','c'}, dimensions={0} | all-to-all | bytes 655360 | tf_op jit(solution)/shard_map/all_to_all | solution.py:428
  89.8 0.1 scale.3
  89.9 9.5 %all_to_all.39.got = bf16[8,32,128]{2,1,0:T(8,128)(2,1)S(1)} all-to-all(bf16[8,32,128]{2,1,0:T(8,128)(2,1)S(1)} %scale.3), channel_id=1, replica_groups=mesh['z'=8,'y'=4,'x'=4,'c'=2] {'z'}, dimensions={0} | all-to-all | bytes 131072 | tf_op jit(solution)/shard_map/all_to_all | solution.py:428
  99.4 13.7 %all_to_all.40 = bf16[32,32,128]{2,1,0:T(8,128)(2,1)S(1)} all-to-all(bf16[32,32,128]{2,1,0:T(8,128)(2,1)S(1)} %add1.1), channel_id=1, replica_groups=mesh['z'=8,'y'=4,'x'=4,'c'=2] {'y','x','c'}, dimensions={0} | all-to-all | bytes 524288 | tf_op jit(solution)/shard_map/all_to_all | solution.py:428
  113.1 0.7 copy_bitcast_fusion
  (1 shorter events, 0.0 us)
Async XLA Ops:
  2.9 31.4 %all-to-all-start = ((bf16[256,4,128]{2,1,0:T(4,128)(2,1)}), bf16[256,4,128]{2,1,0:T(4,128)(2,1)S(1)}, u32[]{:S(2)}, u32[]{:S(2)}) async-start(bf16[256,4,128]{2,1,0:T(4,128)(2,1)} %get-tuple-element.34), calls=%async_computation | async-start | bytes 524288 | tf_op jit(solution)/shard_map/all_to_all | solution.py:428
  71.2 3.3 %collective-permute-start = (bf16[16,96,128]{2,1,0:T(8,128)(2,1)S(1)}, bf16[16,96,128]{2,1,0:T(8,128)(2,1)S(1)}, u32[]{:S(2)}, u32[]{:S(2)}) collective-permute-start(bf16[16,96,128]{2,1,0:T(8,128)(2,1)S(1)} %all_to_all.37.own.hid), channel_id=1, source_target_pairs={{0,1},{1,0},{2,3},{3,2},{4,5},{5,4},{6,7},{7,6},{8,9},{9,8},{10,11... | collective-permute-start | bytes 1179656 | tf_op jit(solution)/shard_map/ppermute | solution.py:469

commit v5 on v4

--- a/solution.py
+++ b/solution.py
@@ -13,6 +13,7 @@
 CH = 32
 N = 128
 GW = 1024
+LINES = B + 2
 EPS = 1e-06
 TP = ("z", "y", "x", "c")
 PLANE = ("y", "x", "c")
@@ -284,13 +285,12 @@
     gated = (found.T + direct) * gate
     total = as_row(jnp.sum(gated * gated, axis=1, keepdims=True))
     high, low = hi_lo(total)
-    row = lax.broadcasted_iota(jnp.int32, (8, B), 0)
-    tail = jnp.where(row == 0, high, jnp.where(row == 1, low, 0.0))
-    tail = jnp.concatenate([tail, jnp.zeros((8, 128 - B), F32)], axis=1).astype(BF16)
+    tail = jnp.where(lax.broadcasted_iota(jnp.int32, (2, B), 0) == 0, high, low)
+    tail = jnp.concatenate([tail, jnp.zeros((2, 128 - B), F32)], axis=1).astype(BF16)
     out = jnp.dot((gated * gain).astype(BF16), w_out[...], preferred_element_type=F32)
     for j in range(D // 128):
-        sent[j, :B] = out[:, 128 * j : 128 * j + 128].astype(BF16)
-        sent[j, B:] = tail
+        sent[LINES * j : LINES * j + B] = out[:, 128 * j : 128 * j + 128].astype(BF16)
+        sent[LINES * j + B : LINES * (j + 1)] = tail
     for copy in copies:
         copy.wait()
 
@@ -303,7 +303,7 @@
     return [pltpu.VMEM(*p) for p in ADVANCE] + [pltpu.SemaphoreType.DMA((4,))]
 
 
-PLANE_SUMS = ((32, B + 8, 128), BF16)
+PLANE_SUMS = ((32 * LINES, 128), BF16)
 
 
 def first_mix_kernel(keys, packed, decay, state, w_out, gain, states, sent, weights, later, last_taps, lines, *scratch):
@@ -387,12 +387,14 @@
 
 
 def scale_kernel(got, sent):
-    total = got[0].astype(F32)
+    total = got[:B].astype(F32)
+    squares = got[B:LINES].astype(F32)
     for j in range(1, 32):
-        total += got[j].astype(F32)
-    squares = total[B : B + 1, :B] + total[B + 1 : B + 2, :B]
+        total += got[LINES * j : LINES * j + B].astype(F32)
+        squares += got[LINES * j + B : LINES * (j + 1)].astype(F32)
+    squares = squares[:1, :B] + squares[1:, :B]
     factor = as_col(lax.rsqrt(squares / GW + EPS))
-    chunk = (total[:B] * factor).astype(BF16)
+    chunk = (total * factor).astype(BF16)
     for plane in range(8):
         sent[plane] = chunk
 
@@ -457,7 +459,7 @@
     packed, decay, value_out, stack, *kept = make_values(scaled, inv, far)
     state, out, gain, next_state, next_out, *rest = kept
     states, sent, weights, later, last_taps = first_mix(keys, packed, decay, [state, out, gain])
-    sent = make_scale(exchange(sent, PLANE))
+    sent = make_scale(exchange(sent.reshape(32, LINES // 2, 2, 128), PLANE).reshape(sent.shape))
     (sent,) = call(
         first_add_kernel,
         "add0",
@@ -470,7 +472,7 @@
     states, sent, key_out, value_out = next_mix(
         own, other, stack, later, last_taps, [next_state, next_out, gain, *rest], key_out, value_out, states
     )
-    sent = make_scale(exchange(sent, PLANE))
+    sent = make_scale(exchange(sent.reshape(32, LINES // 2, 2, 128), PLANE).reshape(sent.shape))
     (sent,) = call(next_add_kernel, "add1", [exchange(sent, ("z",)), own], [], [pltpu.VMEM((32, B, 128), BF16)])
     hid = exchange(sent, PLANE)
     tokens_out = jnp.transpose(hid, (1, 0, 2)).reshape(B, D)

time: 114 us -> 113 us (level)
  blocking collectives: 71.6 us -> 69.8 us
    all_to_all x6, blocking collectives: 71.6 us -> 69.8 us  [exchange(): return lax.all_to_all(value, axes, split_axis=0, concat_axis=0, tiled=True)]
where the time goes in v5:
time: 113 us; the launch traced here: 112 us
  blocking collectives  69.8 us (62%)
  starting transfers between devices  18 us (16%)
  waiting for transfers between devices  13.5 us (12%)
  Pallas kernels  9.73 us (9%)
    all_to_all x6, blocking collectives, exchange(): return lax.all_to_all(value, axes, split_axis=0, concat_axis=0, tiled=True)  69.8 us
    all_to_all x1, starting transfers between devices, exchange(): return lax.all_to_all(value, axes, split_axis=0, concat_axis=0, tiled=True)  15.7 us
    all_to_all x1, waiting for transfers between devices, exchange(): return lax.all_to_all(value, axes, split_axis=0, concat_axis=0, tiled=True)  12.1 us
    pallas_call x8, Pallas kernels, call(): pl.pallas_call(body, in_specs=[vmem()] * len(near) + [anywhere()] * len(f...  9.73 us
    ppermute x1, starting transfers between devices, per_device(): other = lax.ppermute(own, 'c', [(0, 1), (1, 0)])  2.38 us
  transfers between devices with their start and end apart: 2, of which 2 were waited for; matrix products, arithmetic and copies ran while one was open for 0% of the time, Pallas kernels for 3%

profile of v5, /device:TPU:1, one launch (start us, length us, event | category | flops | bytes accessed | tf_op | source)
XLA Modules:
  0.0 112.4 jit_solution(15429628552865174438)
XLA Ops:
  0.6 2.2 %keys.1 = (bf16[256,4,128]{2,1,0:T(4,128)(2,1)}, f32[2,2,4,32]{3,2,1,0:T(4,128)S(1)}, bf16[32,4096]{1,0:T(8,128)(2,1)S(1)}, f32[32,128]{1,0:T(8,128)S(1)}, bf16[32,4096]{1,0:T(8,128)(2,1)S(1)}) custom-call(bf16[32,4096]{1,0:T(8,128)(2,1)} %tokens.1, f32[2,4096]{1,0:T(2,128)} %refs_8_.1, bf16[2,4,4096]{2,1,0:T(4,128)(2,1)} %bitcast.25, ...), custom_call_target="tpu_custom_call" | custom-call | tf_op jit(solution)/shard_map/keys/pallas_call | solution.py:51
  2.9 15.7 %all-to-all-start = ((bf16[256,4,128]{2,1,0:T(4,128)(2,1)}), bf16[256,4,128]{2,1,0:T(4,128)(2,1)S(1)}, u32[]{:S(2)}, u32[]{:S(2)}) async-start(bf16[256,4,128]{2,1,0:T(4,128)(2,1)} %get-tuple-element.34), calls=%async_computation | async-start | bytes 524288 | tf_op jit(solution)/shard_map/all_to_all | solution.py:430
  18.5 3.6 %values.1 = (f32[3,32,32]{2,1,0:T(8,128)S(1)}, f32[32,128]{1,0:T(8,128)S(1)}, f32[32,2,32]{2,1,0:T(2,128)S(1)}, bf16[80,4096]{1,0:T(8,128)(2,1)S(1)}, f32[32,32,...) custom-call(bf16[32,4096]{1,0:T(8,128)(2,1)S(1)} %get-tuple-element., ...), custom_call_target="tpu_custom_call" | custom-call | tf_op jit(solution)/shard_map/values/pallas_call | solution.py:51
  22.1 12.1 %all-to-all-done = bf16[256,4,128]{2,1,0:T(4,128)(2,1)S(1)} async-done(((bf16[256,4,128]{2,1,0:T(4,128)(2,1)}), bf16[256,4,128]{2,1,0:T(4,128)(2,1)S(1)}, u32[]{:S(2)}, u32[]{:S(2)}) %all-to-all-start) | async-done | bytes 262176 | tf_op jit(solution)/shard_map/all_to_all | solution.py:430
  34.2 1.1 mix0.1
  35.3 12.9 %all_to_all.35 = bf16[32,17,2,128]{3,2,1,0:T(2,128)(2,1)S(1)} all-to-all(bf16[32,17,2,128]{3,2,1,0:T(2,128)(2,1)S(1)} %bitcast.22), channel_id=1, replica_groups=mesh['z'=8,'y'=4,'x'=4,'c'=2] {'y','x','c'}, dimensions={0} | all-to-all | bytes 557056 | tf_op jit(solution)/shard_map/all_to_all | solution.py:430
  48.2 0.1 scale.2
  48.3 9.5 %all_to_all.36.got = bf16[8,32,128]{2,1,0:T(8,128)(2,1)S(1)} all-to-all(bf16[8,32,128]{2,1,0:T(8,128)(2,1)S(1)} %scale.2), channel_id=1, replica_groups=mesh['z'=8,'y'=4,'x'=4,'c'=2] {'z'}, dimensions={0} | all-to-all | bytes 131072 | tf_op jit(solution)/shard_map/all_to_all | solution.py:430
  57.8 0.2 add0.1
  58.0 11.9 %all_to_all.37.own.hid = bf16[16,96,128]{2,1,0:T(8,128)(2,1)S(1)} all-to-all(bf16[16,96,128]{2,1,0:T(8,128)(2,1)S(1)} %add0.1), channel_id=1, replica_groups=mesh['z'=8,'y'=4,'x'=4,'c'=2] {'y','x'}, dimensions={0} | all-to-all | bytes 786432 | tf_op jit(solution)/shard_map/all_to_all | solution.py:430
  69.9 2.4 %collective-permute-start = (bf16[16,96,128]{2,1,0:T(8,128)(2,1)S(1)}, bf16[16,96,128]{2,1,0:T(8,128)(2,1)S(1)}, u32[]{:S(2)}, u32[]{:S(2)}) collective-permute-start(bf16[16,96,128]{2,1,0:T(8,128)(2,1)S(1)} %all_to_all.37.own.hid), channel_id=1, source_target_pairs={{0,1},{1,0},{2,3},{3,2},{4,5},{5,4},{6,7},{7,6},{8,9},{9,8},{10,11... | collective-permute-start | bytes 1179656 | tf_op jit(solution)/shard_map/ppermute | solution.py:471
  72.2 1.3 %collective-permute-done.other = bf16[16,96,128]{2,1,0:T(8,128)(2,1)S(1)} collective-permute-done((bf16[16,96,128]{2,1,0:T(8,128)(2,1)S(1)}, bf16[16,96,128]{2,1,0:T(8,128)(2,1)S(1)}, u32[]{:S(2)}, u32[]{:S(2)}) %collective-permute-start) | collective-permute-done | bytes 393248 | tf_op jit(solution)/shard_map/ppermute | solution.py:471
  73.6 2.4 %mix1.1 = (f32[2,32,32,128]{3,2,1,0:T(8,128)}, bf16[1088,128]{1,0:T(8,128)(2,1)S(1)}, f32[2,2,2,4,32]{4,3,2,1,0:T(4,128)}, f32[2,32,2,32]{3,2,1,0:T(2,128)}) custom-call(bf16[16,96,128]{2,1,0:T(8,128)(2,1)S(1)} %all_to_all.37.own.hid, bf16[16,96,128]{2,1,0:T(8,128)(2,1)S(1)} %collective-permute-done.other, ...), custom_call_target="tpu_custom_call", output_to_operand_aliasing={{0}: (17, {})} | custom-call | tf_op jit(solution)/shard_map/mix1/pallas_call | solution.py:51
  76.0 12.4 %all_to_all.38 = bf16[32,17,2,128]{3,2,1,0:T(2,128)(2,1)S(1)} all-to-all(bf16[32,17,2,128]{3,2,1,0:T(2,128)(2,1)S(1)} %bitcast.21), channel_id=1, replica_groups=mesh['z'=8,'y'=4,'x'=4,'c'=2] {'y','x','c'}, dimensions={0} | all-to-all | bytes 557056 | tf_op jit(solution)/shard_map/all_to_all | solution.py:430
  88.4 0.1 scale.3
  88.5 9.5 %all_to_all.39.got = bf16[8,32,128]{2,1,0:T(8,128)(2,1)S(1)} all-to-all(bf16[8,32,128]{2,1,0:T(8,128)(2,1)S(1)} %scale.3), channel_id=1, replica_groups=mesh['z'=8,'y'=4,'x'=4,'c'=2] {'z'}, dimensions={0} | all-to-all | bytes 131072 | tf_op jit(solution)/shard_map/all_to_all | solution.py:430
  98.0 13.7 %all_to_all.40 = bf16[32,32,128]{2,1,0:T(8,128)(2,1)S(1)} all-to-all(bf16[32,32,128]{2,1,0:T(8,128)(2,1)S(1)} %add1.1), channel_id=1, replica_groups=mesh['z'=8,'y'=4,'x'=4,'c'=2] {'y','x','c'}, dimensions={0} | all-to-all | bytes 524288 | tf_op jit(solution)/shard_map/all_to_all | solution.py:430
  111.7 0.7 copy_bitcast_fusion
  (1 shorter events, 0.0 us)
Async XLA Ops:
  2.9 31.4 %all-to-all-start = ((bf16[256,4,128]{2,1,0:T(4,128)(2,1)}), bf16[256,4,128]{2,1,0:T(4,128)(2,1)S(1)}, u32[]{:S(2)}, u32[]{:S(2)}) async-start(bf16[256,4,128]{2,1,0:T(4,128)(2,1)} %get-tuple-element.34), calls=%async_computation | async-start | bytes 524288 | tf_op jit(solution)/shard_map/all_to_all | solution.py:430
  69.9 3.7 %collective-permute-start = (bf16[16,96,128]{2,1,0:T(8,128)(2,1)S(1)}, bf16[16,96,128]{2,1,0:T(8,128)(2,1)S(1)}, u32[]{:S(2)}, u32[]{:S(2)}) collective-permute-start(bf16[16,96,128]{2,1,0:T(8,128)(2,1)S(1)} %all_to_all.37.own.hid), channel_id=1, source_target_pairs={{0,1},{1,0},{2,3},{3,2},{4,5},{5,4},{6,7},{7,6},{8,9},{9,8},{10,11... | collective-permute-start | bytes 1179656 | tf_op jit(solution)/shard_map/ppermute | solution.py:471

commit v6 on v5

--- a/solution.py
+++ b/solution.py
@@ -98,72 +98,79 @@
 
 
 KEY_WEIGHTS = ((4, D), BF16)
-
-
-def keys_kernel(tokens, gain_far, write_far, read_far, conv_far, taps_far, msg, conv_out, scaled, inv_out, hid, *rest):
-    gain, w_write, w_read, next_write, next_read, conv, taps, sems = rest
-    pairs = [
-        (tokens, hid),
-        (gain_far, gain),
-        (write_far.at[0], w_write),
-        (read_far.at[0], w_read),
-        (write_far.at[1], next_write),
-        (read_far.at[1], next_read),
-        (conv_far, conv),
-        (taps_far, taps),
-    ]
-    for copy in start_all(pairs, sems):
+KEY_PARAMS = (((2, 4, D), BF16), ((2, 4, D), BF16), ((2, 2, 2, 4, B), F32), ((2, 3, 2, 4), F32))
+
+
+def start_kernel(tokens, gain_far, *refs):
+    far, (scaled, inv_out, hid), near, (gain, sems, late_sems) = refs[:4], refs[4:7], refs[7:11], refs[11:]
+    copies = start_all([(tokens, hid), (gain_far, gain)], sems)
+    late = start_all(list(zip(far, near)), late_sems)
+    for copy in copies:
         copy.wait()
     inv = scale_tokens(lambda j: hid[:, 128 * j : 128 * j + 128], gain.at[:1], scaled)
     inv_out[...] = jnp.broadcast_to(inv, (B, 128))
-    inv_row = as_row(inv)
-    mixed, later, last_taps = [], [], []
-    for kind, weight in ((0, w_write), (1, w_read)):
-        fresh = dot_nt(weight[...], scaled[...]) * inv_row
-        old, newer = conv[0, 0, kind], conv[0, 1, kind]
-        tap = [[as_col(taps[layer, k, kind : kind + 1, :]) for k in range(3)] for layer in range(2)]
-        mixed.append(silu(old * tap[0][0] + newer * tap[0][1] + fresh * tap[0][2]))
-        later.append(conv[1, 0, kind] * tap[1][0] + conv[1, 1, kind] * tap[1][1])
-        last_taps.append(tap[1][2])
-        conv_out[0, kind] = newer
-        conv_out[1, kind] = fresh
-    mixed_hi, mixed_lo = zip(*(hi_lo(v) for v in mixed))
-    taps_hi, taps_lo = zip(*(hi_lo(v) for v in last_taps))
-    first = jnp.concatenate([*mixed_hi, *later], axis=1)
+    for copy in late:
+        copy.wait()
+
+
+def make_start(tokens, gain, far):
+    outs = [((B, D), BF16), ((B, 128), F32), ((B, D), BF16), *KEY_PARAMS]
+    return call(
+        start_kernel,
+        "start",
+        [],
+        [tokens, gain, *far],
+        [pltpu.VMEM(*p) for p in outs],
+        [pltpu.VMEM((2, D), F32), pltpu.SemaphoreType.DMA((2,)), pltpu.SemaphoreType.DMA((4,))],
+    )
+
+
+def keys_kernel(scaled, inv, *refs):
+    sides, (msg, conv_out) = (refs[:4], refs[4:8]), refs[8:]
+    core = lax.axis_index("c")
+    rows = [weight[0].astype(F32) for side in sides for weight in side[:2]]
+    found = dot_nt(jnp.concatenate(rows, axis=0).astype(BF16), scaled[...]) * as_row(inv[:, :1])
     lane = lax.broadcasted_iota(jnp.int32, (4, B), 1)
-    tail = jnp.zeros((4, B), F32)
-    for at, col in enumerate((taps_hi[0], taps_lo[0], taps_hi[1], taps_lo[1])):
-        tail = jnp.where(lane == at, col, tail)
-    second = jnp.concatenate([*mixed_lo, tail, jnp.zeros((4, B), F32)], axis=1)
     row = lax.broadcasted_iota(jnp.int32, (4, 128), 0)
-    for col in range(4):
-        one = slice(col, col + 1)
-        base = jnp.where(row == 2, first[one], second[one])
-        for place in range(32):
-            cols = slice(128 * place, 128 * place + 128)
-            write = next_write[:, cols].astype(F32)[one]
-            read = next_read[:, cols].astype(F32)[one]
-            tile = jnp.where(row == 0, write, jnp.where(row == 1, read, base)).astype(BF16)
-            at = 128 * (place % 2) + 16 * col + place // 2
-            msg[at] = tile
-            msg[at + 64] = tile
-
-
-def make_keys(tokens, far):
-    scratch = [((2, D), F32)] + [KEY_WEIGHTS] * 4 + [((2, 2, 2, 4, B), F32), ((2, 3, 2, 4), F32)]
+    for of, (w_write, w_read, conv, taps) in enumerate(sides):
+        mixed, later, last_taps = [], [], []
+        for kind in range(2):
+            at = 8 * of + 4 * kind
+            fresh = found[at : at + 4]
+            old, newer = conv[0, 0, kind], conv[0, 1, kind]
+            tap = [[as_col(taps[layer, k, kind : kind + 1, :]) for k in range(3)] for layer in range(2)]
+            mixed.append(silu(old * tap[0][0] + newer * tap[0][1] + fresh * tap[0][2]))
+            later.append(conv[1, 0, kind] * tap[1][0] + conv[1, 1, kind] * tap[1][1])
+            last_taps.append(tap[1][2])
+            if not of:
+                conv_out[0, kind] = newer
+                conv_out[1, kind] = fresh
+        mixed_hi, mixed_lo = zip(*(hi_lo(v) for v in mixed))
+        taps_hi, taps_lo = zip(*(hi_lo(v) for v in last_taps))
+        first = jnp.concatenate([*mixed_hi, *later], axis=1)
+        tail = jnp.zeros((4, B), F32)
+        for at, col in enumerate((taps_hi[0], taps_lo[0], taps_hi[1], taps_lo[1])):
+            tail = jnp.where(lane == at, col, tail)
+        second = jnp.concatenate([*mixed_lo, tail, jnp.zeros((4, B), F32)], axis=1)
+        base = [jnp.where(row == 2, first[col : col + 1], second[col : col + 1]) for col in range(4)]
+        start = 64 * (1 - core if of else core)
+        for place in range(16):
+            cols = pl.ds(pl.multiple_of(128 * (2 * place + core), 128), 128)
+            writes = w_write[1, :, cols].astype(F32)
+            reads = w_read[1, :, cols].astype(F32)
+            for col in range(4):
+                one = slice(col, col + 1)
+                tile = jnp.where(row == 0, writes[one], jnp.where(row == 1, reads[one], base[col]))
+                msg[start + 16 * col + place] = tile.astype(BF16)
+
+
+def make_keys(scaled, inv, own, other):
     return call(
         keys_kernel,
         "keys",
+        [scaled, inv, *own, *other],
         [],
-        [tokens, *far],
-        [
-            shaped((256, 4, 128), BF16),
-            pltpu.VMEM((2, 2, 4, B), F32),
-            pltpu.VMEM((B, D), BF16),
-            pltpu.VMEM((B, 128), F32),
-            pltpu.VMEM((B, D), BF16),
-        ],
-        [pltpu.VMEM(*p) for p in scratch] + [pltpu.SemaphoreType.DMA((8,))],
+        [shaped((128, 4, 128), BF16), pltpu.VMEM((2, 2, 4, B), F32)],
     )
 
 
@@ -307,7 +314,7 @@
 
 
 def first_mix_kernel(keys, packed, decay, state, w_out, gain, states, sent, weights, later, last_taps, lines, *scratch):
-    lines[...] = keys[lax.axis_index("z") // 4].astype(F32)
+    lines[...] = keys[...].astype(F32)
     weights[0] = lines[pl.ds(0, N, stride=4), :].astype(BF16)
     weights[1] = lines[pl.ds(1, N, stride=4), :].astype(BF16)
     first = lines[pl.ds(2, N, stride=4), :].T
@@ -428,6 +435,10 @@
 
 def exchange(value, axes):
     return lax.all_to_all(value, axes, split_axis=0, concat_axis=0, tiled=True)
+
+
+def swap(value):
+    return lax.ppermute(value, "c", [(0, 1), (1, 0)])
 
 
 def per_device(
@@ -454,8 +465,11 @@
     value_taps = jnp.swapaxes(conv_value_weight, 0, 1)
     far = [w_gate, w_value, w_step, w_write, w_read, ssm_state, w_out, group_gain, norm_gain]
     far += [step_bias, decay_rate, skip_gain, conv_value, value_taps, conv_key]
-    msg, key_out, scaled, inv, hid = make_keys(tokens, [norm_gain, w_write, w_read, conv_key, conv_key_weight])
-    keys = exchange(msg, ("c", "z", "y", "x")).reshape(2, 4 * N, 128)
+    key_far = [w_write, w_read, conv_key, conv_key_weight]
+    others = [swap(v) for v in key_far]
+    scaled, inv, hid, *own = make_start(tokens, norm_gain, key_far)
+    msg, key_out = make_keys(scaled, inv, own, others)
+    keys = exchange(msg, ("z", "y", "x")).reshape(4 * N, 128)
     packed, decay, value_out, stack, *kept = make_values(scaled, inv, far)
     state, out, gain, next_state, next_out, *rest = kept
     states, sent, weights, later, last_taps = first_mix(keys, packed, decay, [state, out, gain])
@@ -468,7 +482,7 @@
         [pltpu.VMEM((16, 3 * B, 128), BF16)],
     )
     own = exchange(sent, ("y", "x"))
-    other = lax.ppermute(own, "c", [(0, 1), (1, 0)])
+    other = swap(own)
     states, sent, key_out, value_out = next_mix(
         own, other, stack, later, last_taps, [next_state, next_out, gain, *rest], key_out, value_out, states
     )

time: 113 us -> 111 us (0.982)
  waiting for transfers between devices: 13.5 us -> 9 us
  starting transfers between devices: 18 us -> 20.3 us
    all_to_all x1, waiting for transfers between devices: 12.1 us -> 7.61 us  [exchange(): return lax.all_to_all(value, axes, split_axis=0, concat_axis=0, tiled=True)]
    ppermute x1 -> x5, starting transfers between devices: 2.38 us -> 6.52 us  [swap(): return lax.ppermute(value, 'c', [(0, 1), (1, 0)])]
    all_to_all x1, starting transfers between devices: 15.7 us -> 13.8 us  [exchange(): return lax.all_to_all(value, axes, split_axis=0, concat_axis=0, tiled=True)]
    pallas_call x8 -> x9, Pallas kernels: 9.73 us -> 9.8 us  [call(): pl.pallas_call(body, in_specs=[vmem()] * len(near) + [anywhere()] * len(f...]
  transfers between devices with their start and end apart: 2 -> 6, of which waited for: 2 -> 2; matrix products, arithmetic and copies ran while one was open for 0% -> 0% of each run, Pallas kernels for 3% -> 4%
where the time goes in v6:
time: 111 us
  blocking collectives  70.5 us (64%)
  starting transfers between devices  20.3 us (18%)
  Pallas kernels  9.8 us (9%)
  waiting for transfers between devices  9 us (8%)
    all_to_all x6, blocking collectives, exchange(): return lax.all_to_all(value, axes, split_axis=0, concat_axis=0, tiled=True)  70.5 us
    all_to_all x1, starting transfers between devices, exchange(): return lax.all_to_all(value, axes, split_axis=0, concat_axis=0, tiled=True)  13.8 us
    pallas_call x9, Pallas kernels, call(): pl.pallas_call(body, in_specs=[vmem()] * len(near) + [anywhere()] * len(f...  9.8 us
    all_to_all x1, waiting for transfers between devices, exchange(): return lax.all_to_all(value, axes, split_axis=0, concat_axis=0, tiled=True)  7.61 us
    ppermute x5, starting transfers between devices, swap(): return lax.ppermute(value, 'c', [(0, 1), (1, 0)])  6.52 us
  transfers between devices with their start and end apart: 6, of which 2 were waited for; matrix products, arithmetic and copies ran while one was open for 0% of the time, Pallas kernels for 4%

profile of v6, /device:TPU:1, one launch (start us, length us, event | category | flops | bytes accessed | tf_op | source)
XLA Modules:
  0.0 111.1 jit_solution(13816971338001871749)
XLA Ops:
  0.6 3.3 %collective-permute-start = (bf16[2,4,4096]{2,1,0:T(4,128)(2,1)}, bf16[2,4,4096]{2,1,0:T(4,128)(2,1)S(1)}, u32[]{:S(2)}, u32[]{:S(2)}) collective-permute-start(bf16[2,4,4096]{2,1,0:T(4,128)(2,1)} %bitcast.25), channel_id=1, source_target_pairs={{0,1},{1,0},{2,3},{3,2},{4,5},{5,4},{6,7},{7,6},{8,9},{9,8},{10,11... | collective-permute-start | bytes 196616 | tf_op jit(solution)/shard_map/ppermute | solution.py:441
  3.9 0.1 collective-permute-start.1
  4.0 0.4 collective-permute-start.2
  4.4 0.1 collective-permute-start.3
  4.5 1.2 %start.1 = (bf16[32,4096]{1,0:T(8,128)(2,1)S(1)}, f32[32,128]{1,0:T(8,128)S(1)}, bf16[32,4096]{1,0:T(8,128)(2,1)S(1)}, bf16[2,4,4096]{2,1,0:T(4,128)(2,1)S(1)}, ...) custom-call(bf16[32,4096]{1,0:T(8,128)(2,1)} %tokens.1, ...), custom_call_target="tpu_custom_call" | custom-call | tf_op jit(solution)/shard_map/start/pallas_call | solution.py:51
  5.8 0.0 collective-permute-done.3.refs_7_
  5.8 0.0 collective-permute-done.2.refs_6_
  5.8 0.0 collective-permute-done.refs_4_
  5.8 0.0 collective-permute-done.1.refs_5_
  5.8 1.0 keys.1
  6.9 13.8 %all-to-all-start = ((bf16[128,4,128]{2,1,0:T(4,128)(2,1)}), bf16[128,4,128]{2,1,0:T(4,128)(2,1)S(1)}, u32[]{:S(2)}, u32[]{:S(2)}) async-start(bf16[128,4,128]{2,1,0:T(4,128)(2,1)} %get-tuple-element.44), calls=%async_computation | async-start | bytes 262144 | tf_op jit(solution)/shard_map/all_to_all | solution.py:437
  20.7 3.6 %values.1 = (f32[3,32,32]{2,1,0:T(8,128)S(1)}, f32[32,128]{1,0:T(8,128)S(1)}, f32[32,2,32]{2,1,0:T(2,128)S(1)}, bf16[80,4096]{1,0:T(8,128)(2,1)S(1)}, f32[32,32,...) custom-call(bf16[32,4096]{1,0:T(8,128)(2,1)S(1)} %get-tuple-element., ...), custom_call_target="tpu_custom_call" | custom-call | tf_op jit(solution)/shard_map/values/pallas_call | solution.py:51
  24.2 7.6 %all-to-all-done = bf16[128,4,128]{2,1,0:T(4,128)(2,1)S(1)} async-done(((bf16[128,4,128]{2,1,0:T(4,128)(2,1)}), bf16[128,4,128]{2,1,0:T(4,128)(2,1)S(1)}, u32[]{:S(2)}, u32[]{:S(2)}) %all-to-all-start) | async-done | bytes 131104 | tf_op jit(solution)/shard_map/all_to_all | solution.py:437
  31.8 1.1 mix0.1
  32.9 13.9 %all_to_all.35 = bf16[32,17,2,128]{3,2,1,0:T(2,128)(2,1)S(1)} all-to-all(bf16[32,17,2,128]{3,2,1,0:T(2,128)(2,1)S(1)} %bitcast.22), channel_id=1, replica_groups=mesh['z'=8,'y'=4,'x'=4,'c'=2] {'y','x','c'}, dimensions={0} | all-to-all | bytes 557056 | tf_op jit(solution)/shard_map/all_to_all | solution.py:437
  46.9 0.1 scale.2
  47.0 9.5 %all_to_all.36.got = bf16[8,32,128]{2,1,0:T(8,128)(2,1)S(1)} all-to-all(bf16[8,32,128]{2,1,0:T(8,128)(2,1)S(1)} %scale.2), channel_id=1, replica_groups=mesh['z'=8,'y'=4,'x'=4,'c'=2] {'z'}, dimensions={0} | all-to-all | bytes 131072 | tf_op jit(solution)/shard_map/all_to_all | solution.py:437
  56.5 0.2 add0.1
  56.7 11.6 %all_to_all.37.own.hid = bf16[16,96,128]{2,1,0:T(8,128)(2,1)S(1)} all-to-all(bf16[16,96,128]{2,1,0:T(8,128)(2,1)S(1)} %add0.1), channel_id=1, replica_groups=mesh['z'=8,'y'=4,'x'=4,'c'=2] {'y','x'}, dimensions={0} | all-to-all | bytes 786432 | tf_op jit(solution)/shard_map/all_to_all | solution.py:437
  68.3 2.6 %collective-permute-start.4 = (bf16[16,96,128]{2,1,0:T(8,128)(2,1)S(1)}, bf16[16,96,128]{2,1,0:T(8,128)(2,1)S(1)}, u32[]{:S(2)}, u32[]{:S(2)}) collective-permute-start(bf16[16,96,128]{2,1,0:T(8,128)(2,1)S(1)} %all_to_all.37.own.hid), channel_id=1, source_target_pairs={{0,1},{1,0},{2,3},{3,2},{4,5},{5,4},{6,7},{7,6},{8,9},{9,8},{10,11... | collective-permute-start | bytes 1179656 | tf_op jit(solution)/shard_map/ppermute | solution.py:441
  70.9 1.3 %collective-permute-done.4.other = bf16[16,96,128]{2,1,0:T(8,128)(2,1)S(1)} collective-permute-done((bf16[16,96,128]{2,1,0:T(8,128)(2,1)S(1)}, bf16[16,96,128]{2,1,0:T(8,128)(2,1)S(1)}, u32[]{:S(2)}, u32[]{:S(2)}) %collective-permute-start.4) | collective-permute-done | bytes 393248 | tf_op jit(solution)/shard_map/ppermute | solution.py:441
  72.2 2.4 %mix1.1 = (f32[2,32,32,128]{3,2,1,0:T(8,128)}, bf16[1088,128]{1,0:T(8,128)(2,1)S(1)}, f32[2,2,2,4,32]{4,3,2,1,0:T(4,128)}, f32[2,32,2,32]{3,2,1,0:T(2,128)}) custom-call(bf16[16,96,128]{2,1,0:T(8,128)(2,1)S(1)} %all_to_all.37.own.hid, bf16[16,96,128]{2,1,0:T(8,128)(2,1)S(1)} %collective-permute-done.4.other, ...), custom_call_target="tpu_custom_call", output_to_operand_aliasing={{0}: (17, {})} | custom-call | tf_op jit(solution)/shard_map/mix1/pallas_call | solution.py:51
  74.6 12.4 %all_to_all.38 = bf16[32,17,2,128]{3,2,1,0:T(2,128)(2,1)S(1)} all-to-all(bf16[32,17,2,128]{3,2,1,0:T(2,128)(2,1)S(1)} %bitcast.21), channel_id=1, replica_groups=mesh['z'=8,'y'=4,'x'=4,'c'=2] {'y','x','c'}, dimensions={0} | all-to-all | bytes 557056 | tf_op jit(solution)/shard_map/all_to_all | solution.py:437
  87.0 0.1 scale.3
  87.1 9.5 %all_to_all.39.got = bf16[8,32,128]{2,1,0:T(8,128)(2,1)S(1)} all-to-all(bf16[8,32,128]{2,1,0:T(8,128)(2,1)S(1)} %scale.3), channel_id=1, replica_groups=mesh['z'=8,'y'=4,'x'=4,'c'=2] {'z'}, dimensions={0} | all-to-all | bytes 131072 | tf_op jit(solution)/shard_map/all_to_all | solution.py:437
  96.7 13.7 %all_to_all.40 = bf16[32,32,128]{2,1,0:T(8,128)(2,1)S(1)} all-to-all(bf16[32,32,128]{2,1,0:T(8,128)(2,1)S(1)} %add1.1), channel_id=1, replica_groups=mesh['z'=8,'y'=4,'x'=4,'c'=2] {'y','x','c'}, dimensions={0} | all-to-all | bytes 524288 | tf_op jit(solution)/shard_map/all_to_all | solution.py:437
  110.3 0.7 copy_bitcast_fusion
  (1 shorter events, 0.0 us)
Async XLA Ops:
  0.6 5.2 %collective-permute-start = (bf16[2,4,4096]{2,1,0:T(4,128)(2,1)}, bf16[2,4,4096]{2,1,0:T(4,128)(2,1)S(1)}, u32[]{:S(2)}, u32[]{:S(2)}) collective-permute-start(bf16[2,4,4096]{2,1,0:T(4,128)(2,1)} %bitcast.25), channel_id=1, source_target_pairs={{0,1},{1,0},{2,3},{3,2},{4,5},{5,4},{6,7},{7,6},{8,9},{9,8},{10,11... | collective-permute-start | bytes 196616 | tf_op jit(solution)/shard_map/ppermute | solution.py:441
  3.9 1.9 %collective-permute-start.1 = (bf16[2,4,4096]{2,1,0:T(4,128)(2,1)}, bf16[2,4,4096]{2,1,0:T(4,128)(2,1)S(1)}, u32[]{:S(2)}, u32[]{:S(2)}) collective-permute-start(bf16[2,4,4096]{2,1,0:T(4,128)(2,1)} %bitcast.28), channel_id=1, source_target_pairs={{0,1},{1,0},{2,3},{3,2},{4,5},{5,4},{6,7},{7,6},{8,9},{9,8},{10,11... | collective-permute-start | bytes 196616 | tf_op jit(solution)/shard_map/ppermute | solution.py:441
  4.0 1.8 %collective-permute-start.2 = (f32[2,2,2,4,32]{4,3,2,1,0:T(4,128)}, f32[2,2,2,4,32]{4,3,2,1,0:T(4,128)S(1)}, u32[]{:S(2)}, u32[]{:S(2)}) collective-permute-start(f32[2,2,2,4,32]{4,3,2,1,0:T(4,128)} %bitcast.31), channel_id=1, source_target_pairs={{0,1},{1,0},{2,3},{3,2},{4,5},{5,4},{6,7},{7,6},{8,9},{9,8},{10,11... | collective-permute-start | bytes 12296 | tf_op jit(solution)/shard_map/ppermute | solution.py:441
  4.4 1.4 %collective-permute-start.3 = (f32[2,3,2,4]{3,2,1,0:T(2,128)}, f32[2,3,2,4]{3,2,1,0:T(2,128)S(1)}, u32[]{:S(2)}, u32[]{:S(2)}) collective-permute-start(f32[2,3,2,4]{3,2,1,0:T(2,128)} %refs_3_.1), channel_id=1, source_target_pairs={{0,1},{1,0},{2,3},{3,2},{4,5},{5,4},{6,7},{7,6},{8,9},{9,8},{10,11... | collective-permute-start | bytes 584 | tf_op jit(solution)/shard_map/ppermute | solution.py:441
  6.9 25.0 %all-to-all-start = ((bf16[128,4,128]{2,1,0:T(4,128)(2,1)}), bf16[128,4,128]{2,1,0:T(4,128)(2,1)S(1)}, u32[]{:S(2)}, u32[]{:S(2)}) async-start(bf16[128,4,128]{2,1,0:T(4,128)(2,1)} %get-tuple-element.44), calls=%async_computation | async-start | bytes 262144 | tf_op jit(solution)/shard_map/all_to_all | solution.py:437
  68.3 4.0 %collective-permute-start.4 = (bf16[16,96,128]{2,1,0:T(8,128)(2,1)S(1)}, bf16[16,96,128]{2,1,0:T(8,128)(2,1)S(1)}, u32[]{:S(2)}, u32[]{:S(2)}) collective-permute-start(bf16[16,96,128]{2,1,0:T(8,128)(2,1)S(1)} %all_to_all.37.own.hid), channel_id=1, source_target_pairs={{0,1},{1,0},{2,3},{3,2},{4,5},{5,4},{6,7},{7,6},{8,9},{9,8},{10,11... | collective-permute-start | bytes 1179656 | tf_op jit(solution)/shard_map/ppermute | solution.py:441

commit v7 on v6

--- a/solution.py
+++ b/solution.py
@@ -180,15 +180,13 @@
     return jnp.sum(jnp.where(mine, table, 0.0), axis=1, keepdims=True)
 
 
-def gated_values(layer, gate, fresh, raw, tables, conv, taps):
-    bias, rate, skip = (t[layer : layer + 1, :] for t in tables)
-    old, newer = conv[:, 0, :], conv[:, 1, :]
-    tap = [taps[k, layer : layer + 1, :] for k in range(3)]
-    values = silu(old * tap[0] + newer * tap[1] + fresh * tap[2])
-    raw = raw + of_head(bias)
+def steps_of(raw, rate):
     delta = jnp.maximum(raw, 0.0) + jnp.log1p(jnp.exp(-jnp.abs(raw)))
-    decay = jnp.exp(-delta * of_head(rate))
-    return (delta * values).T, of_head(skip) * values, silu(gate), decay
+    return delta, jnp.exp(-delta * rate)
+
+
+def row_of(table, layer):
+    return table[layer : layer + 1, :]
 
 
 STATE = ((B, CH, N), F32)
@@ -214,8 +212,8 @@
 
 def values_kernel(scaled, inv, *refs):
     far, refs = refs[:15], refs[15:]
-    packed, decay_out, conv_out, stack, *kept = refs[: 4 + len(KEPT)]
-    w_gate, w_value, w_step, next_step, next_write, next_read, sems, late_sems = refs[4 + len(KEPT) :]
+    packed, decay_out, conv_out, halves, ready, *kept = refs[: 5 + len(KEPT)]
+    w_gate, w_value, w_step, next_step, next_write, next_read, stack, sems, late_sems = refs[5 + len(KEPT) :]
     gate_far, value_far, step_far, write_far, read_far, state_far, out_far, *tables_far = far
     tables_group, tables_rest = tables_far[0], tables_far[1:]
     late_sources = [
@@ -241,11 +239,13 @@
     gate = dot_nt(hidden, w_gate[...]) * inv_col
     fresh = dot_nt(hidden, w_value[...]) * inv_col
     raw = of_head(jnp.dot(hidden, w_step[...], preferred_element_type=F32) * inv[...])
-    tables, conv, taps = kept[6:9], kept[9], kept[10]
-    push, direct, gate, decay = gated_values(0, gate, fresh, raw, tables, conv.at[0], taps)
-    packed[0] = push
-    packed[1] = direct
-    packed[2] = gate
+    (bias, rate, skip), conv, taps = kept[6:9], kept[9], kept[10]
+    tap = [[row_of(taps[k], layer) for k in range(3)] for layer in range(2)]
+    values = silu(conv[0, :, 0, :] * tap[0][0] + conv[0, :, 1, :] * tap[0][1] + fresh * tap[0][2])
+    delta, decay = steps_of(raw + of_head(row_of(bias, 0)), of_head(row_of(rate, 0)))
+    packed[0] = (delta * values).T
+    packed[1] = (of_head(row_of(skip, 0)) * values).T
+    packed[2] = silu(gate).T
     decay_out[...] = jnp.broadcast_to(decay, (B, N))
     conv_out[:, 0, :] = conv[0, :, 1, :]
     conv_out[:, 1, :] = fresh
@@ -256,13 +256,23 @@
     stack[2 * CH : 2 * CH + 8] = dot_nt(hot, next_step[...]).astype(BF16)
     both = jnp.concatenate([next_write[...].astype(F32), next_read[...].astype(F32)], axis=0)
     stack[2 * CH + 8 :] = both.astype(BF16)
+    for place in range(16):
+        for side in range(2):
+            at = 128 * (2 * place + side)
+            halves[side, :, 128 * place : 128 * place + 128] = stack[:, at : at + 128]
+    packed[3] = jnp.broadcast_to(as_col(row_of(kept[2], 0)), (CH, B))
+    ready[0] = (conv[1, :, 0, :] * tap[1][0] + conv[1, :, 1, :] * tap[1][1]).T
+    ready[1] = jnp.broadcast_to(as_col(tap[1][2]), (CH, B))
+    ready[2] = jnp.broadcast_to(as_col(row_of(kept[2], 1)), (CH, B))
+    for at, table in enumerate((bias, rate, skip)):
+        ready[3, at : at + 1] = jnp.broadcast_to(of_head(row_of(table, 1)), (1, B))
 
 
 def make_values(scaled, inv, far):
-    outs = [pltpu.VMEM((3, B, CH), F32), pltpu.VMEM((B, N), F32)]
-    outs += [pltpu.VMEM((B, 2, CH), F32), pltpu.VMEM((ROWS, D), BF16)]
+    outs = [pltpu.VMEM((4, CH, B), F32), pltpu.VMEM((B, N), F32)]
+    outs += [pltpu.VMEM((B, 2, CH), F32), pltpu.VMEM((2, ROWS, D // 2), BF16), pltpu.VMEM((4, CH, B), F32)]
     outs += [pltpu.VMEM(*p) for p in KEPT]
-    scratch = [pltpu.VMEM(*p) for p in NOW_FAR + NEXT_FAR]
+    scratch = [pltpu.VMEM(*p) for p in (*NOW_FAR, *NEXT_FAR, ((ROWS, D), BF16))]
     scratch += [pltpu.SemaphoreType.DMA((8,)), pltpu.SemaphoreType.DMA((12,))]
     return call(values_kernel, "values", [scaled, inv], far, outs, scratch)
 
@@ -289,12 +299,12 @@
             part = pl.ds(b - 7, 8)
             copies.append(pltpu.make_async_copy(fresh.at[part], states.at[layer, part], sems.at[b // 8]))
             copies[-1].start()
-    gated = (found.T + direct) * gate
-    total = as_row(jnp.sum(gated * gated, axis=1, keepdims=True))
+    gated = (found + direct) * gate
+    total = jnp.sum(gated * gated, axis=0, keepdims=True)
     high, low = hi_lo(total)
     tail = jnp.where(lax.broadcasted_iota(jnp.int32, (2, B), 0) == 0, high, low)
     tail = jnp.concatenate([tail, jnp.zeros((2, 128 - B), F32)], axis=1).astype(BF16)
-    out = jnp.dot((gated * gain).astype(BF16), w_out[...], preferred_element_type=F32)
+    out = jnp.dot((gated * gain).T.astype(BF16), w_out[...], preferred_element_type=F32)
     for j in range(D // 128):
         sent[LINES * j : LINES * j + B] = out[:, 128 * j : 128 * j + 128].astype(BF16)
         sent[LINES * j + B : LINES * (j + 1)] = tail
@@ -313,7 +323,7 @@
 PLANE_SUMS = ((32 * LINES, 128), BF16)
 
 
-def first_mix_kernel(keys, packed, decay, state, w_out, gain, states, sent, weights, later, last_taps, lines, *scratch):
+def first_mix_kernel(keys, packed, decay, state, w_out, states, sent, weights, later, last_taps, lines, *scratch):
     lines[...] = keys[...].astype(F32)
     weights[0] = lines[pl.ds(0, N, stride=4), :].astype(BF16)
     weights[1] = lines[pl.ds(1, N, stride=4), :].astype(BF16)
@@ -326,7 +336,7 @@
     reads = first[B : 2 * B] + second[B : 2 * B]
     scratch[1][...] = decay[...]
     advance(
-        0, packed[0], packed[1], packed[2], writes, reads, state, w_out, gain[:1, :], sent, states, scratch
+        0, packed[0], packed[1], packed[2], writes, reads, state, w_out, packed[3], sent, states, scratch
     )
 
 
@@ -347,40 +357,65 @@
     )
 
 
-def next_mix_kernel(own, other, stack, later, last_taps, state, w_out, gain, norm_gain, *refs):
-    tables, conv, taps, key_conv, key_before, value_before = refs[:3], refs[3], refs[4], refs[5], refs[6], refs[7]
-    states, sent, key_out, value_out, hid, scaled, *scratch = refs[9:]
-    core = lax.axis_index("c")
-    sums = [jnp.zeros((B, N), F32), jnp.zeros((B, N), F32)]
+def take_half(half, side, norm_gain, weights, scaled, squares, sums):
     for at in range(16):
-        for whose, side in ((own, core), (other, 1 - core)):
-            hid[2 * at + side] = whose[at, :B]
-            for kind in range(2):
-                sums[kind] += whose[at, B * (kind + 1) : B * (kind + 2)].astype(F32)
-    inv = scale_tokens(lambda j: hid[j], norm_gain.at[1:], scaled)
-    found = dot_nt(scaled[...], stack[...]) * inv
+        cols = pl.ds(pl.multiple_of(128 * (2 * at + side), 128), 128)
+        part = half[at, :B].astype(F32)
+        squares += part * part
+        scaled[:, 128 * at : 128 * at + 128] = (part * norm_gain[1:, cols]).astype(BF16)
+        for kind in range(2):
+            sums[kind] += half[at, B * (kind + 1) : B * (kind + 2)].astype(F32)
+    return squares, sums, dot_nt(weights[side], scaled[...])
+
+
+def half_kernel(own, weights, norm_gain, found_out, squares_out, sums_out, scaled):
+    zero = jnp.zeros((B, N), F32)
+    squares, sums, found = take_half(own, lax.axis_index("c"), norm_gain, weights, scaled, zero, [zero, zero])
+    found_out[...] = found
+    squares_out[...] = squares
+    sums_out[0] = sums[0]
+    sums_out[1] = sums[1]
+
+
+HALF = ((B, D // 2), BF16)
+
+
+def make_half(own, weights, norm_gain):
+    outs = [pltpu.VMEM((ROWS, B), F32), pltpu.VMEM((B, N), F32), pltpu.VMEM((2, B, N), F32)]
+    return call(half_kernel, "half", [own, weights, norm_gain], [], outs, [pltpu.VMEM(*HALF)])
+
+
+def next_mix_kernel(other, weights, norm_gain, found, squares, sums, ready, later, last_taps, state, w_out, *refs):
+    conv, key_conv, key_before, value_before = refs[:4]
+    states, sent, key_out, value_out, scaled, *scratch = refs[5:]
+    squares, sums, rest = take_half(
+        other, 1 - lax.axis_index("c"), norm_gain, weights, scaled, squares[...], [sums[0], sums[1]]
+    )
+    inv = lax.rsqrt(jnp.sum(squares, axis=1, keepdims=True) / D + EPS)
+    found = (found[...] + rest) * as_row(inv)
     keys = [silu(later[k] + sums[k] * inv * (last_taps[2 * k : 2 * k + 1] + last_taps[2 * k + 1 : 2 * k + 2])) for k in range(2)]
-    fresh_values = found[:, CH : 2 * CH]
-    push, direct, gate, decay = gated_values(
-        1, found[:, :CH], fresh_values, found[:, 2 * CH : 2 * CH + 1], tables, conv.at[1], taps
-    )
-    scratch[1][...] = jnp.broadcast_to(decay, (B, N))
-    advance(1, push, direct, gate, keys[0], keys[1], state, w_out, gain[1:, :], sent, states, scratch)
+    fresh_values = found[CH : 2 * CH]
+    values = silu(ready[0] + fresh_values * ready[1])
+    delta, decay = steps_of(found[2 * CH : 2 * CH + 1] + ready[3, :1], ready[3, 1:2])
+    scratch[1][...] = jnp.broadcast_to(as_col(decay), (B, N))
+    direct = ready[3, 2:3] * values
+    advance(
+        1, delta * values, direct, silu(found[:CH]), keys[0], keys[1], state, w_out, ready[2], sent, states, scratch
+    )
     value_out[0] = value_before[...]
     value_out[1, :, 0, :] = conv[1, :, 1, :]
-    value_out[1, :, 1, :] = fresh_values
-    turned = found.T
+    value_out[1, :, 1, :] = fresh_values.T
     key_out[0] = key_before[...]
     for kind in range(2):
         key_out[1, 0, kind] = key_conv[1, 1, kind]
-        key_out[1, 1, kind] = turned[2 * CH + 8 + 4 * kind : 2 * CH + 12 + 4 * kind]
-
-
-def next_mix(own, other, stack, later, last_taps, kept, key_before, value_before, states):
+        key_out[1, 1, kind] = found[2 * CH + 8 + 4 * kind : 2 * CH + 12 + 4 * kind]
+
+
+def next_mix(near, states):
     return call(
         next_mix_kernel,
         "mix1",
-        [own, other, stack, later, last_taps, *kept, key_before, value_before],
+        near,
         [states],
         [
             pltpu.HBM(*STATES),
@@ -388,8 +423,8 @@
             shaped((2, 2, 2, 4, B), F32),
             shaped((2, B, 2, CH), F32),
         ],
-        [pltpu.VMEM((32, B, 128), BF16), pltpu.VMEM((B, D), BF16)] + advance_scratch(),
-        {17: 0},
+        [pltpu.VMEM(*HALF)] + advance_scratch(),
+        {len(near): 0},
     )
 
 
@@ -470,9 +505,9 @@
     scaled, inv, hid, *own = make_start(tokens, norm_gain, key_far)
     msg, key_out = make_keys(scaled, inv, own, others)
     keys = exchange(msg, ("z", "y", "x")).reshape(4 * N, 128)
-    packed, decay, value_out, stack, *kept = make_values(scaled, inv, far)
+    packed, decay, value_out, halves, ready, *kept = make_values(scaled, inv, far)
     state, out, gain, next_state, next_out, *rest = kept
-    states, sent, weights, later, last_taps = first_mix(keys, packed, decay, [state, out, gain])
+    states, sent, weights, later, last_taps = first_mix(keys, packed, decay, [state, out])
     sent = make_scale(exchange(sent.reshape(32, LINES // 2, 2, 128), PLANE).reshape(sent.shape))
     (sent,) = call(
         first_add_kernel,
@@ -483,9 +518,10 @@
     )
     own = exchange(sent, ("y", "x"))
     other = swap(own)
-    states, sent, key_out, value_out = next_mix(
-        own, other, stack, later, last_taps, [next_state, next_out, gain, *rest], key_out, value_out, states
-    )
+    norm_far, conv, key_conv = rest[0], rest[4], rest[6]
+    half = make_half(own, halves, norm_far)
+    near = [other, halves, norm_far, *half, ready, later, last_taps, next_state, next_out]
+    states, sent, key_out, value_out = next_mix([*near, conv, key_conv, key_out, value_out], states)
     sent = make_scale(exchange(sent.reshape(32, LINES // 2, 2, 128), PLANE).reshape(sent.shape))
     (sent,) = call(next_add_kernel, "add1", [exchange(sent, ("z",)), own], [], [pltpu.VMEM((32, B, 128), BF16)])
     hid = exchange(sent, PLANE)

time: 111 us -> 111 us (level)
    pallas_call x9 -> x10, Pallas kernels: 9.8 us -> 10.1 us  [call(): pl.pallas_call(body, in_specs=[vmem()] * len(near) + [anywhere()] * len(f...]
  transfers between devices with their start and end apart: 6 -> 6, of which waited for: 2 -> 2; matrix products, arithmetic and copies ran while one was open for 0% -> 0% of each run, Pallas kernels for 4% -> 5%
where the time goes in v7:
time: 111 us
  blocking collectives  70.5 us (64%)
  starting transfers between devices  20.3 us (18%)
  Pallas kernels  10.1 us (9%)
  waiting for transfers between devices  8.39 us (8%)
    all_to_all x6, blocking collectives, exchange(): return lax.all_to_all(value, axes, split_axis=0, concat_axis=0, tiled=True)  70.5 us
    all_to_all x1, starting transfers between devices, exchange(): return lax.all_to_all(value, axes, split_axis=0, concat_axis=0, tiled=True)  13.8 us
    pallas_call x10, Pallas kernels, call(): pl.pallas_call(body, in_specs=[vmem()] * len(near) + [anywhere()] * len(f...  10.1 us
    all_to_all x1, waiting for transfers between devices, exchange(): return lax.all_to_all(value, axes, split_axis=0, concat_axis=0, tiled=True)  7.26 us
    ppermute x5, starting transfers between devices, swap(): return lax.ppermute(value, 'c', [(0, 1), (1, 0)])  6.52 us
  transfers between devices with their start and end apart: 6, of which 2 were waited for; matrix products, arithmetic and copies ran while one was open for 0% of the time, Pallas kernels for 5%

profile of v7, /device:TPU:1, one launch (start us, length us, event | category | flops | bytes accessed | tf_op | source)
XLA Modules:
  0.0 110.7 jit_solution(11721895097548511415)
XLA Ops:
  0.6 3.3 %collective-permute-start = (bf16[2,4,4096]{2,1,0:T(4,128)(2,1)}, bf16[2,4,4096]{2,1,0:T(4,128)(2,1)S(1)}, u32[]{:S(2)}, u32[]{:S(2)}) collective-permute-start(bf16[2,4,4096]{2,1,0:T(4,128)(2,1)} %bitcast.25), channel_id=1, source_target_pairs={{0,1},{1,0},{2,3},{3,2},{4,5},{5,4},{6,7},{7,6},{8,9},{9,8},{10,11... | collective-permute-start | bytes 196616 | tf_op jit(solution)/shard_map/ppermute | solution.py:476
  3.9 0.1 collective-permute-start.1
  4.0 0.4 collective-permute-start.2
  4.4 0.1 collective-permute-start.3
  4.5 1.2 %start.1 = (bf16[32,4096]{1,0:T(8,128)(2,1)S(1)}, f32[32,128]{1,0:T(8,128)S(1)}, bf16[32,4096]{1,0:T(8,128)(2,1)S(1)}, bf16[2,4,4096]{2,1,0:T(4,128)(2,1)S(1)}, ...) custom-call(bf16[32,4096]{1,0:T(8,128)(2,1)} %tokens.1, ...), custom_call_target="tpu_custom_call" | custom-call | tf_op jit(solution)/shard_map/start/pallas_call | solution.py:51
  5.8 0.0 collective-permute-done.3.refs_7_
  5.8 0.0 collective-permute-done.2.refs_6_
  5.8 0.0 collective-permute-done.refs_4_
  5.8 0.0 collective-permute-done.1.refs_5_
  5.8 1.0 keys.1
  6.9 13.8 %all-to-all-start = ((bf16[128,4,128]{2,1,0:T(4,128)(2,1)}), bf16[128,4,128]{2,1,0:T(4,128)(2,1)S(1)}, u32[]{:S(2)}, u32[]{:S(2)}) async-start(bf16[128,4,128]{2,1,0:T(4,128)(2,1)} %get-tuple-element.43), calls=%async_computation | async-start | bytes 262144 | tf_op jit(solution)/shard_map/all_to_all | solution.py:472
  20.7 3.9 %values.1 = (f32[4,32,32]{2,1,0:T(8,128)S(1)}, f32[32,128]{1,0:T(8,128)S(1)}, f32[32,2,32]{2,1,0:T(2,128)S(1)}, bf16[2,80,2048]{2,1,0:T(8,128)(2,1)S(1)}, f32[4,...) custom-call(bf16[32,4096]{1,0:T(8,128)(2,1)S(1)} %get-tuple-element., ...), custom_call_target="tpu_custom_call" | custom-call | tf_op jit(solution)/shard_map/values/pallas_call | solution.py:51
  24.6 7.3 %all-to-all-done = bf16[128,4,128]{2,1,0:T(4,128)(2,1)S(1)} async-done(((bf16[128,4,128]{2,1,0:T(4,128)(2,1)}), bf16[128,4,128]{2,1,0:T(4,128)(2,1)S(1)}, u32[]{:S(2)}, u32[]{:S(2)}) %all-to-all-start) | async-done | bytes 131104 | tf_op jit(solution)/shard_map/all_to_all | solution.py:472
  31.8 1.1 mix0.1
  32.9 13.9 %all_to_all.35 = bf16[32,17,2,128]{3,2,1,0:T(2,128)(2,1)S(1)} all-to-all(bf16[32,17,2,128]{3,2,1,0:T(2,128)(2,1)S(1)} %bitcast.22), channel_id=1, replica_groups=mesh['z'=8,'y'=4,'x'=4,'c'=2] {'y','x','c'}, dimensions={0} | all-to-all | bytes 557056 | tf_op jit(solution)/shard_map/all_to_all | solution.py:472
  46.9 0.1 scale.2
  47.0 9.5 %all_to_all.36.got = bf16[8,32,128]{2,1,0:T(8,128)(2,1)S(1)} all-to-all(bf16[8,32,128]{2,1,0:T(8,128)(2,1)S(1)} %scale.2), channel_id=1, replica_groups=mesh['z'=8,'y'=4,'x'=4,'c'=2] {'z'}, dimensions={0} | all-to-all | bytes 131072 | tf_op jit(solution)/shard_map/all_to_all | solution.py:472
  56.5 0.2 add0.1
  56.7 11.6 %all_to_all.37.own.hid = bf16[16,96,128]{2,1,0:T(8,128)(2,1)S(1)} all-to-all(bf16[16,96,128]{2,1,0:T(8,128)(2,1)S(1)} %add0.1), channel_id=1, replica_groups=mesh['z'=8,'y'=4,'x'=4,'c'=2] {'y','x'}, dimensions={0} | all-to-all | bytes 786432 | tf_op jit(solution)/shard_map/all_to_all | solution.py:472
  68.3 2.6 %collective-permute-start.4 = (bf16[16,96,128]{2,1,0:T(8,128)(2,1)S(1)}, bf16[16,96,128]{2,1,0:T(8,128)(2,1)S(1)}, u32[]{:S(2)}, u32[]{:S(2)}) collective-permute-start(bf16[16,96,128]{2,1,0:T(8,128)(2,1)S(1)} %all_to_all.37.own.hid), channel_id=1, source_target_pairs={{0,1},{1,0},{2,3},{3,2},{4,5},{5,4},{6,7},{7,6},{8,9},{9,8},{10,11... | collective-permute-start | bytes 1179656 | tf_op jit(solution)/shard_map/ppermute | solution.py:476
  70.9 0.2 half.1
  71.1 1.1 collective-permute-done.4.other
  72.2 2.1 %mix1.1 = (f32[2,32,32,128]{3,2,1,0:T(8,128)}, bf16[1088,128]{1,0:T(8,128)(2,1)S(1)}, f32[2,2,2,4,32]{4,3,2,1,0:T(4,128)}, f32[2,32,2,32]{3,2,1,0:T(2,128)}) custom-call(bf16[16,96,128]{2,1,0:T(8,128)(2,1)S(1)} %collective-permute-done.4.other, bf16[2,80,2048]{2,1,0:T(8,128)(2,1)S(1)} %get-tuple-element.52.weights, ...), custom_call_target="tpu_custom_call", output_to_operand_aliasing={{0}: (15, {})} | custom-call | tf_op jit(solution)/shard_map/mix1/pallas_call | solution.py:51
  74.3 12.4 %all_to_all.38 = bf16[32,17,2,128]{3,2,1,0:T(2,128)(2,1)S(1)} all-to-all(bf16[32,17,2,128]{3,2,1,0:T(2,128)(2,1)S(1)} %bitcast.21), channel_id=1, replica_groups=mesh['z'=8,'y'=4,'x'=4,'c'=2] {'y','x','c'}, dimensions={0} | all-to-all | bytes 557056 | tf_op jit(solution)/shard_map/all_to_all | solution.py:472
  86.7 0.1 scale.3
  86.8 9.5 %all_to_all.39.got = bf16[8,32,128]{2,1,0:T(8,128)(2,1)S(1)} all-to-all(bf16[8,32,128]{2,1,0:T(8,128)(2,1)S(1)} %scale.3), channel_id=1, replica_groups=mesh['z'=8,'y'=4,'x'=4,'c'=2] {'z'}, dimensions={0} | all-to-all | bytes 131072 | tf_op jit(solution)/shard_map/all_to_all | solution.py:472
  96.3 13.7 %all_to_all.40 = bf16[32,32,128]{2,1,0:T(8,128)(2,1)S(1)} all-to-all(bf16[32,32,128]{2,1,0:T(8,128)(2,1)S(1)} %add1.1), channel_id=1, replica_groups=mesh['z'=8,'y'=4,'x'=4,'c'=2] {'y','x','c'}, dimensions={0} | all-to-all | bytes 524288 | tf_op jit(solution)/shard_map/all_to_all | solution.py:472
  110.0 0.7 copy_bitcast_fusion
  (1 shorter events, 0.0 us)
Async XLA Ops:
  0.6 5.2 %collective-permute-start = (bf16[2,4,4096]{2,1,0:T(4,128)(2,1)}, bf16[2,4,4096]{2,1,0:T(4,128)(2,1)S(1)}, u32[]{:S(2)}, u32[]{:S(2)}) collective-permute-start(bf16[2,4,4096]{2,1,0:T(4,128)(2,1)} %bitcast.25), channel_id=1, source_target_pairs={{0,1},{1,0},{2,3},{3,2},{4,5},{5,4},{6,7},{7,6},{8,9},{9,8},{10,11... | collective-permute-start | bytes 196616 | tf_op jit(solution)/shard_map/ppermute | solution.py:476
  3.9 1.9 %collective-permute-start.1 = (bf16[2,4,4096]{2,1,0:T(4,128)(2,1)}, bf16[2,4,4096]{2,1,0:T(4,128)(2,1)S(1)}, u32[]{:S(2)}, u32[]{:S(2)}) collective-permute-start(bf16[2,4,4096]{2,1,0:T(4,128)(2,1)} %bitcast.28), channel_id=1, source_target_pairs={{0,1},{1,0},{2,3},{3,2},{4,5},{5,4},{6,7},{7,6},{8,9},{9,8},{10,11... | collective-permute-start | bytes 196616 | tf_op jit(solution)/shard_map/ppermute | solution.py:476
  4.0 1.8 %collective-permute-start.2 = (f32[2,2,2,4,32]{4,3,2,1,0:T(4,128)}, f32[2,2,2,4,32]{4,3,2,1,0:T(4,128)S(1)}, u32[]{:S(2)}, u32[]{:S(2)}) collective-permute-start(f32[2,2,2,4,32]{4,3,2,1,0:T(4,128)} %bitcast.31), channel_id=1, source_target_pairs={{0,1},{1,0},{2,3},{3,2},{4,5},{5,4},{6,7},{7,6},{8,9},{9,8},{10,11... | collective-permute-start | bytes 12296 | tf_op jit(solution)/shard_map/ppermute | solution.py:476
  4.4 1.4 %collective-permute-start.3 = (f32[2,3,2,4]{3,2,1,0:T(2,128)}, f32[2,3,2,4]{3,2,1,0:T(2,128)S(1)}, u32[]{:S(2)}, u32[]{:S(2)}) collective-permute-start(f32[2,3,2,4]{3,2,1,0:T(2,128)} %refs_3_.1), channel_id=1, source_target_pairs={{0,1},{1,0},{2,3},{3,2},{4,5},{5,4},{6,7},{7,6},{8,9},{9,8},{10,11... | collective-permute-start | bytes 584 | tf_op jit(solution)/shard_map/ppermute | solution.py:476
  6.9 25.0 %all-to-all-start = ((bf16[128,4,128]{2,1,0:T(4,128)(2,1)}), bf16[128,4,128]{2,1,0:T(4,128)(2,1)S(1)}, u32[]{:S(2)}, u32[]{:S(2)}) async-start(bf16[128,4,128]{2,1,0:T(4,128)(2,1)} %get-tuple-element.43), calls=%async_computation | async-start | bytes 262144 | tf_op jit(solution)/shard_map/all_to_all | solution.py:472
  68.3 4.0 %collective-permute-start.4 = (bf16[16,96,128]{2,1,0:T(8,128)(2,1)S(1)}, bf16[16,96,128]{2,1,0:T(8,128)(2,1)S(1)}, u32[]{:S(2)}, u32[]{:S(2)}) collective-permute-start(bf16[16,96,128]{2,1,0:T(8,128)(2,1)S(1)} %all_to_all.37.own.hid), channel_id=1, source_target_pairs={{0,1},{1,0},{2,3},{3,2},{4,5},{5,4},{6,7},{7,6},{8,9},{9,8},{10,11... | collective-permute-start | bytes 1179656 | tf_op jit(solution)/shard_map/ppermute | solution.py:476

commit v8 on v7

--- a/solution.py
+++ b/solution.py
@@ -14,6 +14,11 @@
 N = 128
 GW = 1024
 LINES = B + 2
+FIRST_SPOT = 64
+FIRST_MEMBER = 1
+FIRST_PLANE = 4
+FIRST_CHIP = 0
+LAST_MEMBER = 21
 EPS = 1e-06
 TP = ("z", "y", "x", "c")
 PLANE = ("y", "x", "c")
@@ -153,7 +158,8 @@
             tail = jnp.where(lane == at, col, tail)
         second = jnp.concatenate([*mixed_lo, tail, jnp.zeros((4, B), F32)], axis=1)
         base = [jnp.where(row == 2, first[col : col + 1], second[col : col + 1]) for col in range(4)]
-        start = 64 * (1 - core if of else core)
+        side = 1 - core if of else core
+        start = 64 * (1 - side if FIRST_SPOT & 64 else side)
         for place in range(16):
             cols = pl.ds(pl.multiple_of(128 * (2 * place + core), 128), 128)
             writes = w_write[1, :, cols].astype(F32)
@@ -161,7 +167,7 @@
             for col in range(4):
                 one = slice(col, col + 1)
                 tile = jnp.where(row == 0, writes[one], jnp.where(row == 1, reads[one], base[col]))
-                msg[start + 16 * col + place] = tile.astype(BF16)
+                msg[start + ((16 * col + place) ^ (FIRST_SPOT & 63))] = tile.astype(BF16)
 
 
 def make_keys(scaled, inv, own, other):
@@ -258,7 +264,7 @@
     stack[2 * CH + 8 :] = both.astype(BF16)
     for place in range(16):
         for side in range(2):
-            at = 128 * (2 * place + side)
+            at = 128 * (2 * (place ^ FIRST_CHIP) + side)
             halves[side, :, 128 * place : 128 * place + 128] = stack[:, at : at + 128]
     packed[3] = jnp.broadcast_to(as_col(row_of(kept[2], 0)), (CH, B))
     ready[0] = (conv[1, :, 0, :] * tap[1][0] + conv[1, :, 1, :] * tap[1][1]).T
@@ -306,8 +312,9 @@
     tail = jnp.concatenate([tail, jnp.zeros((2, 128 - B), F32)], axis=1).astype(BF16)
     out = jnp.dot((gated * gain).T.astype(BF16), w_out[...], preferred_element_type=F32)
     for j in range(D // 128):
-        sent[LINES * j : LINES * j + B] = out[:, 128 * j : 128 * j + 128].astype(BF16)
-        sent[LINES * j + B : LINES * (j + 1)] = tail
+        to = LINES * (j ^ FIRST_MEMBER)
+        sent[to : to + B] = out[:, 128 * j : 128 * j + 128].astype(BF16)
+        sent[to + B : to + LINES] = tail
     for copy in copies:
         copy.wait()
 
@@ -324,7 +331,11 @@
 
 
 def first_mix_kernel(keys, packed, decay, state, w_out, states, sent, weights, later, last_taps, lines, *scratch):
-    lines[...] = keys[...].astype(F32)
+    for at in range(0, 4 * N, 16):
+        pair = keys[at : at + 16].astype(F32)
+        for half in range(2):
+            to = (at + 8 * half) ^ (4 * FIRST_SPOT)
+            lines[to : to + 8] = pair[8 * half : 8 * half + 8]
     weights[0] = lines[pl.ds(0, N, stride=4), :].astype(BF16)
     weights[1] = lines[pl.ds(1, N, stride=4), :].astype(BF16)
     first = lines[pl.ds(2, N, stride=4), :].T
@@ -359,7 +370,7 @@
 
 def take_half(half, side, norm_gain, weights, scaled, squares, sums):
     for at in range(16):
-        cols = pl.ds(pl.multiple_of(128 * (2 * at + side), 128), 128)
+        cols = pl.ds(pl.multiple_of(128 * (2 * (at ^ FIRST_CHIP) + side), 128), 128)
         part = half[at, :B].astype(F32)
         squares += part * part
         scaled[:, 128 * at : 128 * at + 128] = (part * norm_gain[1:, cols]).astype(BF16)
@@ -463,13 +474,24 @@
     total = got[0].astype(F32)
     for plane in range(1, 8):
         total += got[plane].astype(F32)
-    chunk = (hid[lax.axis_index(("y", "x")), :B].astype(F32) + total).astype(BF16)
+    chunk = (hid[lax.axis_index(("y", "x")) ^ FIRST_CHIP, :B].astype(F32) + total).astype(BF16)
     for j in range(32):
         sent[j] = chunk
 
 
-def exchange(value, axes):
-    return lax.all_to_all(value, axes, split_axis=0, concat_axis=0, tiled=True)
+def tokens_kernel(got, tokens_out):
+    for j in range(32):
+        at = 128 * (j ^ LAST_MEMBER)
+        tokens_out[:, at : at + 128] = got[j]
+
+
+def make_tokens(got):
+    return call(tokens_kernel, "tokens", [got], [], [shaped((B, D), BF16)])[0]
+
+
+def exchange(value, axes, first):
+    order = [spot ^ first for spot in range(value.shape[0])]
+    return lax.all_to_all(value, axes, 0, 0, axis_index_groups=[order], tiled=True)
 
 
 def swap(value):
@@ -504,28 +526,28 @@
     others = [swap(v) for v in key_far]
     scaled, inv, hid, *own = make_start(tokens, norm_gain, key_far)
     msg, key_out = make_keys(scaled, inv, own, others)
-    keys = exchange(msg, ("z", "y", "x")).reshape(4 * N, 128)
+    keys = exchange(msg, ("z", "y", "x"), FIRST_SPOT).reshape(4 * N, 128)
     packed, decay, value_out, halves, ready, *kept = make_values(scaled, inv, far)
     state, out, gain, next_state, next_out, *rest = kept
     states, sent, weights, later, last_taps = first_mix(keys, packed, decay, [state, out])
-    sent = make_scale(exchange(sent.reshape(32, LINES // 2, 2, 128), PLANE).reshape(sent.shape))
+    sent = make_scale(exchange(sent.reshape(32, LINES // 2, 2, 128), PLANE, FIRST_MEMBER).reshape(sent.shape))
     (sent,) = call(
         first_add_kernel,
         "add0",
-        [exchange(sent, ("z",)), hid, rest[0], weights],
+        [exchange(sent, ("z",), FIRST_PLANE), hid, rest[0], weights],
         [],
         [pltpu.VMEM((16, 3 * B, 128), BF16)],
     )
-    own = exchange(sent, ("y", "x"))
+    own = exchange(sent, ("y", "x"), FIRST_CHIP)
     other = swap(own)
     norm_far, conv, key_conv = rest[0], rest[4], rest[6]
     half = make_half(own, halves, norm_far)
     near = [other, halves, norm_far, *half, ready, later, last_taps, next_state, next_out]
     states, sent, key_out, value_out = next_mix([*near, conv, key_conv, key_out, value_out], states)
-    sent = make_scale(exchange(sent.reshape(32, LINES // 2, 2, 128), PLANE).reshape(sent.shape))
-    (sent,) = call(next_add_kernel, "add1", [exchange(sent, ("z",)), own], [], [pltpu.VMEM((32, B, 128), BF16)])
-    hid = exchange(sent, PLANE)
-    tokens_out = jnp.transpose(hid, (1, 0, 2)).reshape(B, D)
+    sent = make_scale(exchange(sent.reshape(32, LINES // 2, 2, 128), PLANE, FIRST_MEMBER).reshape(sent.shape))
+    (sent,) = call(next_add_kernel, "add1", [exchange(sent, ("z",), FIRST_PLANE), own], [], [pltpu.VMEM((32, B, 128), BF16)])
+    hid = exchange(sent, PLANE, LAST_MEMBER)
+    tokens_out = make_tokens(hid)
     return (tokens_out, states, value_out, jnp.transpose(key_out, (0, 4, 1, 2, 3)))
 
 

time: 111 us -> 105 us (0.946)
  waiting for transfers between devices: 8.39 us -> 4.59 us
  blocking collectives: 70.5 us -> 68.2 us
    all_to_all x1, waiting for transfers between devices: 7.26 us -> 3.45 us  [exchange(): lax.all_to_all(value, axes, 0, 0, axis_index_groups=[order], tiled=True)]
    all_to_all x6, blocking collectives: 70.5 us -> 68.2 us  [exchange(): lax.all_to_all(value, axes, 0, 0, axis_index_groups=[order], tiled=True)]
    pallas_call x10 -> x11, Pallas kernels: 10.1 us -> 10.8 us  [call(): pl.pallas_call(body, in_specs=[vmem()] * len(near) + [anywhere()] * len(f...]
where the time goes in v8:
time: 105 us
  blocking collectives  68.2 us (65%)
  starting transfers between devices  20.7 us (20%)
  Pallas kernels  10.8 us (10%)
  waiting for transfers between devices  4.59 us (4%)
    all_to_all x6, blocking collectives, exchange(): lax.all_to_all(value, axes, 0, 0, axis_index_groups=[order], tiled=True)  68.2 us
    all_to_all x1, starting transfers between devices, exchange(): lax.all_to_all(value, axes, 0, 0, axis_index_groups=[order], tiled=True)  14.9 us
    pallas_call x11, Pallas kernels, call(): pl.pallas_call(body, in_specs=[vmem()] * len(near) + [anywhere()] * len(f...  10.8 us
    ppermute x5, starting transfers between devices, swap(): return lax.ppermute(value, 'c', [(0, 1), (1, 0)])  5.85 us
    all_to_all x1, waiting for transfers between devices, exchange(): lax.all_to_all(value, axes, 0, 0, axis_index_groups=[order], tiled=True)  3.45 us
  transfers between devices with their start and end apart: 6, of which 2 were waited for; matrix products, arithmetic and copies ran while one was open for 0% of the time, Pallas kernels for 5%

profile of v8, /device:TPU:1, one launch (start us, length us, event | category | flops | bytes accessed | tf_op | source)
XLA Modules:
  0.0 105.1 jit_solution(8585522705659924464)
XLA Ops:
  0.6 3.3 %collective-permute-start = (bf16[2,4,4096]{2,1,0:T(4,128)(2,1)}, bf16[2,4,4096]{2,1,0:T(4,128)(2,1)S(1)}, u32[]{:S(2)}, u32[]{:S(2)}) collective-permute-start(bf16[2,4,4096]{2,1,0:T(4,128)(2,1)} %bitcast.19), channel_id=1, source_target_pairs={{0,1},{1,0},{2,3},{3,2},{4,5},{5,4},{6,7},{7,6},{8,9},{9,8},{10,11... | collective-permute-start | bytes 196616 | tf_op jit(solution)/shard_map/ppermute | solution.py:498
  3.9 0.1 collective-permute-start.1
  4.0 0.4 collective-permute-start.2
  4.4 0.1 collective-permute-start.3
  4.5 1.2 %start.1 = (bf16[32,4096]{1,0:T(8,128)(2,1)S(1)}, f32[32,128]{1,0:T(8,128)S(1)}, bf16[32,4096]{1,0:T(8,128)(2,1)S(1)}, bf16[2,4,4096]{2,1,0:T(4,128)(2,1)S(1)}, ...) custom-call(bf16[32,4096]{1,0:T(8,128)(2,1)} %tokens.2, ...), custom_call_target="tpu_custom_call" | custom-call | tf_op jit(solution)/shard_map/start/pallas_call | solution.py:56
  5.8 0.0 collective-permute-done.3.refs_7_
  5.8 0.0 collective-permute-done.2.refs_6_
  5.8 0.0 collective-permute-done.refs_4_
  5.8 0.0 collective-permute-done.1.refs_5_
  5.8 1.0 keys.1
  6.9 14.9 %all-to-all-start = ((bf16[128,4,128]{2,1,0:T(4,128)(2,1)}), bf16[128,4,128]{2,1,0:T(4,128)(2,1)S(1)}, u32[]{:S(2)}, u32[]{:S(2)}) async-start(bf16[128,4,128]{2,1,0:T(4,128)(2,1)} %get-tuple-element.43), calls=%async_computation | async-start | bytes 262144 | tf_op jit(solution)/shard_map/all_to_all | solution.py:494
  21.7 3.9 %values.1 = (f32[4,32,32]{2,1,0:T(8,128)S(1)}, f32[32,128]{1,0:T(8,128)S(1)}, f32[32,2,32]{2,1,0:T(2,128)S(1)}, bf16[2,80,2048]{2,1,0:T(8,128)(2,1)S(1)}, f32[4,...) custom-call(bf16[32,4096]{1,0:T(8,128)(2,1)S(1)} %get-tuple-element., ...), custom_call_target="tpu_custom_call" | custom-call | tf_op jit(solution)/shard_map/values/pallas_call | solution.py:56
  25.7 3.5 %all-to-all-done = bf16[128,4,128]{2,1,0:T(4,128)(2,1)S(1)} async-done(((bf16[128,4,128]{2,1,0:T(4,128)(2,1)}), bf16[128,4,128]{2,1,0:T(4,128)(2,1)S(1)}, u32[]{:S(2)}, u32[]{:S(2)}) %all-to-all-start) | async-done | bytes 131104 | tf_op jit(solution)/shard_map/all_to_all | solution.py:494
  29.1 1.1 %mix0.1 = (f32[2,32,32,128]{3,2,1,0:T(8,128)}, bf16[1088,128]{1,0:T(8,128)(2,1)S(1)}, bf16[2,128,128]{2,1,0:T(8,128)(2,1)S(1)}, f32[2,32,128]{2,1,0:T(8,128)S(1)}, f32[8,128]{1,0:T(8,128)S(1)}) custom-call(bf16[512,128]{1,0:T(8,128)(2,1)S(1)} %bitcast.14, f32[4,32,32]{2,1,0:T(8,128)S(1)} %get-tuple-element.44.packed, f32[32,128]{1,0:T(8,128)S(1)} %get-tuple-element.45.decay, ...), custom_call_target="tpu_custom_call" | custom-call | tf_op jit(solution)/shard_map/mix0/pallas_call | solution.py:56
  30.2 13.4 %all_to_all.35 = bf16[32,17,2,128]{3,2,1,0:T(2,128)(2,1)S(1)} all-to-all(bf16[32,17,2,128]{3,2,1,0:T(2,128)(2,1)S(1)} %bitcast.16), channel_id=1, replica_groups={{1,0,3,2,5,4,7,6,9,8,11,10,13,12,15,14,17,16,19,18,21,20,23,22,25,24,27..., dimensions={0} | all-to-all | bytes 557056 | tf_op jit(solution)/shard_map/all_to_all | solution.py:494
  43.6 0.1 scale.2
  43.8 9.3 %all_to_all.36.got = bf16[8,32,128]{2,1,0:T(8,128)(2,1)S(1)} all-to-all(bf16[8,32,128]{2,1,0:T(8,128)(2,1)S(1)} %scale.2), channel_id=1, replica_groups={{128,160,192,224,0,32,64,96},{129,161,193,225,1,33,65,97},{130,162,194,..., dimensions={0} | all-to-all | bytes 131072 | tf_op jit(solution)/shard_map/all_to_all | solution.py:494
  53.0 0.2 add0.1
  53.2 12.2 %all_to_all.37.own.hid = bf16[16,96,128]{2,1,0:T(8,128)(2,1)S(1)} all-to-all(bf16[16,96,128]{2,1,0:T(8,128)(2,1)S(1)} %add0.1), channel_id=1, replica_groups={{0,2,4,6,8,10,12,14,16,18,20,22,24,26,28,30},{1,3,5,7,9,11,13,15,17,19,..., dimensions={0} | all-to-all | bytes 786432 | tf_op jit(solution)/shard_map/all_to_all | solution.py:494
  65.4 2.0 %collective-permute-start.4 = (bf16[16,96,128]{2,1,0:T(8,128)(2,1)S(1)}, bf16[16,96,128]{2,1,0:T(8,128)(2,1)S(1)}, u32[]{:S(2)}, u32[]{:S(2)}) collective-permute-start(bf16[16,96,128]{2,1,0:T(8,128)(2,1)S(1)} %all_to_all.37.own.hid), channel_id=1, source_target_pairs={{0,1},{1,0},{2,3},{3,2},{4,5},{5,4},{6,7},{7,6},{8,9},{9,8},{10,11... | collective-permute-start | bytes 1179656 | tf_op jit(solution)/shard_map/ppermute | solution.py:498
  67.3 0.2 half.1
  67.6 1.1 %collective-permute-done.4.other = bf16[16,96,128]{2,1,0:T(8,128)(2,1)S(1)} collective-permute-done((bf16[16,96,128]{2,1,0:T(8,128)(2,1)S(1)}, bf16[16,96,128]{2,1,0:T(8,128)(2,1)S(1)}, u32[]{:S(2)}, u32[]{:S(2)}) %collective-permute-start.4) | collective-permute-done | bytes 393248 | tf_op jit(solution)/shard_map/ppermute | solution.py:498
  68.7 2.1 %mix1.1 = (f32[2,32,32,128]{3,2,1,0:T(8,128)}, bf16[1088,128]{1,0:T(8,128)(2,1)S(1)}, f32[2,2,2,4,32]{4,3,2,1,0:T(4,128)}, f32[2,32,2,32]{3,2,1,0:T(2,128)}) custom-call(bf16[16,96,128]{2,1,0:T(8,128)(2,1)S(1)} %collective-permute-done.4.other, bf16[2,80,2048]{2,1,0:T(8,128)(2,1)S(1)} %get-tuple-element.52.weights, ...), custom_call_target="tpu_custom_call", output_to_operand_aliasing={{0}: (15, {})} | custom-call | tf_op jit(solution)/shard_map/mix1/pallas_call | solution.py:56
  70.8 12.1 %all_to_all.38 = bf16[32,17,2,128]{3,2,1,0:T(2,128)(2,1)S(1)} all-to-all(bf16[32,17,2,128]{3,2,1,0:T(2,128)(2,1)S(1)} %bitcast.15), channel_id=1, replica_groups={{1,0,3,2,5,4,7,6,9,8,11,10,13,12,15,14,17,16,19,18,21,20,23,22,25,24,27..., dimensions={0} | all-to-all | bytes 557056 | tf_op jit(solution)/shard_map/all_to_all | solution.py:494
  82.9 0.1 scale.3
  83.0 9.6 %all_to_all.39.got = bf16[8,32,128]{2,1,0:T(8,128)(2,1)S(1)} all-to-all(bf16[8,32,128]{2,1,0:T(8,128)(2,1)S(1)} %scale.3), channel_id=1, replica_groups={{128,160,192,224,0,32,64,96},{129,161,193,225,1,33,65,97},{130,162,194,..., dimensions={0} | all-to-all | bytes 131072 | tf_op jit(solution)/shard_map/all_to_all | solution.py:494
  92.6 11.7 %all_to_all.40.got = bf16[32,32,128]{2,1,0:T(8,128)(2,1)S(1)} all-to-all(bf16[32,32,128]{2,1,0:T(8,128)(2,1)S(1)} %add1.1), channel_id=1, replica_groups={{21,20,23,22,17,16,19,18,29,28,31,30,25,24,27,26,5,4,7,6,1,0,3,2,13,12,..., dimensions={0} | all-to-all | bytes 524288 | tf_op jit(solution)/shard_map/all_to_all | solution.py:494
  104.3 0.7 tokens.3
  (1 shorter events, 0.0 us)
Async XLA Ops:
  0.6 5.2 %collective-permute-start = (bf16[2,4,4096]{2,1,0:T(4,128)(2,1)}, bf16[2,4,4096]{2,1,0:T(4,128)(2,1)S(1)}, u32[]{:S(2)}, u32[]{:S(2)}) collective-permute-start(bf16[2,4,4096]{2,1,0:T(4,128)(2,1)} %bitcast.19), channel_id=1, source_target_pairs={{0,1},{1,0},{2,3},{3,2},{4,5},{5,4},{6,7},{7,6},{8,9},{9,8},{10,11... | collective-permute-start | bytes 196616 | tf_op jit(solution)/shard_map/ppermute | solution.py:498
  3.9 1.9 %collective-permute-start.1 = (bf16[2,4,4096]{2,1,0:T(4,128)(2,1)}, bf16[2,4,4096]{2,1,0:T(4,128)(2,1)S(1)}, u32[]{:S(2)}, u32[]{:S(2)}) collective-permute-start(bf16[2,4,4096]{2,1,0:T(4,128)(2,1)} %bitcast.22), channel_id=1, source_target_pairs={{0,1},{1,0},{2,3},{3,2},{4,5},{5,4},{6,7},{7,6},{8,9},{9,8},{10,11... | collective-permute-start | bytes 196616 | tf_op jit(solution)/shard_map/ppermute | solution.py:498
  4.0 1.8 %collective-permute-start.2 = (f32[2,2,2,4,32]{4,3,2,1,0:T(4,128)}, f32[2,2,2,4,32]{4,3,2,1,0:T(4,128)S(1)}, u32[]{:S(2)}, u32[]{:S(2)}) collective-permute-start(f32[2,2,2,4,32]{4,3,2,1,0:T(4,128)} %bitcast.25), channel_id=1, source_target_pairs={{0,1},{1,0},{2,3},{3,2},{4,5},{5,4},{6,7},{7,6},{8,9},{9,8},{10,11... | collective-permute-start | bytes 12296 | tf_op jit(solution)/shard_map/ppermute | solution.py:498
  4.4 1.4 %collective-permute-start.3 = (f32[2,3,2,4]{3,2,1,0:T(2,128)}, f32[2,3,2,4]{3,2,1,0:T(2,128)S(1)}, u32[]{:S(2)}, u32[]{:S(2)}) collective-permute-start(f32[2,3,2,4]{3,2,1,0:T(2,128)} %refs_3_.1), channel_id=1, source_target_pairs={{0,1},{1,0},{2,3},{3,2},{4,5},{5,4},{6,7},{7,6},{8,9},{9,8},{10,11... | collective-permute-start | bytes 584 | tf_op jit(solution)/shard_map/ppermute | solution.py:498
  6.9 22.2 %all-to-all-start = ((bf16[128,4,128]{2,1,0:T(4,128)(2,1)}), bf16[128,4,128]{2,1,0:T(4,128)(2,1)S(1)}, u32[]{:S(2)}, u32[]{:S(2)}) async-start(bf16[128,4,128]{2,1,0:T(4,128)(2,1)} %get-tuple-element.43), calls=%async_computation | async-start | bytes 262144 | tf_op jit(solution)/shard_map/all_to_all | solution.py:494
  65.4 3.3 %collective-permute-start.4 = (bf16[16,96,128]{2,1,0:T(8,128)(2,1)S(1)}, bf16[16,96,128]{2,1,0:T(8,128)(2,1)S(1)}, u32[]{:S(2)}, u32[]{:S(2)}) collective-permute-start(bf16[16,96,128]{2,1,0:T(8,128)(2,1)S(1)} %all_to_all.37.own.hid), channel_id=1, source_target_pairs={{0,1},{1,0},{2,3},{3,2},{4,5},{5,4},{6,7},{7,6},{8,9},{9,8},{10,11... | collective-permute-start | bytes 1179656 | tf_op jit(solution)/shard_map/ppermute | solution.py:498

commit v9 on v8

--- a/solution.py
+++ b/solution.py
@@ -368,24 +368,32 @@
     )
 
 
-def take_half(half, side, norm_gain, weights, scaled, squares, sums):
+def pack_kernel(own, packed):
+    sums = [own[0, B * k : B * (k + 1)].astype(F32) for k in (1, 2)]
+    packed[0] = own[0, :B]
+    for at in range(1, 16):
+        packed[at] = own[at, :B]
+        for kind in range(2):
+            sums[kind] += own[at, B * (kind + 1) : B * (kind + 2)].astype(F32)
+    for kind in range(2):
+        packed[16 + kind] = sums[kind].astype(BF16)
+
+
+def take_half(half, side, norm_gain, weights, scaled, squares):
     for at in range(16):
         cols = pl.ds(pl.multiple_of(128 * (2 * (at ^ FIRST_CHIP) + side), 128), 128)
-        part = half[at, :B].astype(F32)
+        part = half[at].astype(F32)
         squares += part * part
         scaled[:, 128 * at : 128 * at + 128] = (part * norm_gain[1:, cols]).astype(BF16)
-        for kind in range(2):
-            sums[kind] += half[at, B * (kind + 1) : B * (kind + 2)].astype(F32)
-    return squares, sums, dot_nt(weights[side], scaled[...])
+    return squares, dot_nt(weights[side], scaled[...])
 
 
 def half_kernel(own, weights, norm_gain, found_out, squares_out, sums_out, scaled):
-    zero = jnp.zeros((B, N), F32)
-    squares, sums, found = take_half(own, lax.axis_index("c"), norm_gain, weights, scaled, zero, [zero, zero])
+    squares, found = take_half(own, lax.axis_index("c"), norm_gain, weights, scaled, jnp.zeros((B, N), F32))
     found_out[...] = found
     squares_out[...] = squares
-    sums_out[0] = sums[0]
-    sums_out[1] = sums[1]
+    sums_out[0] = own[16].astype(F32)
+    sums_out[1] = own[17].astype(F32)
 
 
 HALF = ((B, D // 2), BF16)
@@ -399,9 +407,8 @@
 def next_mix_kernel(other, weights, norm_gain, found, squares, sums, ready, later, last_taps, state, w_out, *refs):
     conv, key_conv, key_before, value_before = refs[:4]
     states, sent, key_out, value_out, scaled, *scratch = refs[5:]
-    squares, sums, rest = take_half(
-        other, 1 - lax.axis_index("c"), norm_gain, weights, scaled, squares[...], [sums[0], sums[1]]
-    )
+    squares, rest = take_half(other, 1 - lax.axis_index("c"), norm_gain, weights, scaled, squares[...])
+    sums = [sums[k] + other[16 + k].astype(F32) for k in range(2)]
     inv = lax.rsqrt(jnp.sum(squares, axis=1, keepdims=True) / D + EPS)
     found = (found[...] + rest) * as_row(inv)
     keys = [silu(later[k] + sums[k] * inv * (last_taps[2 * k : 2 * k + 1] + last_taps[2 * k + 1 : 2 * k + 2])) for k in range(2)]
@@ -474,7 +481,7 @@
     total = got[0].astype(F32)
     for plane in range(1, 8):
         total += got[plane].astype(F32)
-    chunk = (hid[lax.axis_index(("y", "x")) ^ FIRST_CHIP, :B].astype(F32) + total).astype(BF16)
+    chunk = (hid[lax.axis_index(("y", "x")) ^ FIRST_CHIP].astype(F32) + total).astype(BF16)
     for j in range(32):
         sent[j] = chunk
 
@@ -539,6 +546,7 @@
         [pltpu.VMEM((16, 3 * B, 128), BF16)],
     )
     own = exchange(sent, ("y", "x"), FIRST_CHIP)
+    (own,) = call(pack_kernel, "pack", [own], [], [pltpu.VMEM((18, B, 128), BF16)])
     other = swap(own)
     norm_far, conv, key_conv = rest[0], rest[4], rest[6]
     half = make_half(own, halves, norm_far)

time: 105 us -> 105 us (level)
    pallas_call x11 -> x12, Pallas kernels: 10.8 us -> 10.9 us  [call(): pl.pallas_call(body, in_specs=[vmem()] * len(near) + [anywhere()] * len(f...]
where the time goes in v9:
time: 105 us
  blocking collectives  68.2 us (65%)
  starting transfers between devices  20.8 us (20%)
  Pallas kernels  10.9 us (10%)
  waiting for transfers between devices  4.25 us (4%)
    all_to_all x6, blocking collectives, exchange(): lax.all_to_all(value, axes, 0, 0, axis_index_groups=[order], tiled=True)  68.2 us
    all_to_all x1, starting transfers between devices, exchange(): lax.all_to_all(value, axes, 0, 0, axis_index_groups=[order], tiled=True)  14.9 us
    pallas_call x12, Pallas kernels, call(): pl.pallas_call(body, in_specs=[vmem()] * len(near) + [anywhere()] * len(f...  10.9 us
    ppermute x5, starting transfers between devices, swap(): return lax.ppermute(value, 'c', [(0, 1), (1, 0)])  5.94 us
    all_to_all x1, waiting for transfers between devices, exchange(): lax.all_to_all(value, axes, 0, 0, axis_index_groups=[order], tiled=True)  3.45 us
  transfers between devices with their start and end apart: 6, of which 2 were waited for; matrix products, arithmetic and copies ran while one was open for 0% of the time, Pallas kernels for 5%

profile of v9, /device:TPU:1, one launch (start us, length us, event | category | flops | bytes accessed | tf_op | source)
XLA Modules:
  0.0 104.9 jit_solution(926028257218133668)
XLA Ops:
  0.6 3.3 %collective-permute-start = (bf16[2,4,4096]{2,1,0:T(4,128)(2,1)}, bf16[2,4,4096]{2,1,0:T(4,128)(2,1)S(1)}, u32[]{:S(2)}, u32[]{:S(2)}) collective-permute-start(bf16[2,4,4096]{2,1,0:T(4,128)(2,1)} %bitcast.19), channel_id=1, source_target_pairs={{0,1},{1,0},{2,3},{3,2},{4,5},{5,4},{6,7},{7,6},{8,9},{9,8},{10,11... | collective-permute-start | bytes 196616 | tf_op jit(solution)/shard_map/ppermute | solution.py:505
  3.9 0.1 collective-permute-start.1
  4.0 0.4 collective-permute-start.2
  4.4 0.1 collective-permute-start.3
  4.5 1.2 %start.1 = (bf16[32,4096]{1,0:T(8,128)(2,1)S(1)}, f32[32,128]{1,0:T(8,128)S(1)}, bf16[32,4096]{1,0:T(8,128)(2,1)S(1)}, bf16[2,4,4096]{2,1,0:T(4,128)(2,1)S(1)}, ...) custom-call(bf16[32,4096]{1,0:T(8,128)(2,1)} %tokens.2, ...), custom_call_target="tpu_custom_call" | custom-call | tf_op jit(solution)/shard_map/start/pallas_call | solution.py:56
  5.8 0.0 collective-permute-done.3.refs_7_
  5.8 0.0 collective-permute-done.2.refs_6_
  5.8 0.0 collective-permute-done.refs_4_
  5.8 0.0 collective-permute-done.1.refs_5_
  5.8 1.0 keys.1
  6.9 14.9 %all-to-all-start = ((bf16[128,4,128]{2,1,0:T(4,128)(2,1)}), bf16[128,4,128]{2,1,0:T(4,128)(2,1)S(1)}, u32[]{:S(2)}, u32[]{:S(2)}) async-start(bf16[128,4,128]{2,1,0:T(4,128)(2,1)} %get-tuple-element.43), calls=%async_computation | async-start | bytes 262144 | tf_op jit(solution)/shard_map/all_to_all | solution.py:501
  21.7 3.9 %values.1 = (f32[4,32,32]{2,1,0:T(8,128)S(1)}, f32[32,128]{1,0:T(8,128)S(1)}, f32[32,2,32]{2,1,0:T(2,128)S(1)}, bf16[2,80,2048]{2,1,0:T(8,128)(2,1)S(1)}, f32[4,...) custom-call(bf16[32,4096]{1,0:T(8,128)(2,1)S(1)} %get-tuple-element., ...), custom_call_target="tpu_custom_call" | custom-call | tf_op jit(solution)/shard_map/values/pallas_call | solution.py:56
  25.7 3.5 %all-to-all-done = bf16[128,4,128]{2,1,0:T(4,128)(2,1)S(1)} async-done(((bf16[128,4,128]{2,1,0:T(4,128)(2,1)}), bf16[128,4,128]{2,1,0:T(4,128)(2,1)S(1)}, u32[]{:S(2)}, u32[]{:S(2)}) %all-to-all-start) | async-done | bytes 131104 | tf_op jit(solution)/shard_map/all_to_all | solution.py:501
  29.1 1.1 %mix0.1 = (f32[2,32,32,128]{3,2,1,0:T(8,128)}, bf16[1088,128]{1,0:T(8,128)(2,1)S(1)}, bf16[2,128,128]{2,1,0:T(8,128)(2,1)S(1)}, f32[2,32,128]{2,1,0:T(8,128)S(1)}, f32[8,128]{1,0:T(8,128)S(1)}) custom-call(bf16[512,128]{1,0:T(8,128)(2,1)S(1)} %bitcast.14, f32[4,32,32]{2,1,0:T(8,128)S(1)} %get-tuple-element.44.packed, f32[32,128]{1,0:T(8,128)S(1)} %get-tuple-element.45.decay, ...), custom_call_target="tpu_custom_call" | custom-call | tf_op jit(solution)/shard_map/mix0/pallas_call | solution.py:56
  30.2 13.4 %all_to_all.35 = bf16[32,17,2,128]{3,2,1,0:T(2,128)(2,1)S(1)} all-to-all(bf16[32,17,2,128]{3,2,1,0:T(2,128)(2,1)S(1)} %bitcast.16), channel_id=1, replica_groups={{1,0,3,2,5,4,7,6,9,8,11,10,13,12,15,14,17,16,19,18,21,20,23,22,25,24,27..., dimensions={0} | all-to-all | bytes 557056 | tf_op jit(solution)/shard_map/all_to_all | solution.py:501
  43.6 0.1 scale.2
  43.8 9.3 %all_to_all.36.got = bf16[8,32,128]{2,1,0:T(8,128)(2,1)S(1)} all-to-all(bf16[8,32,128]{2,1,0:T(8,128)(2,1)S(1)} %scale.2), channel_id=1, replica_groups={{128,160,192,224,0,32,64,96},{129,161,193,225,1,33,65,97},{130,162,194,..., dimensions={0} | all-to-all | bytes 131072 | tf_op jit(solution)/shard_map/all_to_all | solution.py:501
  53.0 0.2 add0.1
  53.2 12.2 %all_to_all.37.own = bf16[16,96,128]{2,1,0:T(8,128)(2,1)S(1)} all-to-all(bf16[16,96,128]{2,1,0:T(8,128)(2,1)S(1)} %add0.1), channel_id=1, replica_groups={{0,2,4,6,8,10,12,14,16,18,20,22,24,26,28,30},{1,3,5,7,9,11,13,15,17,19,..., dimensions={0} | all-to-all | bytes 786432 | tf_op jit(solution)/shard_map/all_to_all | solution.py:501
  65.4 2.0 %collective-permute-start.4 = (bf16[18,32,128]{2,1,0:T(8,128)(2,1)S(1)}, bf16[18,32,128]{2,1,0:T(8,128)(2,1)S(1)}, u32[]{:S(2)}, u32[]{:S(2)}) collective-permute-start(bf16[18,32,128]{2,1,0:T(8,128)(2,1)S(1)} %pack.1.own.hid), channel_id=1, source_target_pairs={{0,1},{1,0},{2,3},{3,2},{4,5},{5,4},{6,7},{7,6},{8,9},{9,8},{10,11... | collective-permute-start | bytes 442376 | tf_op jit(solution)/shard_map/ppermute | solution.py:505
  67.5 0.2 half.1
  67.7 0.8 collective-permute-done.4.other
  68.5 2.1 %mix1.1 = (f32[2,32,32,128]{3,2,1,0:T(8,128)}, bf16[1088,128]{1,0:T(8,128)(2,1)S(1)}, f32[2,2,2,4,32]{4,3,2,1,0:T(4,128)}, f32[2,32,2,32]{3,2,1,0:T(2,128)}) custom-call(bf16[18,32,128]{2,1,0:T(8,128)(2,1)S(1)} %collective-permute-done.4.other, bf16[2,80,2048]{2,1,0:T(8,128)(2,1)S(1)} %get-tuple-element.52.weights, ...), custom_call_target="tpu_custom_call", output_to_operand_aliasing={{0}: (15, {})} | custom-call | tf_op jit(solution)/shard_map/mix1/pallas_call | solution.py:56
  70.6 12.1 %all_to_all.38 = bf16[32,17,2,128]{3,2,1,0:T(2,128)(2,1)S(1)} all-to-all(bf16[32,17,2,128]{3,2,1,0:T(2,128)(2,1)S(1)} %bitcast.15), channel_id=1, replica_groups={{1,0,3,2,5,4,7,6,9,8,11,10,13,12,15,14,17,16,19,18,21,20,23,22,25,24,27..., dimensions={0} | all-to-all | bytes 557056 | tf_op jit(solution)/shard_map/all_to_all | solution.py:501
  82.7 0.1 scale.3
  82.8 9.6 %all_to_all.39.got = bf16[8,32,128]{2,1,0:T(8,128)(2,1)S(1)} all-to-all(bf16[8,32,128]{2,1,0:T(8,128)(2,1)S(1)} %scale.3), channel_id=1, replica_groups={{128,160,192,224,0,32,64,96},{129,161,193,225,1,33,65,97},{130,162,194,..., dimensions={0} | all-to-all | bytes 131072 | tf_op jit(solution)/shard_map/all_to_all | solution.py:501
  92.4 11.7 %all_to_all.40.got = bf16[32,32,128]{2,1,0:T(8,128)(2,1)S(1)} all-to-all(bf16[32,32,128]{2,1,0:T(8,128)(2,1)S(1)} %add1.1), channel_id=1, replica_groups={{21,20,23,22,17,16,19,18,29,28,31,30,25,24,27,26,5,4,7,6,1,0,3,2,13,12,..., dimensions={0} | all-to-all | bytes 524288 | tf_op jit(solution)/shard_map/all_to_all | solution.py:501
  104.1 0.7 tokens.3
  (2 shorter events, 0.1 us)
Async XLA Ops:
  0.6 5.2 %collective-permute-start = (bf16[2,4,4096]{2,1,0:T(4,128)(2,1)}, bf16[2,4,4096]{2,1,0:T(4,128)(2,1)S(1)}, u32[]{:S(2)}, u32[]{:S(2)}) collective-permute-start(bf16[2,4,4096]{2,1,0:T(4,128)(2,1)} %bitcast.19), channel_id=1, source_target_pairs={{0,1},{1,0},{2,3},{3,2},{4,5},{5,4},{6,7},{7,6},{8,9},{9,8},{10,11... | collective-permute-start | bytes 196616 | tf_op jit(solution)/shard_map/ppermute | solution.py:505
  3.9 1.9 %collective-permute-start.1 = (bf16[2,4,4096]{2,1,0:T(4,128)(2,1)}, bf16[2,4,4096]{2,1,0:T(4,128)(2,1)S(1)}, u32[]{:S(2)}, u32[]{:S(2)}) collective-permute-start(bf16[2,4,4096]{2,1,0:T(4,128)(2,1)} %bitcast.22), channel_id=1, source_target_pairs={{0,1},{1,0},{2,3},{3,2},{4,5},{5,4},{6,7},{7,6},{8,9},{9,8},{10,11... | collective-permute-start | bytes 196616 | tf_op jit(solution)/shard_map/ppermute | solution.py:505
  4.0 1.8 %collective-permute-start.2 = (f32[2,2,2,4,32]{4,3,2,1,0:T(4,128)}, f32[2,2,2,4,32]{4,3,2,1,0:T(4,128)S(1)}, u32[]{:S(2)}, u32[]{:S(2)}) collective-permute-start(f32[2,2,2,4,32]{4,3,2,1,0:T(4,128)} %bitcast.25), channel_id=1, source_target_pairs={{0,1},{1,0},{2,3},{3,2},{4,5},{5,4},{6,7},{7,6},{8,9},{9,8},{10,11... | collective-permute-start | bytes 12296 | tf_op jit(solution)/shard_map/ppermute | solution.py:505
  4.4 1.4 %collective-permute-start.3 = (f32[2,3,2,4]{3,2,1,0:T(2,128)}, f32[2,3,2,4]{3,2,1,0:T(2,128)S(1)}, u32[]{:S(2)}, u32[]{:S(2)}) collective-permute-start(f32[2,3,2,4]{3,2,1,0:T(2,128)} %refs_3_.1), channel_id=1, source_target_pairs={{0,1},{1,0},{2,3},{3,2},{4,5},{5,4},{6,7},{7,6},{8,9},{9,8},{10,11... | collective-permute-start | bytes 584 | tf_op jit(solution)/shard_map/ppermute | solution.py:505
  6.9 22.2 %all-to-all-start = ((bf16[128,4,128]{2,1,0:T(4,128)(2,1)}), bf16[128,4,128]{2,1,0:T(4,128)(2,1)S(1)}, u32[]{:S(2)}, u32[]{:S(2)}) async-start(bf16[128,4,128]{2,1,0:T(4,128)(2,1)} %get-tuple-element.43), calls=%async_computation | async-start | bytes 262144 | tf_op jit(solution)/shard_map/all_to_all | solution.py:501
  65.4 3.0 %collective-permute-start.4 = (bf16[18,32,128]{2,1,0:T(8,128)(2,1)S(1)}, bf16[18,32,128]{2,1,0:T(8,128)(2,1)S(1)}, u32[]{:S(2)}, u32[]{:S(2)}) collective-permute-start(bf16[18,32,128]{2,1,0:T(8,128)(2,1)S(1)} %pack.1.own.hid), channel_id=1, source_target_pairs={{0,1},{1,0},{2,3},{3,2},{4,5},{5,4},{6,7},{7,6},{8,9},{9,8},{10,11... | collective-permute-start | bytes 442376 | tf_op jit(solution)/shard_map/ppermute | solution.py:505
